TPU v7x, 256 devices: a whole 4x4x8 slice. The times are simulated.
256 devices in a mesh: ep: 64 (over z, x, core), tp: 4 (over y).
Axes of the slice: x: 4, y: 4, z: 8, core: 2. Of those that a mesh axis runs over, the one named last changes fastest.
Arguments:
- mix_in: bfloat16 [32768, 2048], P('ep'), may hold values from -6 to 6
- forget_shift: float32 [32768], P('ep'), may hold values from -2.5 to 2.5, as said below
- mix_gain: float32 [2048], replicated, may hold values from 0.1 to 1.9
- w_query: bfloat16 [2048, 1024], P(None, 'tp'), may hold values from -0.125 to 0.125
- w_forget: bfloat16 [2048, 1024], P(None, 'tp'), may hold values from -0.125 to 0.125
- w_value: bfloat16 [2048, 1024], P(None, 'tp'), may hold values from -0.125 to 0.125
- forget_room: float32 [1024], P('tp'), may hold values from 0 to 1, as said below
- head_gain: float32 [1024], P('tp'), may hold values from 0.1 to 1.9
- w_out: bfloat16 [1024, 2048], P('tp'), may hold values from -0.1875 to 0.1875
- moe_in: bfloat16 [16384, 2048], P('ep'), may hold values from -6 to 6
- moe_gain: float32 [2048], replicated, may hold values from 0.1 to 1.9
- expert_choice: int32 [16384, 4], P('ep'), may hold values from 0 to 63, as said below
- route_logit: float32 [16384, 4], P(('ep', 'tp')), may hold values from -6 to 6
- w_exp_gate: bfloat16 [64, 2048, 1024], P('ep', None, 'tp'), may hold values from -0.125 to 0.125
- w_exp_up: bfloat16 [64, 2048, 1024], P('ep', None, 'tp'), may hold values from -0.125 to 0.125
- w_exp_down: bfloat16 [64, 1024, 2048], P('ep', 'tp'), may hold values from -0.1875 to 0.1875
- w_sh_gate: bfloat16 [2048, 512], P(None, 'tp'), may hold values from -0.125 to 0.125
- w_sh_up: bfloat16 [2048, 512], P(None, 'tp'), may hold values from -0.125 to 0.125
- w_sh_down: bfloat16 [512, 2048], P('tp'), may hold values from -0.25 to 0.25
Outputs:
- mixer_out: bfloat16 [32768, 2048], P(('ep', 'tp'))
- moe_out: bfloat16 [16384, 2048], P(('ep', 'tp'))
Inputs may be any that keep to these rules, and one draw needn't show every extreme that they name: `forget_room`: positive and at most 1/6 in every entry. `forget_shift`: constant over each aligned span of 64 positions. `expert_choice`: each row names 4 different experts. In each aligned block of 64 rows no expert is named by more than 6 rows; in every draw one expert is named by exactly 6 rows in every block.
All inputs are finite; a program needn't handle non-finite values.
Results may differ from a plain program's by a relative error of at most 0.02.
Values may be sent and summed in bfloat16 or wider, within the bound.
No kernel may reach another device: no remote copies, remote signals or barrier semaphores. Data moves between devices by JAX's collectives and lax.ppermute only.
A program may use at most 128 MiB of HBM per device.

v0:
```python
import jax
import jax.numpy as jnp
from jax import lax
from jax.sharding import Mesh
from jax.sharding import PartitionSpec as P

HEAD_K = 64
HEAD_V = 64
SPAN = 64
TOP_K = 4
EP = ("ep_0", "ep_1", "ep_2")
EP_TP = ("ep_0", "ep_1", "ep_2", "tp")


epsilon = 1e-06
route_scale = 2.5


def neutral_like(x, identity):
    return jax.tree.map(
        lambda a, e: jnp.broadcast_to(jnp.asarray(e, a.dtype), a.shape), x, identity
    )


def prefix_by_axis(x, axes, combine, identity):
    before = start = neutral_like(x, identity)
    running = x
    for axis in reversed(axes):
        peers, index = (lax.axis_size(axis), lax.axis_index(axis))
        pieces = jax.tree.map(
            lambda part, kind: lax.all_gather(part.astype(kind), axis),
            running,
            (jnp.bfloat16, jnp.bfloat16),
        )
        inside, running = (start, start)
        for k in range(peers):
            passed = k < index
            running = combine(
                running, jax.tree.map(lambda part, own: part[k].astype(own.dtype), pieces, x)
            )
            inside = jax.tree.map(lambda new, old: jnp.where(passed, new, old), running, inside)
        before = combine(inside, before)
    return before


def norm_rows(row_data, gain_vec):
    widened = row_data.astype(jnp.float32)
    scaled = widened * lax.rsqrt(jnp.mean(widened * widened, axis=-1, keepdims=True) + epsilon)
    return (scaled * gain_vec).astype(jnp.bfloat16)


def join_states(earlier, latter):
    return (earlier[0] * latter[0], latter[0][..., None] * earlier[1] + latter[1])


def block_terms(queries, keyed, log_forget, values, span_len):
    token_count, head_count, key_width = queries.shape
    blocks = token_count // span_len
    key_shape = (blocks, span_len, head_count, key_width)
    queries = queries.reshape(key_shape)
    keyed = keyed.reshape(key_shape)
    log_forget = log_forget.reshape(key_shape)
    values = values.reshape(blocks, span_len, head_count, values.shape[-1])
    log_decay = jnp.cumsum(log_forget, axis=1)
    middle = log_decay[:, span_len // 2 : span_len // 2 + 1]
    block_end = log_decay[:, span_len - 1 :]
    scores = jnp.einsum(
        "nthd,nshd->nhts",
        queries * jnp.exp(log_decay - middle),
        keyed * jnp.exp(middle - log_decay),
    )
    causal = jnp.arange(span_len)[:, None] >= jnp.arange(span_len)[None, :]
    scores = jnp.where(causal, scores, 0.0)
    within = jnp.einsum("nhts,nshv->nthv", scores, values)
    query_decay = queries * jnp.exp(log_decay)
    decay_total = jnp.exp(block_end[:, 0])
    state_added = jnp.einsum("nshd,nshv->nhdv", keyed * jnp.exp(block_end - log_decay), values)
    return (within, query_decay, decay_total, state_added)


def local(
    mix_in,
    forget_shift,
    mix_gain,
    w_query,
    w_forget,
    w_value,
    forget_room,
    head_gain,
    w_out,
    moe_in,
    moe_gain,
    expert_choice,
    route_logit,
    w_exp_gate,
    w_exp_up,
    w_exp_down,
    w_sh_gate,
    w_sh_up,
    w_sh_down,
):
    tp_count = lax.axis_size("tp")
    tp_rank = lax.axis_index("tp")
    gate_whole, up_whole, down_whole = (
        lax.all_gather(w_exp_gate, "tp", axis=2, tiled=True),
        lax.all_gather(w_exp_up, "tp", axis=2, tiled=True),
        lax.all_gather(w_exp_down, "tp", axis=1, tiled=True),
    )
    normed = norm_rows(mix_in, mix_gain)
    queries = jax.nn.silu(jnp.dot(normed, w_query, preferred_element_type=jnp.float32))
    before = jnp.dot(normed, w_forget, preferred_element_type=jnp.float32) + forget_shift[:, None]
    values = jnp.dot(normed, w_value, preferred_element_type=jnp.float32)
    forget_rate = forget_room * jax.nn.sigmoid(-before)
    log_forget = jnp.log1p(-forget_rate)
    token_count = normed.shape[0]
    head_count = values.shape[1] // HEAD_V
    key_shape = (token_count, head_count, HEAD_K)
    within, query_decay, decay_total, state_added = block_terms(
        queries.reshape(key_shape),
        forget_rate.reshape(key_shape),
        log_forget.reshape(key_shape),
        values.reshape(token_count, head_count, HEAD_V),
        SPAN,
    )
    run_total, run_added = lax.associative_scan(join_states, (decay_total, state_added), axis=0)
    start_total, start_added = prefix_by_axis(
        (run_total[-1], run_added[-1]),
        EP,
        join_states,
        (jnp.ones_like(run_total[-1]), jnp.zeros_like(run_added[-1])),
    )
    prior_total = jnp.concatenate([jnp.ones_like(run_total[:1]), run_total[:-1]], axis=0)
    prior_added = jnp.concatenate([jnp.zeros_like(run_added[:1]), run_added[:-1]], axis=0)
    state_in = prior_total[..., None] * start_added[None] + prior_added
    mixed = within + jnp.einsum("nthd,nhdv->nthv", query_decay, state_in)
    mixed = mixed.reshape(token_count, head_count, HEAD_V)
    normal = mixed * lax.rsqrt(jnp.mean(mixed * mixed, axis=-1, keepdims=True) + epsilon)
    head_out = (normal * head_gain.reshape(head_count, HEAD_V)).astype(jnp.bfloat16)
    mixer_part = jnp.dot(
        head_out.reshape(token_count, head_count * HEAD_V),
        w_out,
        preferred_element_type=jnp.float32,
    )
    row_count = moe_in.shape[0]
    model_width = moe_in.shape[1]
    quarter = row_count // tp_count
    experts = lax.axis_size(EP) * w_exp_gate.shape[0]
    mean_load = quarter * TOP_K // experts
    capacity = mean_load + mean_load // 2
    hidden = norm_rows(moe_in, moe_gain)
    labels = expert_choice.reshape(tp_count, quarter * TOP_K)
    onehot = (labels[..., None] == jnp.arange(experts, dtype=jnp.int32)).astype(jnp.int32)
    places = jnp.sum(jnp.cumsum(onehot, axis=1) * onehot, axis=-1) - 1
    slot_ids = labels * capacity + places
    own_slots = lax.dynamic_index_in_dim(slot_ids, tp_rank, 0, keepdims=False)
    padded = jnp.concatenate([hidden, jnp.zeros((1, model_width), jnp.bfloat16)], axis=0)
    own_tokens = tp_rank * quarter + jnp.arange(quarter * TOP_K) // TOP_K
    own_source = jnp.full((experts * capacity,), row_count, jnp.int32).at[own_slots].set(own_tokens)
    outgoing = padded[own_source].reshape(1, experts, capacity, model_width)
    group_width = gate_whole.shape[2] // tp_count
    down_groups = down_whole[0].reshape(tp_count, group_width, model_width)
    arrived = lax.all_to_all(outgoing, EP, split_axis=1, concat_axis=1, tiled=True)
    gate_pre = jnp.einsum(
        "qecd,df->qecf", arrived, gate_whole[0], preferred_element_type=jnp.float32
    )
    up_pre = jnp.einsum("qecd,df->qecf", arrived, up_whole[0], preferred_element_type=jnp.float32)
    activations = (jax.nn.silu(gate_pre) * up_pre).astype(jnp.bfloat16)
    grouped = activations.reshape(activations.shape[:3] + (tp_count, group_width))
    partial_value = jnp.einsum(
        "qecgf,gfd->qecgd", grouped, down_groups, preferred_element_type=jnp.float32
    )
    summed = jnp.sum(partial_value.astype(jnp.bfloat16).astype(jnp.float32), axis=3)
    results = lax.all_to_all(
        summed.astype(jnp.bfloat16), EP, split_axis=1, concat_axis=1, tiled=True
    )
    returned_rows = results.reshape(experts * capacity, model_width)
    picked = returned_rows[own_slots].reshape(quarter, TOP_K, model_width).astype(jnp.float32)
    chance = jax.nn.sigmoid(route_logit)
    weights = chance / jnp.sum(chance, axis=-1, keepdims=True) * route_scale
    routed = jnp.sum(weights[..., None] * picked, axis=1)
    shared_gate = jnp.dot(hidden, w_sh_gate, preferred_element_type=jnp.float32)
    shared_up = jnp.dot(hidden, w_sh_up, preferred_element_type=jnp.float32)
    shared_act = (jax.nn.silu(shared_gate) * shared_up).astype(jnp.bfloat16)
    shared_part = jnp.dot(shared_act, w_sh_down, preferred_element_type=jnp.float32)
    mixer_sum, shared_sum = (
        lax.psum_scatter(
            mixer_part.astype(jnp.bfloat16), "tp", scatter_dimension=0, tiled=True
        ).astype(jnp.float32),
        lax.psum_scatter(
            shared_part.astype(jnp.bfloat16), "tp", scatter_dimension=0, tiled=True
        ).astype(jnp.float32),
    )
    return (mixer_sum.astype(jnp.bfloat16), (routed + shared_sum).astype(jnp.bfloat16))


def solution(mesh):
    finer = Mesh(mesh.devices.reshape(8, 4, 2, mesh.shape["tp"]), ("ep_0", "ep_1", "ep_2", "tp"))
    in_specs = (
        P(EP, None),
        P(EP),
        P(),
        P(None, "tp"),
        P(None, "tp"),
        P(None, "tp"),
        P("tp"),
        P("tp"),
        P("tp", None),
        P(EP, None),
        P(),
        P(EP, None),
        P(EP_TP, None),
        P(EP, None, "tp"),
        P(EP, None, "tp"),
        P(EP, "tp", None),
        P(None, "tp"),
        P(None, "tp"),
        P("tp", None),
    )
    out_specs = (P(EP_TP, None), P(EP_TP, None))
    return jax.shard_map(local, mesh=finer, in_specs=in_specs, out_specs=out_specs, check_vma=False)
```

profile of v0, /device:TPU:2, one launch (start us, length us, event | category | flops | bytes accessed | tf_op | source)
XLA Modules:
  0.0 262.9 jit_solution(2775184898795424189)
XLA Ops:
  7.2 0.7 all-gather.4.cloned.1.call-update
  8.0 0.7 all-gather.6.cloned.1.call-update
  8.7 0.7 all-gather.8.cloned.1.call-update
  9.9 2.4 reduce-window.6
  12.6 0.3 fusion.7
  12.9 0.3 fusion.9
  13.5 1.4 scatter_custom_fusion
  14.9 3.1 %gather_fusion = bf16[384,2048]{1,0:T(8,128)(2,1)} fusion(bf16[257,2048]{1,0:T(8,128)(2,1)S(1)} %concatenate.27, s32[1024]{0:T(1024)S(1)} %pad_clamp_fusion.1), kind=kCustom, calls=%fused_computation | custom fusion | bytes 3147264 | tf_op jit(solution)/shard_map/gather | solution.py:159
  18.1 3.7 %reshape.273 = bf16[1,64,6,2048]{3,2,1,0:T(8,128)(2,1)} reshape(bf16[384,2048]{1,0:T(8,128)(2,1)} %gather_fusion) | data formatting | bytes 3145728 | tf_op jit(solution)/shard_map/reshape | solution.py:159
  21.7 12.3 %all-to-all-start = ((bf16[1,64,6,2048]{3,2,0,1:T(8,128)(2,1)}), bf16[1,64,6,2048]{3,2,0,1:T(8,128)(2,1)}, u32[]{:S(2)}, u32[]{:S(2)}) async-start(bf16[1,64,6,2048]{3,2,0,1:T(8,128)(2,1)} %bitcast.171), calls=%async_computation.1 | async-start | bytes 4194304 | tf_op jit(solution)/shard_map/all_to_all | solution.py:162
  34.1 1.5 fusion.107
  35.6 1.8 convolution_convert_fusion.1
  37.5 2.2 fusion
  39.9 1.9 negate_log-plus-one_fusion
  41.8 2.6 reshape_reshape.14
  44.4 1.3 fusion.32
  46.1 0.6 add_multiply_fusion.1
  46.7 0.6 copy.132
  47.4 2.0 all_gather.33
  49.3 0.5 fusion.73
  49.9 0.6 convert_bitcast_fusion.4
  50.4 1.4 reshape_reshape.15
  51.8 2.6 %divide_multiply_fusion = f32[512,256]{1,0:T(8,128)S(1)} fusion(bf16[2048,256]{1,0:T(8,128)(2,1)} %param.22, bf16[512,2048]{1,0:T(8,128)(2,1)} %param.19, f32[2048]{0:T(1024)S(1)} %copy-done.30, f32[512]{0:T(512)S(1)} %add_rsqrt_fusion), kind=kOutput, calls=%fused_computation.66 | convolution fusion | flops 541589504 | bytes 3680256 | tf_op jit(solution)/shard_map/dot_general | solution.py:110
  54.5 1.5 reshape_reshape.13
  56.0 2.7 %fusion.99 = bf16[512,256]{1,0:T(8,128)(2,1)S(1)} fusion(bf16[2048,256]{1,0:T(8,128)(2,1)} %param.24, bf16[512,2048]{1,0:T(8,128)(2,1)} %param.19, f32[2048]{0:T(1024)S(1)} %copy-done.30, f32[512]{0:T(512)S(1)} %add_rsqrt_fusion), kind=kOutput, calls=%fused_computation.183 | convolution fusion | flops 541065216 | bytes 3418112 | tf_op jit(solution)/shard_map/dot_general | solution.py:112
  58.7 0.2 reshape_reshape.12
  58.9 4.2 %exponential_multiply_fusion = (bf16[8,64,4,64]{3,0,1,2:T(8,128)(2,1)}, bf16[8,64,4,64]{3,0,1,2:T(8,128)(2,1)}, bf16[8,64,4,64]{3,0,1,2:T(8,128)(2,1)}, bf16[8,64,4,64]{3,0,1,2:T(8,128)(2,1)S(1)}) fusion(f32[8,64,4,64]{3,0,1,2:T(8,128)S(1)} %fusion.32, f32[8,64,4,64]{3,2,1,0:T(4,128)} %reshape_reshape.13, f32[8,4,64]{2,0,1:T(8,128)S(1)} %get-tuple-element.11, ...), kind=kLoop, calls=%fused_computation.45 | loop fusion | flops 1441792 | bytes 2637824 | tf_op jit(solution)/shard_map/mul | solution.py:75
  63.1 0.3 fusion.26
  64.0 0.7 pad_maximum_fusion.1
  64.8 3.1 %pad.49 = f32[4,4,64,64]{3,2,1,0:T(8,128)S(1)} pad(f32[2,4,64,64]{3,2,1,0:T(8,128)} %pad_maximum_fusion.1, f32[]{:T(128)} %constant.32.clone.1), padding=0_1_1x0_0_0x0_0_0x0_0_0 | pad | bytes 393220 | tf_op jit(solution)/shard_map/pad | solution.py:125
  67.9 3.2 %pad.50 = f32[4,4,64,64]{3,2,1,0:T(8,128)} pad(f32[2,4,64,64]{3,2,1,0:T(8,128)S(1)} %pad_add_fusion, f32[]{:T(128)} %constant.32.clone.1), padding=1_0_1x0_0_0x0_0_0x0_0_0 | pad | bytes 393220 | tf_op jit(solution)/shard_map/pad | solution.py:125
  71.1 1.9 add.256
  73.0 9.2 %pad.101 = f32[8,4,64,64]{3,2,1,0:T(8,128)} pad(f32[4,4,64,64]{3,2,1,0:T(8,128)} %add.256, f32[]{:T(128)} %constant.32.clone.1), padding=1_0_1x0_0_0x0_0_0x0_0_0 | pad | bytes 786436
  82.3 1.2 fusion.47
  83.5 0.2 pad.51
  83.7 0.9 add_convert_fusion.1
  84.7 1.9 all_gather.36
  86.6 7.8 %all_gather.34 = bf16[4,4,64]{2,1,0:T(4,128)(2,1)S(1)} all-gather(bf16[1,4,64]{2,1,0:T(4,128)(2,1)S(1)} %copy-done.27), channel_id=1, replica_groups=mesh['ep_0'=8,'ep_1'=4,'ep_2'=2,'tp'=4] {'ep_1'}, dimensions={0}, use_global_device_ids=true | all-gather | bytes 2560 | tf_op jit(solution)/shard_map/all_gather | solution.py:31
  94.4 0.6 fusion.77
  95.1 0.4 copy-done.17
  95.7 17.1 %all_gather.35 = bf16[8,4,64]{2,1,0:T(4,128)(2,1)} all-gather(bf16[1,4,64]{2,1,0:T(4,128)(2,1)S(1)} %fusion.78), channel_id=1, replica_groups=mesh['ep_0'=8,'ep_1'=4,'ep_2'=2,'tp'=4] {'ep_0'}, dimensions={0}, use_global_device_ids=true | all-gather | bytes 4608 | tf_op jit(solution)/shard_map/all_gather | solution.py:31
  112.7 11.6 %all_gather.37 = bf16[4,4,64,64]{3,2,1,0:T(8,128)(2,1)S(1)} all-gather(bf16[1,4,64,64]{3,2,1,0:T(8,128)(2,1)S(1)} %fusion.60), channel_id=1, replica_groups=mesh['ep_0'=8,'ep_1'=4,'ep_2'=2,'tp'=4] {'ep_1'}, dimensions={0}, use_global_device_ids=true | all-gather | bytes 163840 | tf_op jit(solution)/shard_map/all_gather | solution.py:31
  124.4 0.6 iota_compare_fusion.2
  125.0 0.2 fusion.59
  125.2 27.5 %all_gather.38 = bf16[8,4,64,64]{3,2,1,0:T(8,128)(2,1)} all-gather(bf16[1,4,64,64]{3,2,1,0:T(8,128)(2,1)S(1)} %fusion.59), channel_id=1, replica_groups=mesh['ep_0'=8,'ep_1'=4,'ep_2'=2,'tp'=4] {'ep_0'}, dimensions={0}, use_global_device_ids=true | all-gather | bytes 294912 | tf_op jit(solution)/shard_map/all_gather | solution.py:31
  153.0 2.3 add_bitcast_fusion.1
  155.3 1.9 fusion.17
  157.2 1.4 slice_add_fusion.4
  158.6 1.2 multiply_reduce_fusion.1
  159.9 0.6 copy.138
  160.5 0.3 reshape.270
  161.0 2.1 convolution_convert_fusion
  163.1 5.1 %fusion.5 = f32[64,6,1024]{2,0,1:T(8,128)S(1)} fusion(bf16[1,2048,1024]{2,1,0:T(8,128)(2,1)} %all-gather.4.cloned.1.call-done, bf16[1,64,6,2048]{3,2,0,1:T(8,128)(2,1)} %all-to-all-done), kind=kOutput, calls=%fused_computation.11 | convolution fusion | flops 1610612736 | bytes 7340032 | tf_op jit(solution)/shard_map/qecd,df->qecf/dot_general | solution.py:163
  168.3 5.1 %multiply_convert_fusion = bf16[64,6,1024]{2,0,1:T(8,128)(2,1)S(1)} fusion(f32[64,6,1024]{2,0,1:T(8,128)S(1)} %fusion.5, bf16[1,2048,1024]{2,1,0:T(8,128)(2,1)} %all-gather.6.cloned.1.call-done, bf16[1,64,6,2048]{3,2,0,1:T(8,128)(2,1)} %all-to-all-done), kind=kOutput, calls=%fused_computation.23 | convolution fusion | flops 1612972032 | bytes 8126464 | tf_op jit(solution)/shard_map/qecd,df->qecf/dot_general | solution.py:166
  173.4 3.6 %all-gather.8.cloned.1.call-done = bf16[1,1024,2048]{2,1,0:T(8,128)(2,1)} async-done(((bf16[1,256,2048]{2,1,0:T(8,128)(2,1)}), bf16[1,1024,2048]{2,1,0:T(8,128)(2,1)}) %all-gather.8.cloned.1.call-update) | async-done | bytes 4194320 | tf_op jit(solution)/shard_map/all_gather | solution.py:107
  177.1 4.1 %convert_reduce_fusion = bf16[64,6,2048]{2,0,1:T(8,128)(2,1)S(1)} fusion(bf16[4,256,2048,1]{2,1,3,0:T(8,128)(2,1)} %bitcast.177, bf16[6,8,4,8,256]{4,3,2,1,0:T(8,128)(2,1)S(1)} %bitcast.178), kind=kOutput, calls=%fused_computation.3 | convolution fusion | flops 1616117760 | bytes 6553600 | tf_op jit(solution)/shard_map/qecgf,gfd->qecgd/dot_general | solution.py:169
  181.2 2.2 copy.149
  183.4 10.9 %all-to-all-start.1 = ((bf16[1,64,6,2048]{3,2,0,1:T(8,128)(2,1)}), bf16[1,64,6,2048]{3,2,0,1:T(8,128)(2,1)}, u32[]{:S(2)}, u32[]{:S(2)}) async-start(bf16[1,64,6,2048]{3,2,0,1:T(8,128)(2,1)} %copy.149), calls=%async_computation.2 | async-start | bytes 4194304 | tf_op jit(solution)/shard_map/all_to_all | solution.py:173
  194.5 51.0 %all-to-all-done.1 = bf16[1,64,6,2048]{3,2,0,1:T(8,128)(2,1)} async-done(((bf16[1,64,6,2048]{3,2,0,1:T(8,128)(2,1)}), bf16[1,64,6,2048]{3,2,0,1:T(8,128)(2,1)}, u32[]{:S(2)}, u32[]{:S(2)}) %all-to-all-start.1) | async-done | bytes 1572896 | tf_op jit(solution)/shard_map/all_to_all | solution.py:173
  245.4 2.6 reshape.276
  248.0 2.4 gather_fusion.1
  250.4 1.7 reshape.290
  252.1 2.3 multiply_reduce_fusion
  254.5 1.9 add_convert_fusion
  (143 shorter events, 3.3 us)
Async XLA Ops:
  7.2 153.8 %copy-start = (bf16[256,2048]{1,0:T(8,128)(2,1)S(1)}, bf16[256,2048]{1,0:T(8,128)(2,1)}, u32[]{:S(2)}) copy-start(bf16[256,2048]{1,0:T(8,128)(2,1)} %param.27) | copy-start | bytes 3145732
  7.2 2.3 copy-start.24
  7.2 155.9 %all-gather.4.cloned.1.call-start = ((), (), s32[]{:S(2)}) async-start(), calls=%async_computation.5 | async-start | bytes 5242880 | tf_op jit(solution)/shard_map/all_gather | solution.py:105
  7.9 4.6 %copy-start.1 = (bf16[256,2048]{1,0:T(8,128)(2,1)S(1)}, bf16[256,2048]{1,0:T(8,128)(2,1)}, u32[]{:S(2)}) copy-start(bf16[256,2048]{1,0:T(8,128)(2,1)} %param.28) | copy-start | bytes 3145732
  7.9 160.4 %all-gather.6.cloned.1.call-start = ((), (), s32[]{:S(2)}) async-start(), calls=%async_computation.6 | async-start | bytes 5242880 | tf_op jit(solution)/shard_map/all_gather | solution.py:106
  8.7 4.2 %copy-start.20 = (f32[2048]{0:T(1024)S(1)}, f32[2048]{0:T(1024)}, u32[]{:S(2)}) copy-start(f32[2048]{0:T(1024)} %param.29) | copy-start | bytes 24580
  8.7 168.4 %all-gather.8.cloned.1.call-start = ((), (), s32[]{:S(2)}) async-start(), calls=%async_computation.7 | async-start | bytes 5242880 | tf_op jit(solution)/shard_map/all_gather | solution.py:107
  13.5 4.6 %copy-start.25 = (s32[256,1]{0,1:T(1,128)}, s32[256,1]{0,1:T(1,128)S(1)}, u32[]{:S(2)}) copy-start(s32[256,1]{0,1:T(1,128)S(1)} %compare_select_fusion) | copy-start | bytes 3076
  21.7 13.9 %copy-start.4 = (bf16[128,2048]{1,0:T(8,128)(2,1)S(1)}, bf16[128,2048]{1,0:T(8,128)(2,1)}, u32[]{:S(2)}) copy-start(bf16[128,2048]{1,0:T(8,128)(2,1)} %param.37) | copy-start | bytes 1572868
  21.7 13.9 %copy-start.5 = (bf16[2048,128]{1,0:T(8,128)(2,1)S(1)}, bf16[2048,128]{1,0:T(8,128)(2,1)}, u32[]{:S(2)}) copy-start(bf16[2048,128]{1,0:T(8,128)(2,1)} %param.36) | copy-start | bytes 1572868
  21.7 141.3 %all-to-all-start = ((bf16[1,64,6,2048]{3,2,0,1:T(8,128)(2,1)}), bf16[1,64,6,2048]{3,2,0,1:T(8,128)(2,1)}, u32[]{:S(2)}, u32[]{:S(2)}) async-start(bf16[1,64,6,2048]{3,2,0,1:T(8,128)(2,1)} %bitcast.171), calls=%async_computation.1 | async-start | bytes 4194304 | tf_op jit(solution)/shard_map/all_to_all | solution.py:162
  34.1 220.4 %reduce-scatter.5.cloned.1.call-start = ((), (), s32[]{:S(2)}) async-start(), calls=%async_computation.8 | async-start | bytes 1310720 | tf_op jit(solution)/shard_map/reduce_scatter | solution.py:189
  35.6 4.1 %copy-start.31 = (f32[512]{0:T(512)S(1)}, f32[512]{0:T(512)}, u32[]{:S(2)}) copy-start(f32[512]{0:T(512)} %param.20) | copy-start | bytes 6148
  37.4 2.3 copy-start.3
  37.4 2.3 copy-start.30
  37.4 2.4 copy-start.32
  37.5 218.9 %reduce-scatter.3.cloned.1.call-start = ((), (), s32[]{:S(2)}) async-start(), calls=%async_computation.4 | async-start | bytes 2621440 | tf_op jit(solution)/shard_map/reduce_scatter | solution.py:186
  37.5 2.4 copy-start.29
  41.8 8.6 %copy-start.6 = (f32[512,256]{1,0:T(8,128)S(1)}, f32[512,256]{1,0:T(8,128)}, u32[]{:S(2)}) copy-start(f32[512,256]{1,0:T(8,128)} %get-tuple-element.35) | copy-start | bytes 1572868
  45.8 8.7 %copy-start.8 = (f32[8,4,64]{2,0,1:T(8,128)}, f32[8,4,64]{2,0,1:T(8,128)S(1)}, u32[]{:S(2)}) copy-start(f32[8,4,64]{2,0,1:T(8,128)S(1)} %fusion.95) | copy-start | bytes 24580
  46.1 8.4 %copy-start.9 = (f32[4,4,64]{2,0,1:T(4,128)}, f32[4,4,64]{2,0,1:T(4,128)S(1)}, u32[]{:S(2)}) copy-start(f32[4,4,64]{2,0,1:T(4,128)S(1)} %add.249) | copy-start | bytes 12292
  49.3 5.2 %copy-start.13 = (bf16[2,4,64]{2,1,0:T(4,128)(2,1)}, bf16[2,4,64]{2,1,0:T(4,128)(2,1)S(1)}, u32[]{:S(2)}) copy-start(bf16[2,4,64]{2,1,0:T(4,128)(2,1)S(1)} %all_gather.33) | copy-start | bytes 3076
  67.9 14.3 %copy-start.15 = (f32[3,4,64]{2,1,0:T(4,128)S(1)}, f32[3,4,64]{2,1,0:T(4,128)}, u32[]{:S(2)}) copy-start(f32[3,4,64]{2,1,0:T(4,128)} %copy.132) | copy-start | bytes 9220
  82.2 4.4 %copy-start.27 = (bf16[1,4,64]{2,1,0:T(4,128)(2,1)S(1)}, bf16[1,4,64]{2,1,0:T(4,128)(2,1)}, u32[]{:S(2)}) copy-start(bf16[1,4,64]{2,1,0:T(4,128)(2,1)} %fusion.73) | copy-start | bytes 1540
  82.2 12.2 %copy-start.14 = (bf16[2,4,64]{2,1,0:T(4,128)(2,1)S(1)}, bf16[2,4,64]{2,1,0:T(4,128)(2,1)}, u32[]{:S(2)}) copy-start(bf16[2,4,64]{2,1,0:T(4,128)(2,1)} %copy-done.13) | copy-start | bytes 3076
  82.2 12.8 %copy-start.19 = (f32[4,64]{1,0:T(4,128)S(1)}, f32[4,64]{1,0:T(4,128)}, u32[]{:S(2)}) copy-start(f32[4,64]{1,0:T(4,128)} %convert_bitcast_fusion.4) | copy-start | bytes 3076
  82.2 13.4 %slice-start = ((f32[8,4,64]{2,0,1:T(8,128)}), f32[1,4,64]{2,0,1:T(1,128)S(1)}, s32[]{:S(2)}) async-start(f32[8,4,64]{2,0,1:T(8,128)} %copy-done.8), calls=%async_computation.9 | async-start | bytes 4096 | tf_op jit(solution)/shard_map/slice | solution.py:125
  82.2 13.3 %copy-start.11 = (f32[3,4,64]{2,0,1:T(4,128)S(1)}, f32[3,4,64]{2,0,1:T(4,128)}, u32[]{:S(2)}) copy-start(f32[3,4,64]{2,0,1:T(4,128)} %add_multiply_fusion.1) | copy-start | bytes 9220
  82.2 13.4 %copy-start.10 = (f32[4,4,64]{2,0,1:T(4,128)S(1)}, f32[4,4,64]{2,0,1:T(4,128)}, u32[]{:S(2)}) copy-start(f32[4,4,64]{2,0,1:T(4,128)} %copy-done.9) | copy-start | bytes 12292
  95.0 0.6 copy-start.17
  95.0 30.2 %copy-start.16 = (f32[4,64]{1,0:T(4,128)}, f32[4,64]{1,0:T(4,128)S(1)}, u32[]{:S(2)}) copy-start(f32[4,64]{1,0:T(4,128)S(1)} %get-tuple-element.26) | copy-start | bytes 3076
  124.4 28.6 %copy-start.12 = (bf16[8,4,64]{2,1,0:T(4,128)(2,1)S(1)}, bf16[8,4,64]{2,1,0:T(4,128)(2,1)}, u32[]{:S(2)}) copy-start(bf16[8,4,64]{2,1,0:T(4,128)(2,1)} %all_gather.35) | copy-start | bytes 12292
  124.4 28.6 %copy-start.18 = (f32[4,64]{1,0:T(4,128)S(1)}, f32[4,64]{1,0:T(4,128)}, u32[]{:S(2)}) copy-start(f32[4,64]{1,0:T(4,128)} %copy-done.17) | copy-start | bytes 3076
  124.4 28.6 %copy-start.21 = (f32[4,64]{1,0:T(4,128)S(1)}, f32[4,64]{1,0:T(4,128)}, u32[]{:S(2)}) copy-start(f32[4,64]{1,0:T(4,128)} %get-tuple-element.2) | copy-start | bytes 3076
  124.4 28.6 %copy-start.22 = (f32[4,64]{1,0:T(4,128)S(1)}, f32[4,64]{1,0:T(4,128)}, u32[]{:S(2)}) copy-start(f32[4,64]{1,0:T(4,128)} %get-tuple-element.3) | copy-start | bytes 3076
  157.2 1.4 copy-start.2
  157.2 1.4 copy-start.7
  159.9 1.0 copy-start.28
  183.4 10.9 %copy-start.23 = (f32[64,4]{0,1:T(4,128)S(1)}, f32[64,4]{0,1:T(4,128)}, u32[]{:S(2)}) copy-start(f32[64,4]{0,1:T(4,128)} %param.31) | copy-start | bytes 3076
  183.4 11.0 %copy-start.26 = (s32[256,1]{0,1:T(1,128)S(1)}, s32[256,1]{0,1:T(1,128)}, u32[]{:S(2)}) copy-start(s32[256,1]{0,1:T(1,128)} %copy-done.25) | copy-start | bytes 3076
  183.4 62.0 %all-to-all-start.1 = ((bf16[1,64,6,2048]{3,2,0,1:T(8,128)(2,1)}), bf16[1,64,6,2048]{3,2,0,1:T(8,128)(2,1)}, u32[]{:S(2)}, u32[]{:S(2)}) async-start(bf16[1,64,6,2048]{3,2,0,1:T(8,128)(2,1)} %copy.149), calls=%async_computation.2 | async-start | bytes 4194304 | tf_op jit(solution)/shard_map/all_to_all | solution.py:173
Sparse Core Ops, SparseCore 0:
  9.8 56.9 all-gather.3
  68.6 54.8 all-gather.5
  125.3 51.7 all-gather.7
  179.5 26.6 reduce-scatter.4
  209.1 32.0 reduce-scatter.2
where the time goes:
time: 265 us; the launch traced here: 263 us
  blocking collectives  67.9 us (26%)
  waiting for transfers between devices  56.7 us (21%)
  local copies, waits for them, and re-layouts  42.2 us (16%)
  matrix products  30.4 us (11%)
  other arithmetic  27.6 us (10%)
  starting transfers between devices  23.4 us (9%)
  between operations  14.6 us (6%)
    all_gather x6, blocking collectives, prefix_by_axis(): lax.all_gather(part.astype(kind), axis)  67.9 us
    all_to_all x1, waiting for transfers between devices, local(): lax.all_to_all(summed.astype(jnp.bfloat16), EP, split_axis=1, concat_axis...  51 us
    all_to_all x1, starting transfers between devices, local(): lax.all_to_all(outgoing, EP, split_axis=1, concat_axis=1, tiled=True)  12.3 us
    all_to_all x1, starting transfers between devices, local(): lax.all_to_all(summed.astype(jnp.bfloat16), EP, split_axis=1, concat_axis...  10.9 us
    unnamed x70, local copies, waits for them, and re-layouts  10.1 us
    pad x7, local copies, waits for them, and re-layouts, local(): lax.associative_scan(join_states, (decay_total, state_added), axis=0)  6.75 us
  transfers between devices with their start and end apart: 7, of which 2 were waited for; matrix products, arithmetic and copies ran while one was open for 38% of the time, Pallas kernels for 0%

commit v1 on v0

v1 whole, which is shorter than its diff:
```python
import jax
import jax.numpy as jnp
from jax import lax
from jax.experimental import pallas as pl
from jax.experimental.pallas import tpu as pltpu
from jax.sharding import Mesh
from jax.sharding import PartitionSpec as P

HEAD = 64
SPAN = 64
TOP_K = 4
EP = ("ep_0", "ep_1", "ep_2")
EP_TP = ("ep_0", "ep_1", "ep_2", "tp")
UP = [(i, (i + 1) % 4) for i in range(4)]
DOWN = [(i, (i - 1) % 4) for i in range(4)]

epsilon = 1e-06
route_scale = 2.5
f32 = jnp.float32
bf16 = jnp.bfloat16


def dot(a, b, ca=1, cb=0, **kw):
    return lax.dot_general(a, b, (((ca,), (cb,)), ((), ())), preferred_element_type=f32, **kw)


def norm_rows(row_data, gain_vec):
    widened = row_data.astype(f32)
    scaled = widened * lax.rsqrt(jnp.mean(widened * widened, axis=-1, keepdims=True) + epsilon)
    return (scaled * gain_vec).astype(bf16)


def same_head(rows, cols):
    row_head = lax.broadcasted_iota(jnp.int32, (rows, cols), 0) // HEAD
    col_head = lax.broadcasted_iota(jnp.int32, (rows, cols), 1) // HEAD
    return row_head == col_head


def mixer_local_body(
    shift_ref, x_hbm, gain_ref, wq_hbm, wf_hbm, wv_hbm, room_ref,
    part_ref, reach_ref, state_ref, total_ref,
    x_ref, wq_ref, wf_ref, wv_ref, normed_ref, q_ref, f_ref, v_ref, sems,
):
    pairs = ((x_hbm, x_ref), (wf_hbm, wf_ref), (wq_hbm, wq_ref), (wv_hbm, wv_ref))
    copies = [pltpu.make_async_copy(a, b, sems.at[i]) for i, (a, b) in enumerate(pairs)]
    for copy in copies:
        copy.start()
    rows, width = q_ref.shape
    blocks = rows // SPAN
    heads = width // HEAD
    gain = gain_ref[...]

    def norm_block(n, carry):
        at = pl.ds(n * SPAN, SPAN)
        normed_ref[at, :] = norm_rows(x_ref[at, :], gain)
        return carry

    copies[0].wait()
    lax.fori_loop(0, blocks, norm_block, 0)
    normed = normed_ref[...]
    copies[1].wait()
    f_ref[...] = dot(normed, wf_ref[...])
    copies[2].wait()
    q_ref[...] = dot(normed, wq_ref[...])
    copies[3].wait()
    v_ref[...] = dot(normed, wv_ref[...])
    room = room_ref[...]
    diagonal = same_head(width, width).astype(f32)
    row_at = lax.broadcasted_iota(jnp.int32, (width, SPAN), 0) % SPAN
    causal = row_at >= lax.broadcasted_iota(jnp.int32, (width, SPAN), 1)
    lower = (
        lax.broadcasted_iota(jnp.int32, (SPAN, SPAN), 0)
        >= lax.broadcasted_iota(jnp.int32, (SPAN, SPAN), 1)
    ).astype(f32)
    state = jnp.zeros((width, width), f32)
    log_before = jnp.zeros((1, width), f32)
    for n in range(blocks):
        at = pl.ds(n * SPAN, SPAN)
        queries = jax.nn.silu(q_ref[at, :])
        rate = room * jax.nn.sigmoid(-(f_ref[at, :] + shift_ref[n]))
        values = v_ref[at, :].astype(bf16)
        log_decay = dot(lower, jnp.log1p(-rate), precision=lax.Precision.HIGHEST)
        middle = log_decay[SPAN // 2 : SPAN // 2 + 1]
        block_end = log_decay[SPAN - 1 :]
        from_middle = queries * jnp.exp(log_decay - middle)
        to_middle = (rate * jnp.exp(middle - log_decay)).astype(bf16)
        by_head = (jnp.concatenate([from_middle] * heads, axis=0) * diagonal).astype(bf16)
        scores = jnp.where(causal, dot(by_head, to_middle, 1, 1), 0.0).astype(bf16)
        all_pairs = dot(scores, values) * diagonal
        mixed = all_pairs[:SPAN]
        for h in range(1, heads):
            mixed = mixed + all_pairs[h * SPAN : (h + 1) * SPAN]
        decayed = queries * jnp.exp(log_decay)
        part_ref[at, :] = mixed + dot(decayed.astype(bf16), state.astype(bf16), 1, 1)
        reach_ref[at, :] = (decayed * jnp.exp(log_before)).astype(bf16)
        to_end = (rate * jnp.exp(block_end - log_decay)).astype(bf16)
        state = state * jnp.exp(block_end) + dot(values, to_end, 0, 0) * diagonal
        log_before = log_before + block_end
    packed = state[:HEAD]
    for h in range(1, heads):
        packed = packed + state[h * HEAD : (h + 1) * HEAD]
    state_ref[...] = packed
    total_ref[...] = jnp.exp(log_before)


def mixer_local(mix_in, shifts, gain, w_query, w_forget, w_value, room):
    rows = mix_in.shape[0]
    width = w_query.shape[1]
    vmem = pl.BlockSpec(memory_space=pltpu.VMEM)
    hbm = pl.BlockSpec(memory_space=pltpu.HBM)
    return pl.pallas_call(
        mixer_local_body,
        in_specs=[pl.BlockSpec(memory_space=pltpu.SMEM), hbm, vmem, hbm, hbm, hbm, vmem],
        out_specs=[vmem] * 4,
        out_shape=[
            jax.ShapeDtypeStruct((rows, width), f32),
            jax.ShapeDtypeStruct((rows, width), bf16),
            jax.ShapeDtypeStruct((HEAD, width), f32),
            jax.ShapeDtypeStruct((1, width), f32),
        ],
        scratch_shapes=[pltpu.VMEM(mix_in.shape, bf16)]
        + [pltpu.VMEM(w_query.shape, bf16)] * 3
        + [pltpu.VMEM(mix_in.shape, bf16)]
        + [pltpu.VMEM((rows, width), f32)] * 3
        + [pltpu.SemaphoreType.DMA((4,))],
        compiler_params=pltpu.CompilerParams(vmem_limit_bytes=60 << 20),
        cost_estimate=pl.CostEstimate(
            flops=rows * mix_in.shape[1] * width * 6, bytes_accessed=6 << 20, transcendentals=0
        ),
        name="mixer_local",
    )(shifts, mix_in, gain, w_query, w_forget, w_value, room)


def state_scan_body(got_ref, out_ref):
    def step(i, state):
        tile = got_ref[i].astype(f32)
        out_ref[i] = state.astype(bf16)
        added = tile[0:2] + tile[2:4]
        decay = tile[4:6] + tile[6:8]
        return decay * state + added

    lax.fori_loop(0, got_ref.shape[0], step, jnp.zeros((2, 128), f32), unroll=8)


def state_scan(got):
    return pl.pallas_call(
        state_scan_body,
        out_shape=jax.ShapeDtypeStruct((got.shape[0], 2, 128), bf16),
        name="state_scan",
    )(got)


def split_bf16(x):
    high = x.astype(bf16)
    return high, (x - high.astype(f32)).astype(bf16)


def mixer_out_body(rank_ref, part_ref, reach_ref, state_ref, gain_ref, w_ref, out_ref):
    width = part_ref.shape[1]
    heads = width // HEAD
    diagonal = same_head(width, width).astype(f32)
    state = jnp.concatenate([state_ref[...].astype(f32)] * heads, axis=0) * diagonal
    mixed = part_ref[...] + dot(reach_ref[...], state.astype(bf16), 1, 1)
    square = dot(mixed * mixed, diagonal * (1.0 / HEAD), precision=lax.Precision.HIGHEST)
    head_out = (mixed * lax.rsqrt(square + epsilon) * gain_ref[...]).astype(bf16)
    out_ref[0] = dot(head_out, w_ref[...]).astype(bf16)


def mixer_out(rank, part, reach, state, gain, w_out, tp_count):
    rows, width = part.shape
    quarter = rows // tp_count
    model = w_out.shape[1]
    mine = lambda i, rank: ((rank[0] + i) % tp_count, 0)
    whole = lambda i, rank: (0, 0)
    return pl.pallas_call(
        mixer_out_body,
        grid_spec=pltpu.PrefetchScalarGridSpec(
            num_scalar_prefetch=1,
            grid=(tp_count,),
            in_specs=[
                pl.BlockSpec((quarter, width), mine),
                pl.BlockSpec((quarter, width), mine),
                pl.BlockSpec((HEAD, width), whole),
                pl.BlockSpec((1, width), whole),
                pl.BlockSpec((width, model), whole),
            ],
            out_specs=pl.BlockSpec((1, quarter, model), lambda i, rank: (i, 0, 0)),
        ),
        out_shape=jax.ShapeDtypeStruct((tp_count, quarter, model), bf16),
        cost_estimate=pl.CostEstimate(
            flops=rows * width * model * 2, bytes_accessed=4 << 20, transcendentals=0
        ),
        name="mixer_out",
    )(rank, part, reach, state, gain, w_out)


def hidden_units_body(x_ref, gate_ref, up_ref, out_ref, gate_sum, up_sum):
    step = pl.program_id(0)

    @pl.when(step == 0)
    def _():
        gate_sum[...] = jnp.zeros(gate_sum.shape, f32)
        up_sum[...] = jnp.zeros(up_sum.shape, f32)

    x = x_ref[...]
    gate_sum[...] += dot(x, gate_ref[...])
    up_sum[...] += dot(x, up_ref[...])

    @pl.when(step == pl.num_programs(0) - 1)
    def _():
        out_ref[...] = (jax.nn.silu(gate_sum[...]) * up_sum[...]).astype(bf16)


def hidden_units(x, gate, up):
    rows, model = x.shape
    width = gate.shape[1]
    part = model // 4
    return pl.pallas_call(
        hidden_units_body,
        grid=(model // part,),
        in_specs=[
            pl.BlockSpec((rows, part), lambda i: (0, i)),
            pl.BlockSpec((part, width), lambda i: (i, 0)),
            pl.BlockSpec((part, width), lambda i: (i, 0)),
        ],
        out_specs=pl.BlockSpec((rows, width), lambda i: (0, 0)),
        out_shape=jax.ShapeDtypeStruct((rows, width), bf16),
        scratch_shapes=[pltpu.VMEM((rows, width), f32)] * 2,
        cost_estimate=pl.CostEstimate(
            flops=rows * model * width * 4, bytes_accessed=4 << 20, transcendentals=0
        ),
        name="hidden_units",
    )(x, gate, up)


def shift_up(x):
    return lax.ppermute(x, "tp", UP)


def shift_down(x):
    return lax.ppermute(x, "tp", DOWN)


def after(x, *others):
    return lax.optimization_barrier((x, *others))[0]


def local(
    mix_in,
    forget_shift,
    mix_gain,
    w_query,
    w_forget,
    w_value,
    forget_room,
    head_gain,
    w_out,
    moe_in,
    moe_gain,
    expert_choice,
    route_logit,
    w_exp_gate,
    w_exp_up,
    w_exp_down,
    w_sh_gate,
    w_sh_up,
    w_sh_down,
):
    tp_count = 4
    tp_rank = lax.axis_index("tp")
    row_count, model = moe_in.shape
    quarter = row_count // tp_count
    experts = lax.axis_size(EP) * w_exp_gate.shape[0]
    mean_load = quarter * TOP_K // experts
    capacity = mean_load + mean_load // 2
    slots = experts * capacity
    pieces = capacity * model // 128

    gate_own, up_own, down_own = w_exp_gate[0], w_exp_up[0], w_exp_down[0]
    gate_below = shift_up(gate_own)
    up_above = shift_down(up_own)
    up_below = shift_up(up_own)
    gate_above = shift_down(gate_own)
    gate_far = shift_up(gate_below)
    up_far = shift_down(up_above)
    half_units = down_own.shape[0] // 2
    top, low = down_own[:half_units], down_own[half_units:]
    top_below = shift_up(top)
    low_above = shift_down(low)
    low_below = shift_up(low)
    top_above = shift_down(top)

    shifts = forget_shift.reshape(-1, SPAN)[:, 0]
    part, reach, added, total = mixer_local(
        mix_in, shifts, mix_gain[None], w_query, w_forget, w_value, forget_room[None]
    )
    added_high, added_low = split_bf16(added)
    total_high, total_low = split_bf16(total)
    whole_row = lambda x: jnp.broadcast_to(x.reshape(1, 2, 128), (HEAD, 2, 128))
    state_send = [
        added_high.reshape(HEAD, 2, 128),
        added_low.reshape(HEAD, 2, 128),
        whole_row(total_high),
        whole_row(total_low),
    ]

    moe_in, expert_choice = lax.optimization_barrier((moe_in, expert_choice, total))[:2]
    own_rows = lax.dynamic_slice_in_dim(moe_in, tp_rank * quarter, quarter, 0)
    own_hidden = norm_rows(own_rows, moe_gain)
    labels = lax.dynamic_slice_in_dim(expert_choice, tp_rank * quarter, quarter, 0).reshape(-1)
    onehot = labels[:, None] == jnp.arange(experts, dtype=jnp.int32)[None, :]
    earlier = jnp.arange(labels.shape[0])[:, None] > jnp.arange(labels.shape[0])[None, :]
    counts = dot(earlier.astype(bf16), onehot.astype(bf16))
    places = jnp.sum(jnp.where(onehot, counts, 0.0), axis=-1).astype(jnp.int32)
    slot_ids = (labels * capacity + places).reshape(quarter, TOP_K)
    slot_axis = jnp.arange(slots, dtype=jnp.int32)
    holds = sum((slot_ids[:, k][None, :] == slot_axis[:, None]).astype(bf16) for k in range(TOP_K))
    outgoing = dot(holds, own_hidden).astype(bf16)
    arrived = lax.all_to_all(
        jnp.concatenate([outgoing.reshape(experts, pieces, 128)] + state_send, axis=1),
        EP, split_axis=0, concat_axis=0, tiled=True,
    )
    state_next = state_scan(arrived[:, pieces:])
    top_far = shift_up(after(top_below, state_next))
    low_far = shift_down(after(low_above, state_next))
    state_start = lax.all_to_all(
        state_next, EP, split_axis=0, concat_axis=0, tiled=True
    ).reshape(HEAD, -1)
    mixer_parts = mixer_out(
        tp_rank.reshape(1), part, reach, state_start, head_gain[None], w_out, tp_count
    )

    hidden = norm_rows(moe_in, moe_gain)
    shared_gate = dot(hidden, w_sh_gate)
    shared_up = dot(hidden, w_sh_up)
    shared_act = (jax.nn.silu(shared_gate) * shared_up).astype(bf16)
    shared_part = dot(shared_act, w_sh_down).astype(bf16)
    chunk = lambda i: jnp.concatenate(
        [
            mixer_parts[i],
            lax.dynamic_slice_in_dim(shared_part, ((tp_rank + i) % tp_count) * quarter, quarter, 0),
        ],
        axis=0,
    )

    x = arrived[:, :pieces].reshape(slots, model)
    acts = [
        hidden_units(x, gate_own, up_own),
        hidden_units(x, gate_below, up_below),
        hidden_units(x, gate_above, up_above),
        hidden_units(x, gate_far, up_far),
    ]
    down = [(top, low), (top_below, low_below), (top_above, low_above), (top_far, low_far)]
    weights = jax.nn.sigmoid(route_logit)
    weights = weights / jnp.sum(weights, axis=-1, keepdims=True) * route_scale
    choose = sum(
        jnp.where(slot_ids[:, k][:, None] == slot_axis[None, :], weights[:, k][:, None], 0.0)
        for k in range(TOP_K)
    )
    choose_high, choose_low = split_bf16(choose)
    summed = sum(
        (dot(a[:, :half_units], top) + dot(a[:, half_units:], low)).astype(bf16).astype(f32)
        for a, (top, low) in zip(acts, down)
    )
    returned = lax.all_to_all(
        summed.astype(bf16).reshape(experts, pieces, 128),
        EP, split_axis=0, concat_axis=0, tiled=True,
    ).reshape(slots, model)
    routed = dot(choose_high, returned) + dot(choose_low, returned)

    across = chunk(2)
    middle = across.shape[0] // 2
    via_below = shift_up(across[:middle])
    via_above = shift_down(across[middle:])
    to_above = chunk(1)
    to_above = jnp.concatenate([to_above[:middle] + via_below, to_above[middle:]], axis=0)
    to_below = chunk(3)
    to_below = jnp.concatenate([to_below[:middle], to_below[middle:] + via_above], axis=0)
    from_below = shift_up(to_above)
    from_above = shift_down(to_below)
    total_rows = chunk(0).astype(f32) + from_below.astype(f32) + from_above.astype(f32)
    mixer_rows = mix_in.shape[0] // tp_count
    return (
        total_rows[:mixer_rows].astype(bf16),
        (routed + total_rows[mixer_rows:]).astype(bf16),
    )


def solution(mesh):
    finer = Mesh(mesh.devices.reshape(8, 4, 2, mesh.shape["tp"]), ("ep_0", "ep_1", "ep_2", "tp"))
    in_specs = (
        P(EP, None),
        P(EP),
        P(),
        P(None, "tp"),
        P(None, "tp"),
        P(None, "tp"),
        P("tp"),
        P("tp"),
        P("tp", None),
        P(EP, None),
        P(),
        P(EP, None),
        P(EP_TP, None),
        P(EP, None, "tp"),
        P(EP, None, "tp"),
        P(EP, "tp", None),
        P(None, "tp"),
        P(None, "tp"),
        P("tp", None),
    )
    out_specs = (P(EP_TP, None), P(EP_TP, None))

    return jax.shard_map(local, mesh=finer, in_specs=in_specs, out_specs=out_specs, check_vma=False)
```

time: 265 us -> 227 us (0.86)
  blocking collectives: 67.9 us -> 0 us
  Pallas kernels: 0 us -> 36.7 us
  starting transfers between devices: 23.4 us -> 51.2 us
  other arithmetic: 27.6 us -> 4.15 us
  waiting for transfers between devices: 56.7 us -> 73.7 us
  between operations: 14.6 us -> 1.04 us
  local copies, waits for them, and re-layouts: 42.2 us -> 33.7 us
  matrix products: 30.4 us -> 25.5 us
    all_gather x6 -> x0, blocking collectives: 67.9 us -> none  [prefix_by_axis(): lax.all_gather(part.astype(kind), axis)]
    ppermute x0 -> x16, waiting for transfers between devices: none -> 43 us  [the longest x8 28.3 us: shift_up(): return lax.ppermute(x, 'tp', UP)]
    pallas_call x0 -> x7, Pallas kernels: none -> 36.7 us  [the longest x4 17.3 us: hidden_units(): pl.pallas_call(hidden_units_body, grid=(model // part,), in_specs=[pl.Blo...]
    ppermute x0 -> x16, starting transfers between devices: none -> 23.1 us  [the longest x8 15.7 us: shift_down(): return lax.ppermute(x, 'tp', DOWN)]
    all_to_all x2 -> x3, waiting for transfers between devices: 51 us -> 30.6 us  [the longest x1 25.8 us: local(): lax.all_to_all(jnp.concatenate([outgoing.reshape(experts, pieces, 128)] +...]
    concatenate x2 -> x1, local copies, waits for them, and re-layouts: 0.12 us -> 8.32 us  [local(): jnp.concatenate([outgoing.reshape(experts, pieces, 128)] + state_send, ax...]
    mul x8 -> x1, other arithmetic: 7.71 us -> 0.01 us  [local(): weights = weights / jnp.sum(weights, axis=-1, keepdims=True) * route_scale]
    pad x7 -> x0, local copies, waits for them, and re-layouts: 6.75 us -> none  [local(): lax.associative_scan(join_states, (decay_total, state_added), axis=0)]
  transfers between devices with their start and end apart: 7 -> 19, of which waited for: 2 -> 7; matrix products, arithmetic and copies ran while one was open for 38% -> 18% of each run, Pallas kernels for 0% -> 11%
where the time goes in v1:
time: 227 us; the launch traced here: 226 us
  waiting for transfers between devices  73.7 us (32%)
  starting transfers between devices  51.2 us (23%)
  Pallas kernels  36.7 us (16%)
  local copies, waits for them, and re-layouts  33.7 us (15%)
  matrix products  25.5 us (11%)
  other arithmetic  4.15 us (2%)
    ppermute x8, waiting for transfers between devices, shift_up(): return lax.ppermute(x, 'tp', UP)  28.3 us
    all_to_all x1, waiting for transfers between devices, local(): lax.all_to_all(jnp.concatenate([outgoing.reshape(experts, pieces, 128)] +...  25.8 us
    dot_general x14, matrix products, dot(): lax.dot_general(a, b, (((ca,), (cb,)), ((), ())), preferred_element_type=...  25.5 us
    pallas_call x4, Pallas kernels, hidden_units(): pl.pallas_call(hidden_units_body, grid=(model // part,), in_specs=[pl.Blo...  17.3 us
    ppermute x8, starting transfers between devices, shift_down(): return lax.ppermute(x, 'tp', DOWN)  15.7 us
    ppermute x8, waiting for transfers between devices, shift_down(): return lax.ppermute(x, 'tp', DOWN)  14.7 us
    all_to_all x1, starting transfers between devices, local(): lax.all_to_all(jnp.concatenate([outgoing.reshape(experts, pieces, 128)] +...  12.1 us
    pallas_call x1, Pallas kernels, mixer_local(): pl.pallas_call(mixer_local_body, in_specs=[pl.BlockSpec(memory_space=pltp...  11.8 us
  transfers between devices with their start and end apart: 19, of which 7 were waited for; matrix products, arithmetic and copies ran while one was open for 18% of the time, Pallas kernels for 11%

profile of v1, /device:TPU:2, one launch (start us, length us, event | category | flops | bytes accessed | tf_op | source)
XLA Modules:
  0.0 225.9 jit_solution(7013203937638245756)
XLA Ops:
  0.7 0.8 reshape.68
  1.5 0.7 slice_reduce_fusion.4.shift_ref
  2.2 11.8 %mixer_local.1 = (f32[512,256]{1,0:T(8,128)}, bf16[512,256]{1,0:T(8,128)(2,1)}, f32[64,256]{1,0:T(8,128)}, f32[1,256]{1,0:T(1,128)}) custom-call(f32[8]{0:T(128)} %slice_reduce_fusion.4.shift_ref, bf16[512,2048]{1,0:T(8,128)(2,1)} %x_hbm.1, f32[1,2048]{1,0:T(1,128)} %bitcast.64, bf16[2048,256]{1,0:T(8,128)(2,1)} %wq_hbm.1, bf16[2048,256]{1,0:T(8,128)(2,1)} %wf_hbm.1, ...), custom_call_target="tpu_custom_call" | custom-call | flops 1610612736 | bytes 6291456 | tf_op jit(solution)/shard_map/mixer_local/pallas_call | solution.py:111
  14.0 0.7 convert_reduce_fusion
  15.8 0.6 convolution_convert_fusion
  16.4 2.1 reshape.69
  18.6 8.3 %concatenate.21 = bf16[64,104,128]{2,1,0:T(8,128)(2,1)} concatenate(bf16[64,96,128]{2,1,0:T(8,128)(2,1)} %reshape.69, bf16[64,2,128]{2,1,0:T(2,128)(2,1)S(1)} %reshape.70, bf16[64,2,128]{2,1,0:T(2,128)(2,1)S(1)} %reshape.71, bf16[64,2,128]{2,1,0:T(2,128)(2,1)S(1)} %broadcast_in_dim.85, bf16[64,2,128]{2,1,0:T(2,128)(2,1)S(1)} %broadcast_in_dim.87), dimensions={1} | concatenate | bytes 3407872 | tf_op jit(solution)/shard_map/concatenate | solution.py:320
  26.9 12.1 %all-to-all-start = ((bf16[64,104,128]{2,1,0:T(8,128)(2,1)}), bf16[64,104,128]{2,1,0:T(8,128)(2,1)S(1)}, u32[]{:S(2)}, u32[]{:S(2)}) async-start(bf16[64,104,128]{2,1,0:T(8,128)(2,1)} %concatenate.21), calls=%async_computation | async-start | bytes 3407872 | tf_op jit(solution)/shard_map/all_to_all | solution.py:319
  39.1 1.6 collective-permute-start.5
  40.8 1.7 collective-permute-start.9
  42.8 2.9 %collective-permute-start.8 = (bf16[2048,256]{1,0:T(8,128)(2,1)}, bf16[2048,256]{1,0:T(8,128)(2,1)}, u32[]{:S(2)}, u32[]{:S(2)}) collective-permute-start(bf16[2048,256]{1,0:T(8,128)(2,1)} %bitcast.54), channel_id=1, source_target_pairs={{0,3},{1,0},{2,1},{3,2},{4,7},{5,4},{6,5},{7,6},{8,11},{9,8},{10,9... | collective-permute-start | bytes 3145736 | tf_op jit(solution)/shard_map/ppermute | solution.py:241
  45.7 1.1 slice_bitcast_fusion.5
  46.8 0.6 collective-permute-start.11
  47.3 1.5 fusion
  48.9 1.9 fusion.16
  50.7 3.3 %convolution_convert_fusion.1 = bf16[256,2048]{1,0:T(8,128)(2,1)} fusion(bf16[128,2048]{1,0:T(8,128)(2,1)S(1)} %copy-done, bf16[2048,128]{1,0:T(8,128)(2,1)} %param.36, bf16[256,2048]{1,0:T(8,128)(2,1)} %param.28, f32[2048]{0:T(1024)S(1)} %copy-done.20, f32[256]{0:T(256)S(1)} %add_rsqrt_fusion, f32[256,128]{1,0:T(8,128)S(1)} %fusion.16), kind=kOutput, calls=%fused_computation.8 | convolution fusion | flops 271253504 | bytes 3286016 | tf_op jit(solution)/shard_map/dot_general | solution.py:24
  54.0 2.1 constant_dynamic-slice_fusion.3
  56.1 25.8 %all-to-all-done = bf16[64,104,128]{2,1,0:T(8,128)(2,1)S(1)} async-done(((bf16[64,104,128]{2,1,0:T(8,128)(2,1)}), bf16[64,104,128]{2,1,0:T(8,128)(2,1)S(1)}, u32[]{:S(2)}, u32[]{:S(2)}) %all-to-all-start) | async-done | bytes 1703968 | tf_op jit(solution)/shard_map/all_to_all | solution.py:319
  81.9 1.3 slice.173
  83.2 3.7 %reshape.73.x_ref = bf16[384,2048]{1,0:T(8,128)(2,1)} reshape(bf16[64,96,128]{2,1,0:T(8,128)(2,1)} %slice.173) | data formatting | bytes 3145728 | tf_op jit(solution)/shard_map/reshape | solution.py:346
  86.9 0.7 slice.164.got_ref
  87.6 1.7 state_scan.1
  89.3 5.4 %all-to-all-start.1 = ((bf16[64,2,128]{2,1,0:T(2,128)(2,1)}), bf16[64,2,128]{2,1,0:T(2,128)(2,1)S(1)}, u32[]{:S(2)}, u32[]{:S(2)}) async-start(bf16[64,2,128]{2,1,0:T(2,128)(2,1)} %state_scan.1), calls=%async_computation.1 | async-start | bytes 65536 | tf_op jit(solution)/shard_map/all_to_all | solution.py:326
  94.7 4.3 %hidden_units.4 = bf16[384,256]{1,0:T(8,128)(2,1)} custom-call(bf16[384,2048]{1,0:T(8,128)(2,1)} %reshape.73.x_ref, bf16[2048,256]{1,0:T(8,128)(2,1)} %bitcast.55, bf16[2048,256]{1,0:T(8,128)(2,1)} %bitcast.58), custom_call_target="tpu_custom_call" | custom-call | flops 805306368 | bytes 4194304 | tf_op jit(solution)/shard_map/hidden_units/pallas_call | solution.py:218
  99.0 1.6 collective-permute-start.7
  100.6 1.6 collective-permute-start.6
  102.2 4.3 %hidden_units.6 = bf16[384,256]{1,0:T(8,128)(2,1)} custom-call(bf16[384,2048]{1,0:T(8,128)(2,1)} %reshape.73.x_ref, bf16[2048,256]{1,0:T(8,128)(2,1)} %collective-permute-done.8.gate_ref, bf16[2048,256]{1,0:T(8,128)(2,1)} %collective-permute-done.9.up_ref), custom_call_target="tpu_custom_call" | custom-call | flops 805306368 | bytes 4194304 | tf_op jit(solution)/shard_map/hidden_units/pallas_call | solution.py:218
  106.5 0.6 fusion.48
  107.1 1.7 collective-permute-start.10
  108.8 3.2 %fusion.41 = f32[384,2048]{1,0:T(8,128)} fusion(bf16[128,2048]{1,0:T(8,128)(2,1)} %collective-permute-done.11, bf16[384,256]{1,0:T(8,128)(2,1)S(1)} %copy-done.16), kind=kOutput, calls=%fused_computation.68 | convolution fusion | flops 201326592 | bytes 3768320 | tf_op jit(solution)/shard_map/dot_general | solution.py:24
  112.1 1.7 add_convert_fusion.4
  113.8 0.5 collective-permute-start.13
  114.3 1.6 collective-permute-start.12
  115.8 4.3 %hidden_units.5 = bf16[384,256]{1,0:T(8,128)(2,1)} custom-call(bf16[384,2048]{1,0:T(8,128)(2,1)} %reshape.73.x_ref, bf16[2048,256]{1,0:T(8,128)(2,1)} %collective-permute-done.4.gate_ref, bf16[2048,256]{1,0:T(8,128)(2,1)} %collective-permute-done.5.up_ref), custom_call_target="tpu_custom_call" | custom-call | flops 805306368 | bytes 4194304 | tf_op jit(solution)/shard_map/hidden_units/pallas_call | solution.py:218
  120.2 6.4 %collective-permute-done.6 = bf16[128,2048]{1,0:T(8,128)(2,1)} collective-permute-done((bf16[128,2048]{1,0:T(8,128)(2,1)}, bf16[128,2048]{1,0:T(8,128)(2,1)}, u32[]{:S(2)}, u32[]{:S(2)}) %collective-permute-start.6) | collective-permute-done | bytes 524320 | tf_op jit(solution)/shard_map/ppermute | solution.py:237
  126.6 1.8 collective-permute-start.15
  128.6 1.7 fusion.44
  130.3 2.9 %add_convert_fusion.3 = bf16[384,2048]{1,0:T(8,128)(2,1)} fusion(f32[384,2048]{1,0:T(8,128)S(1)} %fusion.44, bf16[128,2048]{1,0:T(8,128)(2,1)} %collective-permute-done.6, bf16[384,256]{1,0:T(8,128)(2,1)S(1)} %copy-done.18), kind=kOutput, calls=%fused_computation.3 | convolution fusion | flops 202899456 | bytes 5341184 | tf_op jit(solution)/shard_map/dot_general | solution.py:24
  133.2 2.9 %add_convert_fusion.2 = bf16[384,2048]{1,0:T(8,128)(2,1)} fusion(f32[384,2048]{1,0:T(8,128)S(1)} %copy-done.3, bf16[128,2048]{1,0:T(8,128)(2,1)} %collective-permute-done.10, bf16[384,256]{1,0:T(8,128)(2,1)S(1)} %copy-done.16), kind=kOutput, calls=%fused_computation.2 | convolution fusion | flops 202899456 | bytes 5341184 | tf_op jit(solution)/shard_map/dot_general | solution.py:24
  136.1 12.9 %collective-permute-done.12.gate_ref = bf16[2048,256]{1,0:T(8,128)(2,1)S(1)} collective-permute-done((bf16[2048,256]{1,0:T(8,128)(2,1)}, bf16[2048,256]{1,0:T(8,128)(2,1)S(1)}, u32[]{:S(2)}, u32[]{:S(2)}) %collective-permute-start.12) | collective-permute-done | bytes 1048608 | tf_op jit(solution)/shard_map/ppermute | solution.py:237
  149.0 1.0 copy-done.13
  150.0 1.0 copy-done.12
  150.9 4.3 %hidden_units.7 = bf16[384,256]{1,0:T(8,128)(2,1)} custom-call(bf16[384,2048]{1,0:T(8,128)(2,1)} %reshape.73.x_ref, bf16[2048,256]{1,0:T(8,128)(2,1)} %copy-done.13, bf16[2048,256]{1,0:T(8,128)(2,1)} %copy-done.12), custom_call_target="tpu_custom_call" | custom-call | flops 805306368 | bytes 4194304 | tf_op jit(solution)/shard_map/hidden_units/pallas_call | solution.py:218
  155.2 0.6 copy.25
  155.8 5.9 %mixer_out.1 = bf16[4,128,2048]{2,1,0:T(8,128)(2,1)} custom-call(s32[1]{0:T(128)} %bitcast.rank_ref, f32[512,256]{1,0:T(8,128)} %get-tuple-element.10.part_ref, bf16[512,256]{1,0:T(8,128)(2,1)} %get-tuple-element.11.reach_ref, bf16[64,256]{1,0:T(8,128)(2,1)} %bitcast.59, f32[1,256]{1,0:T(1,128)} %bitcast.63, bf16[256,2048]{1,0:T(8,128)(2,1)} %w_ref.1), custom_call_target="tpu_custom_call" | custom-call | flops 536870912 | bytes 4194304 | tf_op jit(solution)/shard_map/mixer_out/pallas_call | solution.py:175
  161.8 2.0 slice_bitcast_fusion.7
  164.2 1.8 fusion.38
  166.0 2.0 add_convert_fusion
  168.0 2.1 reshape.74
  170.1 10.6 %all-to-all-start.2 = ((bf16[64,96,128]{2,1,0:T(8,128)(2,1)}), bf16[64,96,128]{2,1,0:T(8,128)(2,1)}, u32[]{:S(2)}, u32[]{:S(2)}) async-start(bf16[64,96,128]{2,1,0:T(8,128)(2,1)} %reshape.74), calls=%async_computation.2 | async-start | bytes 3145728 | tf_op jit(solution)/shard_map/all_to_all | solution.py:365
  180.9 0.7 copy-done.11
  181.7 2.8 %collective-permute-start.2 = (bf16[96,2048]{1,0:T(8,128)(2,1)S(1)}, bf16[96,2048]{1,0:T(8,128)(2,1)S(1)}, u32[]{:S(2)}, u32[]{:S(2)}) collective-permute-start(bf16[96,2048]{1,0:T(8,128)(2,1)S(1)} %pad_maximum_fusion.1), channel_id=1, source_target_pairs={{0,3},{1,0},{2,1},{3,2},{4,7},{5,4},{6,5},{7,6},{8,11},{9,8},{10,9... | collective-permute-start | bytes 1179656 | tf_op jit(solution)/shard_map/ppermute | solution.py:241
  184.5 1.0 fusion.13
  185.7 7.4 %collective-permute-done.2 = bf16[96,2048]{1,0:T(8,128)(2,1)S(1)} collective-permute-done((bf16[96,2048]{1,0:T(8,128)(2,1)S(1)}, bf16[96,2048]{1,0:T(8,128)(2,1)S(1)}, u32[]{:S(2)}, u32[]{:S(2)}) %collective-permute-start.2) | collective-permute-done | bytes 393248 | tf_op jit(solution)/shard_map/ppermute | solution.py:241
  193.3 3.8 %collective-permute-start.3 = (bf16[192,2048]{1,0:T(8,128)(2,1)S(1)}, bf16[192,2048]{1,0:T(8,128)(2,1)S(1)}, u32[]{:S(2)}, u32[]{:S(2)}) collective-permute-start(bf16[192,2048]{1,0:T(8,128)(2,1)S(1)} %pad_maximum_fusion), channel_id=1, source_target_pairs={{0,3},{1,0},{2,1},{3,2},{4,7},{5,4},{6,5},{7,6},{8,11},{9,8},{10,9... | collective-permute-start | bytes 2359304 | tf_op jit(solution)/shard_map/ppermute | solution.py:241
  197.1 9.0 %collective-permute-done.1 = bf16[192,2048]{1,0:T(8,128)(2,1)S(1)} collective-permute-done((bf16[192,2048]{1,0:T(8,128)(2,1)S(1)}, bf16[192,2048]{1,0:T(8,128)(2,1)S(1)}, u32[]{:S(2)}, u32[]{:S(2)}) %collective-permute-start.1) | collective-permute-done | bytes 786464 | tf_op jit(solution)/shard_map/ppermute | solution.py:237
  206.2 7.2 %collective-permute-done.3 = bf16[192,2048]{1,0:T(8,128)(2,1)S(1)} collective-permute-done((bf16[192,2048]{1,0:T(8,128)(2,1)S(1)}, bf16[192,2048]{1,0:T(8,128)(2,1)S(1)}, u32[]{:S(2)}, u32[]{:S(2)}) %collective-permute-start.3) | collective-permute-done | bytes 786464 | tf_op jit(solution)/shard_map/ppermute | solution.py:241
  213.4 0.4 convert_add_fusion
  213.8 1.2 copy-done.7
  215.0 0.9 slice.225
  215.8 4.8 %all-to-all-done.2 = bf16[64,96,128]{2,1,0:T(8,128)(2,1)} async-done(((bf16[64,96,128]{2,1,0:T(8,128)(2,1)}), bf16[64,96,128]{2,1,0:T(8,128)(2,1)}, u32[]{:S(2)}, u32[]{:S(2)}) %all-to-all-start.2) | async-done | bytes 1572896 | tf_op jit(solution)/shard_map/all_to_all | solution.py:365
  220.6 2.5 %reshape.75 = bf16[384,2048]{1,0:T(8,128)(2,1)S(1)} reshape(bf16[64,96,128]{2,1,0:T(8,128)(2,1)} %all-to-all-done.2) | data formatting | bytes 3145728 | tf_op jit(solution)/shard_map/reshape | solution.py:368
  223.2 0.5 fusion.67
  223.7 2.2 fusion.11
  (82 shorter events, 2.7 us)
Async XLA Ops:
  0.6 50.1 %copy-start = (bf16[128,2048]{1,0:T(8,128)(2,1)S(1)}, bf16[128,2048]{1,0:T(8,128)(2,1)}, u32[]{:S(2)}) copy-start(bf16[128,2048]{1,0:T(8,128)(2,1)} %param.37) | copy-start | bytes 1572868
  2.1 12.6 %copy-start.22 = (s32[256,4]{0,1:T(4,128)S(1)}, s32[256,4]{0,1:T(4,128)}, u32[]{:S(2)}) copy-start(s32[256,4]{0,1:T(4,128)} %param.30) | copy-start | bytes 12292
  2.2 13.4 %copy-start.9 = (bf16[256,2048]{1,0:T(8,128)(2,1)S(1)}, bf16[256,2048]{1,0:T(8,128)(2,1)}, u32[]{:S(2)}) copy-start(bf16[256,2048]{1,0:T(8,128)(2,1)} %param.28) | copy-start | bytes 3145732
  2.2 13.6 %copy-start.20 = (f32[2048]{0:T(1024)S(1)}, f32[2048]{0:T(1024)}, u32[]{:S(2)}) copy-start(f32[2048]{0:T(1024)} %param.29) | copy-start | bytes 24580
  16.4 2.1 copy-start.19
  26.9 18.7 %copy-start.8 = (bf16[1,256,2048]{2,1,0:T(8,128)(2,1)S(1)}, bf16[1,256,2048]{2,1,0:T(8,128)(2,1)}, u32[]{:S(2)}) copy-start(bf16[1,256,2048]{2,1,0:T(8,128)(2,1)} %param.34) | copy-start | bytes 3145732
  26.9 55.0 %all-to-all-start = ((bf16[64,104,128]{2,1,0:T(8,128)(2,1)}), bf16[64,104,128]{2,1,0:T(8,128)(2,1)S(1)}, u32[]{:S(2)}, u32[]{:S(2)}) async-start(bf16[64,104,128]{2,1,0:T(8,128)(2,1)} %concatenate.21), calls=%async_computation | async-start | bytes 3407872 | tf_op jit(solution)/shard_map/all_to_all | solution.py:319
  39.1 75.2 %collective-permute-start.5 = (bf16[2048,256]{1,0:T(8,128)(2,1)}, bf16[2048,256]{1,0:T(8,128)(2,1)}, u32[]{:S(2)}, u32[]{:S(2)}) collective-permute-start(bf16[2048,256]{1,0:T(8,128)(2,1)} %bitcast.56), channel_id=1, source_target_pairs={{0,1},{1,2},{2,3},{3,0},{4,5},{5,6},{6,7},{7,4},{8,9},{9,10},{10,1... | collective-permute-start | bytes 3145736 | tf_op jit(solution)/shard_map/ppermute | solution.py:237
  40.8 58.3 %collective-permute-start.9 = (bf16[2048,256]{1,0:T(8,128)(2,1)}, bf16[2048,256]{1,0:T(8,128)(2,1)}, u32[]{:S(2)}, u32[]{:S(2)}) collective-permute-start(bf16[2048,256]{1,0:T(8,128)(2,1)} %bitcast.57), channel_id=1, source_target_pairs={{0,3},{1,0},{2,1},{3,2},{4,7},{5,4},{6,5},{7,6},{8,11},{9,8},{10,9... | collective-permute-start | bytes 3145736 | tf_op jit(solution)/shard_map/ppermute | solution.py:241
  42.4 71.4 %collective-permute-start.4 = (bf16[2048,256]{1,0:T(8,128)(2,1)}, bf16[2048,256]{1,0:T(8,128)(2,1)}, u32[]{:S(2)}, u32[]{:S(2)}) collective-permute-start(bf16[2048,256]{1,0:T(8,128)(2,1)} %bitcast.53), channel_id=1, source_target_pairs={{0,1},{1,2},{2,3},{3,0},{4,5},{5,6},{6,7},{7,4},{8,9},{9,10},{10,1... | collective-permute-start | bytes 3145736 | tf_op jit(solution)/shard_map/ppermute | solution.py:237
  42.8 57.8 %collective-permute-start.8 = (bf16[2048,256]{1,0:T(8,128)(2,1)}, bf16[2048,256]{1,0:T(8,128)(2,1)}, u32[]{:S(2)}, u32[]{:S(2)}) collective-permute-start(bf16[2048,256]{1,0:T(8,128)(2,1)} %bitcast.54), channel_id=1, source_target_pairs={{0,3},{1,0},{2,1},{3,2},{4,7},{5,4},{6,5},{7,6},{8,11},{9,8},{10,9... | collective-permute-start | bytes 3145736 | tf_op jit(solution)/shard_map/ppermute | solution.py:241
  46.8 60.3 %collective-permute-start.11 = (bf16[128,2048]{1,0:T(8,128)(2,1)}, bf16[128,2048]{1,0:T(8,128)(2,1)}, u32[]{:S(2)}, u32[]{:S(2)}) collective-permute-start(bf16[128,2048]{1,0:T(8,128)(2,1)} %get-tuple-element.33), channel_id=1, source_target_pairs={{0,3},{1,0},{2,1},{3,2},{4,7},{5,4},{6,5},{7,6},{8,11},{9,8},{10,9... | collective-permute-start | bytes 1572872 | tf_op jit(solution)/shard_map/ppermute | solution.py:241
  89.3 66.0 %all-to-all-start.1 = ((bf16[64,2,128]{2,1,0:T(2,128)(2,1)}), bf16[64,2,128]{2,1,0:T(2,128)(2,1)S(1)}, u32[]{:S(2)}, u32[]{:S(2)}) async-start(bf16[64,2,128]{2,1,0:T(2,128)(2,1)} %state_scan.1), calls=%async_computation.1 | async-start | bytes 65536 | tf_op jit(solution)/shard_map/all_to_all | solution.py:326
  99.0 29.4 %collective-permute-start.7 = (bf16[128,2048]{1,0:T(8,128)(2,1)}, bf16[128,2048]{1,0:T(8,128)(2,1)}, u32[]{:S(2)}, u32[]{:S(2)}) collective-permute-start(bf16[128,2048]{1,0:T(8,128)(2,1)} %get-tuple-element.33), channel_id=1, source_target_pairs={{0,1},{1,2},{2,3},{3,0},{4,5},{5,6},{6,7},{7,4},{8,9},{9,10},{10,1... | collective-permute-start | bytes 1572872 | tf_op jit(solution)/shard_map/ppermute | solution.py:237
  100.6 5.9 %copy-start.17 = (bf16[384,256]{1,0:T(8,128)(2,1)S(1)}, bf16[384,256]{1,0:T(8,128)(2,1)}, u32[]{:S(2)}) copy-start(bf16[384,256]{1,0:T(8,128)(2,1)} %hidden_units.4) | copy-start | bytes 589828
  100.6 26.0 %collective-permute-start.6 = (bf16[128,2048]{1,0:T(8,128)(2,1)}, bf16[128,2048]{1,0:T(8,128)(2,1)}, u32[]{:S(2)}, u32[]{:S(2)}) collective-permute-start(bf16[128,2048]{1,0:T(8,128)(2,1)} %get-tuple-element.32), channel_id=1, source_target_pairs={{0,1},{1,2},{2,3},{3,0},{4,5},{5,6},{6,7},{7,4},{8,9},{9,10},{10,1... | collective-permute-start | bytes 1572872 | tf_op jit(solution)/shard_map/ppermute | solution.py:237
  106.5 2.3 %copy-start.16 = (bf16[384,256]{1,0:T(8,128)(2,1)S(1)}, bf16[384,256]{1,0:T(8,128)(2,1)}, u32[]{:S(2)}) copy-start(bf16[384,256]{1,0:T(8,128)(2,1)} %hidden_units.6) | copy-start | bytes 589828
  107.1 26.1 %collective-permute-start.10 = (bf16[128,2048]{1,0:T(8,128)(2,1)}, bf16[128,2048]{1,0:T(8,128)(2,1)}, u32[]{:S(2)}, u32[]{:S(2)}) collective-permute-start(bf16[128,2048]{1,0:T(8,128)(2,1)} %get-tuple-element.32), channel_id=1, source_target_pairs={{0,3},{1,0},{2,1},{3,2},{4,7},{5,4},{6,5},{7,6},{8,11},{9,8},{10,9... | collective-permute-start | bytes 1572872 | tf_op jit(solution)/shard_map/ppermute | solution.py:241
  113.8 35.2 %collective-permute-start.13 = (bf16[2048,256]{1,0:T(8,128)(2,1)}, bf16[2048,256]{1,0:T(8,128)(2,1)S(1)}, u32[]{:S(2)}, u32[]{:S(2)}) collective-permute-start(bf16[2048,256]{1,0:T(8,128)(2,1)} %collective-permute-done.9.up_ref), channel_id=1, source_target_pairs={{0,3},{1,0},{2,1},{3,2},{4,7},{5,4},{6,5},{7,6},{8,11},{9,8},{10,9... | collective-permute-start | bytes 3145736 | tf_op jit(solution)/shard_map/ppermute | solution.py:241
  114.3 34.7 %collective-permute-start.12 = (bf16[2048,256]{1,0:T(8,128)(2,1)}, bf16[2048,256]{1,0:T(8,128)(2,1)S(1)}, u32[]{:S(2)}, u32[]{:S(2)}) collective-permute-start(bf16[2048,256]{1,0:T(8,128)(2,1)} %collective-permute-done.4.gate_ref), channel_id=1, source_target_pairs={{0,1},{1,2},{2,3},{3,0},{4,5},{5,6},{6,7},{7,4},{8,9},{9,10},{10,1... | collective-permute-start | bytes 3145736 | tf_op jit(solution)/shard_map/ppermute | solution.py:237
  120.2 10.1 %copy-start.18 = (bf16[384,256]{1,0:T(8,128)(2,1)S(1)}, bf16[384,256]{1,0:T(8,128)(2,1)}, u32[]{:S(2)}) copy-start(bf16[384,256]{1,0:T(8,128)(2,1)} %hidden_units.5) | copy-start | bytes 589828
  126.6 37.6 %collective-permute-start.15 = (bf16[128,2048]{1,0:T(8,128)(2,1)}, bf16[128,2048]{1,0:T(8,128)(2,1)}, u32[]{:S(2)}, u32[]{:S(2)}) collective-permute-start(bf16[128,2048]{1,0:T(8,128)(2,1)} %collective-permute-done.11), channel_id=1, source_target_pairs={{0,3},{1,0},{2,1},{3,2},{4,7},{5,4},{6,5},{7,6},{8,11},{9,8},{10,9... | collective-permute-start | bytes 1572872 | tf_op jit(solution)/shard_map/ppermute | solution.py:241
  128.4 37.5 %collective-permute-start.14 = (bf16[128,2048]{1,0:T(8,128)(2,1)}, bf16[128,2048]{1,0:T(8,128)(2,1)}, u32[]{:S(2)}, u32[]{:S(2)}) collective-permute-start(bf16[128,2048]{1,0:T(8,128)(2,1)} %collective-permute-done.6), channel_id=1, source_target_pairs={{0,1},{1,2},{2,3},{3,0},{4,5},{5,6},{6,7},{7,4},{8,9},{9,10},{10,1... | collective-permute-start | bytes 1572872 | tf_op jit(solution)/shard_map/ppermute | solution.py:237
  130.3 2.9 %copy-start.3 = (f32[384,2048]{1,0:T(8,128)S(1)}, f32[384,2048]{1,0:T(8,128)}, u32[]{:S(2)}) copy-start(f32[384,2048]{1,0:T(8,128)} %fusion.41) | copy-start | bytes 9437188
  149.0 1.0 copy-start.13
  150.0 1.0 copy-start.12
  155.8 8.3 %copy-start.15 = (bf16[384,256]{1,0:T(8,128)(2,1)S(1)}, bf16[384,256]{1,0:T(8,128)(2,1)}, u32[]{:S(2)}) copy-start(bf16[384,256]{1,0:T(8,128)(2,1)} %hidden_units.7) | copy-start | bytes 589828
  161.8 4.2 %copy-start.6 = (bf16[384,2048]{1,0:T(8,128)(2,1)S(1)}, bf16[384,2048]{1,0:T(8,128)(2,1)}, u32[]{:S(2)}) copy-start(bf16[384,2048]{1,0:T(8,128)(2,1)} %add_convert_fusion.2) | copy-start | bytes 4718596
  163.8 2.2 copy-start.4
  163.8 2.2 copy-start.5
  163.8 20.7 %collective-permute-start = (bf16[96,2048]{1,0:T(8,128)(2,1)}, bf16[96,2048]{1,0:T(8,128)(2,1)}, u32[]{:S(2)}, u32[]{:S(2)}) collective-permute-start(bf16[96,2048]{1,0:T(8,128)(2,1)} %get-tuple-element.30), channel_id=1, source_target_pairs={{0,1},{1,2},{2,3},{3,0},{4,5},{5,6},{6,7},{7,4},{8,9},{9,10},{10,1... | collective-permute-start | bytes 1179656 | tf_op jit(solution)/shard_map/ppermute | solution.py:237
  170.1 10.6 %copy-start.2 = (bf16[4,128,2048]{2,1,0:T(8,128)(2,1)S(1)}, bf16[4,128,2048]{2,1,0:T(8,128)(2,1)}, u32[]{:S(2)}) copy-start(bf16[4,128,2048]{2,1,0:T(8,128)(2,1)} %mixer_out.1) | copy-start | bytes 6291460
  170.1 50.5 %all-to-all-start.2 = ((bf16[64,96,128]{2,1,0:T(8,128)(2,1)}), bf16[64,96,128]{2,1,0:T(8,128)(2,1)}, u32[]{:S(2)}, u32[]{:S(2)}) async-start(bf16[64,96,128]{2,1,0:T(8,128)(2,1)} %reshape.74), calls=%async_computation.2 | async-start | bytes 3145728 | tf_op jit(solution)/shard_map/all_to_all | solution.py:365
  180.7 1.0 copy-start.11
  181.7 11.4 %copy-start.10 = (bf16[64,2048]{1,0:T(8,128)(2,1)S(1)}, bf16[64,2048]{1,0:T(8,128)(2,1)}, u32[]{:S(2)}) copy-start(bf16[64,2048]{1,0:T(8,128)(2,1)} %get-tuple-element.36) | copy-start | bytes 786436
  181.7 11.4 %collective-permute-start.2 = (bf16[96,2048]{1,0:T(8,128)(2,1)S(1)}, bf16[96,2048]{1,0:T(8,128)(2,1)S(1)}, u32[]{:S(2)}, u32[]{:S(2)}) collective-permute-start(bf16[96,2048]{1,0:T(8,128)(2,1)S(1)} %pad_maximum_fusion.1), channel_id=1, source_target_pairs={{0,3},{1,0},{2,1},{3,2},{4,7},{5,4},{6,5},{7,6},{8,11},{9,8},{10,9... | collective-permute-start | bytes 1179656 | tf_op jit(solution)/shard_map/ppermute | solution.py:241
  185.6 11.5 %copy-start.21 = (f32[64,4]{0,1:T(4,128)S(1)}, f32[64,4]{0,1:T(4,128)}, u32[]{:S(2)}) copy-start(f32[64,4]{0,1:T(4,128)} %param.31) | copy-start | bytes 3076
  185.6 27.8 %copy-start.14 = (bf16[64,2048]{1,0:T(8,128)(2,1)S(1)}, bf16[64,2048]{1,0:T(8,128)(2,1)}, u32[]{:S(2)}) copy-start(bf16[64,2048]{1,0:T(8,128)(2,1)} %get-tuple-element.34) | copy-start | bytes 786436
  185.6 20.6 %collective-permute-start.1 = (bf16[192,2048]{1,0:T(8,128)(2,1)S(1)}, bf16[192,2048]{1,0:T(8,128)(2,1)S(1)}, u32[]{:S(2)}, u32[]{:S(2)}) collective-permute-start(bf16[192,2048]{1,0:T(8,128)(2,1)S(1)} %fusion.7), channel_id=1, source_target_pairs={{0,1},{1,2},{2,3},{3,0},{4,5},{5,6},{6,7},{7,4},{8,9},{9,10},{10,1... | collective-permute-start | bytes 2359304 | tf_op jit(solution)/shard_map/ppermute | solution.py:237
  193.3 20.1 %collective-permute-start.3 = (bf16[192,2048]{1,0:T(8,128)(2,1)S(1)}, bf16[192,2048]{1,0:T(8,128)(2,1)S(1)}, u32[]{:S(2)}, u32[]{:S(2)}) collective-permute-start(bf16[192,2048]{1,0:T(8,128)(2,1)S(1)} %pad_maximum_fusion), channel_id=1, source_target_pairs={{0,3},{1,0},{2,1},{3,2},{4,7},{5,4},{6,5},{7,6},{8,11},{9,8},{10,9... | collective-permute-start | bytes 2359304 | tf_op jit(solution)/shard_map/ppermute | solution.py:241
  213.8 1.2 copy-start.7
  223.2 2.7 %copy-start.1 = (bf16[128,2048]{1,0:T(8,128)(2,1)S(1)}, bf16[128,2048]{1,0:T(8,128)(2,1)}, u32[]{:S(2)}) copy-start(bf16[128,2048]{1,0:T(8,128)(2,1)} %param.37) | copy-start | bytes 1572868

commit v2 on v1

--- a/solution.py
+++ b/solution.py
@@ -142,12 +142,17 @@
     lax.fori_loop(0, got_ref.shape[0], step, jnp.zeros((2, 128), f32), unroll=8)
 
 
-def state_scan(got):
+def state_scan(arrived, pieces):
+    peers = arrived.shape[0]
     return pl.pallas_call(
         state_scan_body,
-        out_shape=jax.ShapeDtypeStruct((got.shape[0], 2, 128), bf16),
+        grid=(1,),
+        in_specs=[pl.BlockSpec((peers, 8, 128), lambda i: (0, pieces // 8, 0))],
+        out_specs=pl.BlockSpec((peers, 2, 128), lambda i: (0, 0, 0)),
+        out_shape=jax.ShapeDtypeStruct((peers, 2, 128), bf16),
+        compiler_params=pltpu.CompilerParams(vmem_limit_bytes=60 << 20),
         name="state_scan",
-    )(got)
+    )(arrived)
 
 
 def split_bf16(x):
@@ -194,43 +199,212 @@
     )(rank, part, reach, state, gain, w_out)
 
 
-def hidden_units_body(x_ref, gate_ref, up_ref, out_ref, gate_sum, up_sum):
+def dispatch_body(
+    rank_ref, x_ref, choice_ref, gain_ref, state_ref, total_ref, out_ref, slot_ref, rows_ref
+):
+    quarter, model = x_ref.shape
+    experts, stride, _ = out_ref.shape
+    capacity = (stride - 8) * 128 // model
+    per_row = model // 128
+    hidden = norm_rows(x_ref[...], gain_ref[...])
+    expert_at = lax.broadcasted_iota(jnp.int32, (quarter, experts), 1)
+    chosen = [choice_ref[:, k : k + 1] == expert_at for k in range(TOP_K)]
+    named = sum(one.astype(f32) for one in chosen)
+    earlier = lax.broadcasted_iota(jnp.int32, (quarter, quarter), 0) > lax.broadcasted_iota(
+        jnp.int32, (quarter, quarter), 1
+    )
+    ranks = dot(earlier.astype(bf16), named.astype(bf16))
+    for k in range(TOP_K):
+        place = jnp.sum(jnp.where(chosen[k], ranks, 0.0), axis=-1, keepdims=True)
+        slot_ref[:, k : k + 1] = choice_ref[:, k : k + 1] * capacity + place.astype(jnp.int32)
+    for c in range(capacity):
+        holds = jnp.where(ranks == c, named, 0.0).astype(bf16)
+        rows = dot(holds, hidden, 0, 0)
+        for k in range(per_row):
+            rows_ref[pl.ds(c * per_row + k, experts, stride=stride), :] = rows[
+                :, k * 128 : (k + 1) * 128
+            ]
+    base = stride - 8
+    state_high = state_ref[...].astype(bf16).astype(f32)
+    total = jnp.broadcast_to(total_ref[...], state_ref.shape)
+    total_high = total.astype(bf16).astype(f32)
+    sent = (state_high, state_ref[...] - state_high, total_high, total - total_high)
+    for i, part in enumerate(sent):
+        for j in range(2):
+            rows_ref[pl.ds(base + 2 * i + j, experts, stride=stride), :] = part[
+                :, j * 128 : (j + 1) * 128
+            ]
+
+    def narrow(e, carry):
+        at = pl.multiple_of(e * stride, 8)
+        out_ref[e] = rows_ref[pl.ds(at, stride), :].astype(bf16)
+        return carry
+
+    lax.fori_loop(0, experts, narrow, 0)
+
+
+def dispatch(rank, moe_in, choice, gain, state, total, quarter, experts, pieces):
+    model = moe_in.shape[1]
+    mine = lambda i, rank: (rank[0], 0)
+    whole = lambda i, rank: (0, 0)
+    return pl.pallas_call(
+        dispatch_body,
+        grid_spec=pltpu.PrefetchScalarGridSpec(
+            num_scalar_prefetch=1,
+            grid=(1,),
+            in_specs=[
+                pl.BlockSpec((quarter, model), mine),
+                pl.BlockSpec((quarter, TOP_K), mine),
+                pl.BlockSpec((1, model), whole),
+                pl.BlockSpec(state.shape, whole),
+                pl.BlockSpec(total.shape, whole),
+            ],
+            out_specs=[
+                pl.BlockSpec((experts, pieces + 8, 128), lambda i, rank: (0, 0, 0)),
+                pl.BlockSpec((quarter, TOP_K), whole),
+            ],
+            scratch_shapes=[pltpu.VMEM((experts * (pieces + 8), 128), f32)],
+        ),
+        out_shape=[
+            jax.ShapeDtypeStruct((experts, pieces + 8, 128), bf16),
+            jax.ShapeDtypeStruct((quarter, TOP_K), jnp.int32),
+        ],
+        name="dispatch",
+    )(rank, moe_in, choice, gain, state, total)
+
+
+def hidden_units_body(got_ref, *refs):
+    groups = (len(refs) - 4) // 2
+    gates, ups = refs[:groups], refs[groups : 2 * groups]
+    out_ref, rows_ref, x_ref, sums_ref = refs[2 * groups :]
     step = pl.program_id(0)
+    peers, pieces, _ = got_ref.shape
+    steps, slots, part = x_ref.shape
+    capacity = slots // peers
+    per_row = pieces // capacity
 
     @pl.when(step == 0)
     def _():
-        gate_sum[...] = jnp.zeros(gate_sum.shape, f32)
-        up_sum[...] = jnp.zeros(up_sum.shape, f32)
-
-    x = x_ref[...]
-    gate_sum[...] += dot(x, gate_ref[...])
-    up_sum[...] += dot(x, up_ref[...])
-
-    @pl.when(step == pl.num_programs(0) - 1)
+        def widen(e, carry):
+            at = pl.multiple_of(e * pieces, 8)
+            rows_ref[pl.ds(at, pieces), :] = got_ref[e].astype(f32)
+            return carry
+
+        lax.fori_loop(0, peers, widen, 0)
+        for c in range(capacity):
+            for k in range(per_row):
+                column = k * 128 % part
+                x_ref[k * 128 // part, c * peers : (c + 1) * peers, column : column + 128] = (
+                    rows_ref[pl.ds(c * per_row + k, peers, stride=pieces), :].astype(bf16)
+                )
+        sums_ref[...] = jnp.zeros(sums_ref.shape, f32)
+
+    x = x_ref[step]
+    for i, ref in enumerate(gates + ups):
+        sums_ref[i] += dot(x, ref[...])
+
+    @pl.when(step == steps - 1)
     def _():
-        out_ref[...] = (jax.nn.silu(gate_sum[...]) * up_sum[...]).astype(bf16)
-
-
-def hidden_units(x, gate, up):
-    rows, model = x.shape
-    width = gate.shape[1]
-    part = model // 4
+        for i in range(groups):
+            out_ref[i] = (jax.nn.silu(sums_ref[i]) * sums_ref[groups + i]).astype(bf16)
+
+
+def hidden_units(arrived, gates, ups, pieces):
+    peers = arrived.shape[0]
+    model, width = gates[0].shape
+    slots = peers * pieces * 128 // model
+    steps = 4
+    part = model // steps
+    groups = len(gates)
+    weight = pl.BlockSpec((part, width), lambda i: (i, 0))
     return pl.pallas_call(
         hidden_units_body,
-        grid=(model // part,),
-        in_specs=[
-            pl.BlockSpec((rows, part), lambda i: (0, i)),
-            pl.BlockSpec((part, width), lambda i: (i, 0)),
-            pl.BlockSpec((part, width), lambda i: (i, 0)),
+        grid=(steps,),
+        in_specs=[pl.BlockSpec((peers, pieces, 128), lambda i: (0, 0, 0))]
+        + [weight] * (2 * groups),
+        out_specs=pl.BlockSpec((groups, slots, width), lambda i: (0, 0, 0)),
+        out_shape=jax.ShapeDtypeStruct((groups, slots, width), bf16),
+        scratch_shapes=[
+            pltpu.VMEM((peers * pieces, 128), f32),
+            pltpu.VMEM((steps, slots, part), bf16),
+            pltpu.VMEM((2 * groups, slots, width), f32),
         ],
-        out_specs=pl.BlockSpec((rows, width), lambda i: (0, 0)),
-        out_shape=jax.ShapeDtypeStruct((rows, width), bf16),
-        scratch_shapes=[pltpu.VMEM((rows, width), f32)] * 2,
+        compiler_params=pltpu.CompilerParams(vmem_limit_bytes=60 << 20),
         cost_estimate=pl.CostEstimate(
-            flops=rows * model * width * 4, bytes_accessed=4 << 20, transcendentals=0
+            flops=slots * model * width * 4 * groups,
+            bytes_accessed=10 << 20,
+            transcendentals=0,
         ),
         name="hidden_units",
-    )(x, gate, up)
+    )(arrived, *gates, *ups)
+
+
+def results_body(act_ref, *refs):
+    groups = act_ref.shape[0]
+    halves = refs[: 2 * groups]
+    out_ref, weight_ref, sum_ref, rows_ref, sems = refs[2 * groups :]
+    half = halves[0].shape[0]
+    copies = []
+    for i, ref in enumerate(halves):
+        at = pl.ds(i % 2 * half, half)
+        copies.append(pltpu.make_async_copy(ref, weight_ref.at[i // 2, at], sems.at[i]))
+        copies[-1].start()
+    slots, model = sum_ref.shape
+    peers, pieces, _ = out_ref.shape
+    capacity = slots // peers
+    per_row = model // 128
+    part = 256
+    for g in range(groups):
+        copies[2 * g].wait()
+        copies[2 * g + 1].wait()
+        act = act_ref[g]
+        for col in range(0, model, part):
+            cols = slice(col, col + part)
+            one = dot(act, weight_ref[g, :, cols]).astype(bf16).astype(f32)
+            if g == 0:
+                sum_ref[:, cols] = one
+            elif g < groups - 1:
+                sum_ref[:, cols] += one
+            else:
+                whole = sum_ref[:, cols] + one
+                for c in range(capacity):
+                    for j in range(part // 128):
+                        k = col // 128 + j
+                        rows_ref[pl.ds(c * per_row + k, peers, stride=pieces), :] = whole[
+                            c * peers : (c + 1) * peers, j * 128 : (j + 1) * 128
+                        ]
+
+    def narrow(e, carry):
+        at = pl.multiple_of(e * pieces, 8)
+        out_ref[e] = rows_ref[pl.ds(at, pieces), :].astype(bf16)
+        return carry
+
+    lax.fori_loop(0, peers, narrow, 0)
+
+
+def results(acts, halves, peers):
+    groups, slots, width = acts.shape
+    model = halves[0].shape[1]
+    pieces = slots // peers * model // 128
+    hbm = pl.BlockSpec(memory_space=pltpu.HBM)
+    vmem = pl.BlockSpec(memory_space=pltpu.VMEM)
+    return pl.pallas_call(
+        results_body,
+        in_specs=[vmem] + [hbm] * len(halves),
+        out_specs=vmem,
+        out_shape=jax.ShapeDtypeStruct((peers, pieces, 128), bf16),
+        scratch_shapes=[
+            pltpu.VMEM((groups, width, model), bf16),
+            pltpu.VMEM((slots, model), f32),
+            pltpu.VMEM((peers * pieces, 128), f32),
+            pltpu.SemaphoreType.DMA((len(halves),)),
+        ],
+        compiler_params=pltpu.CompilerParams(vmem_limit_bytes=60 << 20),
+        cost_estimate=pl.CostEstimate(
+            flops=slots * model * width * 2 * groups, bytes_accessed=6 << 20, transcendentals=0
+        ),
+        name="results",
+    )(acts, *halves)
 
 
 def shift_up(x):
@@ -294,33 +468,12 @@
     part, reach, added, total = mixer_local(
         mix_in, shifts, mix_gain[None], w_query, w_forget, w_value, forget_room[None]
     )
-    added_high, added_low = split_bf16(added)
-    total_high, total_low = split_bf16(total)
-    whole_row = lambda x: jnp.broadcast_to(x.reshape(1, 2, 128), (HEAD, 2, 128))
-    state_send = [
-        added_high.reshape(HEAD, 2, 128),
-        added_low.reshape(HEAD, 2, 128),
-        whole_row(total_high),
-        whole_row(total_low),
-    ]
-
-    moe_in, expert_choice = lax.optimization_barrier((moe_in, expert_choice, total))[:2]
-    own_rows = lax.dynamic_slice_in_dim(moe_in, tp_rank * quarter, quarter, 0)
-    own_hidden = norm_rows(own_rows, moe_gain)
-    labels = lax.dynamic_slice_in_dim(expert_choice, tp_rank * quarter, quarter, 0).reshape(-1)
-    onehot = labels[:, None] == jnp.arange(experts, dtype=jnp.int32)[None, :]
-    earlier = jnp.arange(labels.shape[0])[:, None] > jnp.arange(labels.shape[0])[None, :]
-    counts = dot(earlier.astype(bf16), onehot.astype(bf16))
-    places = jnp.sum(jnp.where(onehot, counts, 0.0), axis=-1).astype(jnp.int32)
-    slot_ids = (labels * capacity + places).reshape(quarter, TOP_K)
-    slot_axis = jnp.arange(slots, dtype=jnp.int32)
-    holds = sum((slot_ids[:, k][None, :] == slot_axis[:, None]).astype(bf16) for k in range(TOP_K))
-    outgoing = dot(holds, own_hidden).astype(bf16)
-    arrived = lax.all_to_all(
-        jnp.concatenate([outgoing.reshape(experts, pieces, 128)] + state_send, axis=1),
-        EP, split_axis=0, concat_axis=0, tiled=True,
-    )
-    state_next = state_scan(arrived[:, pieces:])
+    outgoing, slot_ids = dispatch(
+        tp_rank.reshape(1), moe_in, expert_choice, moe_gain[None], added, total,
+        quarter, experts, pieces,
+    )
+    arrived = lax.all_to_all(outgoing, EP, split_axis=0, concat_axis=0, tiled=True)
+    state_next = state_scan(arrived, pieces)
     top_far = shift_up(after(top_below, state_next))
     low_far = shift_down(after(low_above, state_next))
     state_start = lax.all_to_all(
@@ -343,14 +496,13 @@
         axis=0,
     )
 
-    x = arrived[:, :pieces].reshape(slots, model)
-    acts = [
-        hidden_units(x, gate_own, up_own),
-        hidden_units(x, gate_below, up_below),
-        hidden_units(x, gate_above, up_above),
-        hidden_units(x, gate_far, up_far),
-    ]
-    down = [(top, low), (top_below, low_below), (top_above, low_above), (top_far, low_far)]
+    acts = hidden_units(
+        arrived,
+        [gate_own, gate_below, gate_above, gate_far],
+        [up_own, up_below, up_above, up_far],
+        pieces,
+    )
+    slot_axis = jnp.arange(slots, dtype=jnp.int32)
     weights = jax.nn.sigmoid(route_logit)
     weights = weights / jnp.sum(weights, axis=-1, keepdims=True) * route_scale
     choose = sum(
@@ -358,14 +510,13 @@
         for k in range(TOP_K)
     )
     choose_high, choose_low = split_bf16(choose)
-    summed = sum(
-        (dot(a[:, :half_units], top) + dot(a[:, half_units:], low)).astype(bf16).astype(f32)
-        for a, (top, low) in zip(acts, down)
-    )
-    returned = lax.all_to_all(
-        summed.astype(bf16).reshape(experts, pieces, 128),
-        EP, split_axis=0, concat_axis=0, tiled=True,
-    ).reshape(slots, model)
+    ready = results(
+        acts,
+        [top, low, top_below, low_below, top_above, low_above, top_far, low_far],
+        experts,
+    )
+    returned = lax.all_to_all(ready, EP, split_axis=0, concat_axis=0, tiled=True)
+    returned = returned.reshape(slots, model)
     routed = dot(choose_high, returned) + dot(choose_low, returned)
 
     across = chunk(2)

time: 227 us -> 207 us (0.912)
  matrix products: 25.5 us -> 7.21 us
  local copies, waits for them, and re-layouts: 33.7 us -> 18.5 us
  starting transfers between devices: 51.2 us -> 57.2 us
  Pallas kernels: 36.7 us -> 42.3 us
  waiting for transfers between devices: 73.7 us -> 78.1 us
    ppermute x8, waiting for transfers between devices: 28.3 us -> 57.4 us  [shift_up(): return lax.ppermute(x, 'tp', UP)]
    all_to_all x2, waiting for transfers between devices: 30.6 us -> 4.37 us  [the longest x1 4.37 us: local(): lax.all_to_all(ready, EP, split_axis=0, concat_axis=0, tiled=True)]
    dot_general x14 -> x4, matrix products: 25.5 us -> 7.21 us  [dot(): lax.dot_general(a, b, (((ca,), (cb,)), ((), ())), preferred_element_type=...]
    concatenate x1 -> x0, local copies, waits for them, and re-layouts: 8.32 us -> none  [local(): jnp.concatenate([outgoing.reshape(experts, pieces, 128)] + state_send, ax...]
    reshape x6 -> x1, local copies, waits for them, and re-layouts: 10.4 us -> 2.55 us  [local(): returned = returned.reshape(slots, model)]
    pallas_call x5 -> x4, Pallas kernels: 19 us -> 24.7 us  [the longest x1 10.4 us: hidden_units(): pl.pallas_call(hidden_units_body, grid=(steps,), in_specs=[pl.BlockSpec((...]
    all_to_all x1, starting transfers between devices: 5.43 us -> 10.3 us  [local(): lax.all_to_all(state_next, EP, split_axis=0, concat_axis=0, tiled=True)]
    ppermute x8, starting transfers between devices: 15.7 us -> 19.7 us  [shift_down(): return lax.ppermute(x, 'tp', DOWN)]
  transfers between devices with their start and end apart: 19 -> 19, of which waited for: 7 -> 8; matrix products, arithmetic and copies ran while one was open for 18% -> 7% of each run, Pallas kernels for 11% -> 13%
where the time goes in v2:
time: 207 us; the launch traced here: 206 us
  waiting for transfers between devices  78.1 us (38%)
  starting transfers between devices  57.2 us (28%)
  Pallas kernels  42.3 us (20%)
  local copies, waits for them, and re-layouts  18.5 us (9%)
  matrix products  7.21 us (3%)
    ppermute x8, waiting for transfers between devices, shift_up(): return lax.ppermute(x, 'tp', UP)  57.4 us
    ppermute x8, starting transfers between devices, shift_down(): return lax.ppermute(x, 'tp', DOWN)  19.7 us
    ppermute x8, waiting for transfers between devices, shift_down(): return lax.ppermute(x, 'tp', DOWN)  16.4 us
    all_to_all x1, starting transfers between devices, local(): lax.all_to_all(outgoing, EP, split_axis=0, concat_axis=0, tiled=True)  12 us
    pallas_call x1, Pallas kernels, mixer_local(): pl.pallas_call(mixer_local_body, in_specs=[pl.BlockSpec(memory_space=pltp...  11.7 us
    all_to_all x1, starting transfers between devices, local(): lax.all_to_all(ready, EP, split_axis=0, concat_axis=0, tiled=True)  10.6 us
    pallas_call x1, Pallas kernels, hidden_units(): pl.pallas_call(hidden_units_body, grid=(steps,), in_specs=[pl.BlockSpec((...  10.4 us
    all_to_all x1, starting transfers between devices, local(): lax.all_to_all(state_next, EP, split_axis=0, concat_axis=0, tiled=True)  10.3 us
  transfers between devices with their start and end apart: 19, of which 8 were waited for; matrix products, arithmetic and copies ran while one was open for 7% of the time, Pallas kernels for 13%

profile of v2, /device:TPU:2, one launch (start us, length us, event | category | flops | bytes accessed | tf_op | source)
XLA Modules:
  0.0 206.3 jit_solution(9947388175484326256)
XLA Ops:
  0.6 0.0 copy-start
  0.6 0.8 reshape.33
  1.5 0.7 slice_reduce_fusion.4.shift_ref
  2.2 1.5 copy.23.choice_ref
  3.6 11.7 %mixer_local.1 = (f32[512,256]{1,0:T(8,128)}, bf16[512,256]{1,0:T(8,128)(2,1)}, f32[64,256]{1,0:T(8,128)}, f32[1,256]{1,0:T(1,128)}) custom-call(f32[8]{0:T(128)} %slice_reduce_fusion.4.shift_ref, bf16[512,2048]{1,0:T(8,128)(2,1)} %x_hbm.1, f32[1,2048]{1,0:T(1,128)} %bitcast.54, bf16[2048,256]{1,0:T(8,128)(2,1)} %wq_hbm.1, bf16[2048,256]{1,0:T(8,128)(2,1)} %wf_hbm.1, ...), custom_call_target="tpu_custom_call" | custom-call | flops 1610612736 | bytes 6291456 | tf_op jit(solution)/shard_map/mixer_local/pallas_call | solution.py:111
  15.4 3.9 %dispatch.1 = (bf16[64,104,128]{2,1,0:T(8,128)(2,1)}, s32[64,4]{1,0:T(8,128)}) custom-call(s32[1]{0:T(128)} %bitcast.rank_ref, bf16[256,2048]{1,0:T(8,128)(2,1)} %x_ref.1, s32[256,4]{1,0:T(8,128)} %copy.23.choice_ref, f32[1,2048]{1,0:T(1,128)} %bitcast.46, f32[64,256]{1,0:T(8,128)} %get-tuple-element.12.state_ref, f32[1,256]{1,0:T(1,128)} %get-tuple-element.13.total_ref), custom_call_target="tpu_custom_call" | custom-call | tf_op jit(solution)/shard_map/dispatch/pallas_call | solution.py:250
  19.3 12.0 %all-to-all-start = ((bf16[64,104,128]{2,1,0:T(8,128)(2,1)}), bf16[64,104,128]{2,1,0:T(8,128)(2,1)S(1)}, u32[]{:S(2)}, u32[]{:S(2)}) async-start(bf16[64,104,128]{2,1,0:T(8,128)(2,1)} %get-tuple-element.14), calls=%async_computation | async-start | bytes 3407872 | tf_op jit(solution)/shard_map/all_to_all | solution.py:475
  31.3 0.0 copy-start.4
  31.4 1.7 collective-permute-start.4
  33.0 1.7 collective-permute-start.8
  34.7 1.8 collective-permute-start.5
  36.5 0.2 collective-permute-start.7
  36.7 2.3 %slice_bitcast_fusion.4 = (bf16[128,2048]{1,0:T(8,128)(2,1)}, bf16[128,2048]{1,0:T(8,128)(2,1)}) fusion(bf16[1,256,2048]{2,1,0:T(8,128)(2,1)} %param.34), kind=kLoop, calls=%fused_computation.22 | loop fusion | bytes 2097152 | tf_op jit(solution)/shard_map/slice | solution.py:461
  39.0 0.4 collective-permute-start.10
  39.4 0.3 fusion.2
  39.7 19.3 %collective-permute-done.4.refs_1_ = bf16[2048,256]{1,0:T(8,128)(2,1)} collective-permute-done((bf16[2048,256]{1,0:T(8,128)(2,1)}, bf16[2048,256]{1,0:T(8,128)(2,1)}, u32[]{:S(2)}, u32[]{:S(2)}) %collective-permute-start.4) | collective-permute-done | bytes 1048608 | tf_op jit(solution)/shard_map/ppermute | solution.py:411
  59.0 0.4 collective-permute-start.6
  59.4 2.9 %collective-permute-start.9 = (bf16[2048,256]{1,0:T(8,128)(2,1)}, bf16[2048,256]{1,0:T(8,128)(2,1)}, u32[]{:S(2)}, u32[]{:S(2)}) collective-permute-start(bf16[2048,256]{1,0:T(8,128)(2,1)} %collective-permute-done.8.refs_6_), channel_id=1, source_target_pairs={{0,3},{1,0},{2,1},{3,2},{4,7},{5,4},{6,5},{7,6},{8,11},{9,8},{10,9... | collective-permute-start | bytes 3145736 | tf_op jit(solution)/shard_map/ppermute | solution.py:415
  62.2 1.5 fusion.13
  63.8 28.9 %collective-permute-done.10.refs_2_ = bf16[128,2048]{1,0:T(8,128)(2,1)} collective-permute-done((bf16[128,2048]{1,0:T(8,128)(2,1)}, bf16[128,2048]{1,0:T(8,128)(2,1)}, u32[]{:S(2)}, u32[]{:S(2)}) %collective-permute-start.10) | collective-permute-done | bytes 524320 | tf_op jit(solution)/shard_map/ppermute | solution.py:411
  92.7 1.8 collective-permute-start.13
  94.5 3.0 %convolution_convert_fusion = bf16[256,2048]{1,0:T(8,128)(2,1)} fusion(bf16[128,2048]{1,0:T(8,128)(2,1)S(1)} %copy-done, bf16[2048,128]{1,0:T(8,128)(2,1)} %param.36, bf16[256,2048]{1,0:T(8,128)(2,1)S(1)} %copy-done.4, f32[2048]{0:T(1024)S(1)} %copy-done.12, f32[256]{0:T(256)S(1)} %add_rsqrt_fusion, f32[256,128]{1,0:T(8,128)S(1)} %fusion.13), kind=kOutput, calls=%fused_computation.2 | convolution fusion | flops 271253504 | bytes 3286016 | tf_op jit(solution)/shard_map/dot_general | solution.py:24
  97.5 2.1 constant_dynamic-slice_fusion.3
  99.5 1.2 copy-done.2
  100.8 1.7 state_scan.1
  102.5 10.3 %all-to-all-start.1 = ((bf16[64,2,128]{2,1,0:T(2,128)(2,1)}), bf16[64,2,128]{2,1,0:T(2,128)(2,1)S(1)}, u32[]{:S(2)}, u32[]{:S(2)}) async-start(bf16[64,2,128]{2,1,0:T(2,128)(2,1)} %state_scan.1), calls=%async_computation.1 | async-start | bytes 65536 | tf_op jit(solution)/shard_map/all_to_all | solution.py:479
  112.8 1.6 collective-permute-done.13.refs_5_
  114.4 1.6 collective-permute-start.11
  116.0 1.7 collective-permute-start.12
  117.7 0.4 collective-permute-start.14
  118.0 0.0 collective-permute-done.6.refs_3_
  118.0 2.9 %collective-permute-start.15 = (bf16[128,2048]{1,0:T(8,128)(2,1)}, bf16[128,2048]{1,0:T(8,128)(2,1)S(1)}, u32[]{:S(2)}, u32[]{:S(2)}) collective-permute-start(bf16[128,2048]{1,0:T(8,128)(2,1)} %collective-permute-done.13.refs_5_), channel_id=1, source_target_pairs={{0,3},{1,0},{2,1},{3,2},{4,7},{5,4},{6,5},{7,6},{8,11},{9,8},{10,9... | collective-permute-start | bytes 1572872 | tf_op jit(solution)/shard_map/ppermute | solution.py:415
  120.9 10.4 %hidden_units.1.act_ref = bf16[4,384,256]{2,1,0:T(8,128)(2,1)} custom-call(bf16[64,104,128]{2,1,0:T(8,128)(2,1)} %copy-done.2, bf16[2048,256]{1,0:T(8,128)(2,1)} %bitcast.50, bf16[2048,256]{1,0:T(8,128)(2,1)} %collective-permute-done.4.refs_1_, bf16[2048,256]{1,0:T(8,128)(2,1)} %collective-permute-done.5.refs_2_, ...), custom_call_target="tpu_custom_call" | custom-call | flops 3221225472 | bytes 10485760 | tf_op jit(solution)/shard_map/hidden_units/pallas_call | solution.py:320
  131.3 0.6 copy.26
  131.9 5.9 %mixer_out.1 = bf16[4,128,2048]{2,1,0:T(8,128)(2,1)} custom-call(s32[1]{0:T(128)} %bitcast.rank_ref, f32[512,256]{1,0:T(8,128)} %get-tuple-element.10.part_ref, bf16[512,256]{1,0:T(8,128)(2,1)} %get-tuple-element.11.reach_ref, bf16[64,256]{1,0:T(8,128)(2,1)} %bitcast.44, f32[1,256]{1,0:T(1,128)} %bitcast.47, bf16[256,2048]{1,0:T(8,128)(2,1)} %w_ref.1), custom_call_target="tpu_custom_call" | custom-call | flops 536870912 | bytes 4194304 | tf_op jit(solution)/shard_map/mixer_out/pallas_call | solution.py:180
  137.8 1.9 slice_bitcast_fusion.7
  139.7 0.0 collective-permute-start
  139.7 0.4 collective-permute-done.14.refs_6_
  140.1 0.4 copy-done.7
  140.5 0.2 copy-done.8
  140.7 0.3 copy-done.9
  140.9 0.8 copy-done.10
  141.7 8.7 %results.1 = bf16[64,96,128]{2,1,0:T(8,128)(2,1)} custom-call(bf16[4,384,256]{2,1,0:T(8,128)(2,1)} %hidden_units.1.act_ref, bf16[128,2048]{1,0:T(8,128)(2,1)} %get-tuple-element.29.refs_0_, bf16[128,2048]{1,0:T(8,128)(2,1)} %get-tuple-element.28.refs_1_, bf16[128,2048]{1,0:T(8,128)(2,1)} %collective-permute-done.10.refs_2_, bf16[128,2048]{1,0:T(8,128)(2,1)} %copy-done.7, ...), custom_call_target="tpu_custom_call" | custom-call | flops 1610612736 | bytes 6291456 | tf_op jit(solution)/shard_map/results/pallas_call | solution.py:391
  150.4 10.6 %all-to-all-start.2 = ((bf16[64,96,128]{2,1,0:T(8,128)(2,1)}), bf16[64,96,128]{2,1,0:T(8,128)(2,1)}, u32[]{:S(2)}, u32[]{:S(2)}) async-start(bf16[64,96,128]{2,1,0:T(8,128)(2,1)} %results.1), calls=%async_computation.2 | async-start | bytes 3145728 | tf_op jit(solution)/shard_map/all_to_all | solution.py:518
  161.0 0.2 slice_bitcast_fusion.3
  161.3 0.7 copy-done.5
  162.0 3.2 %collective-permute-start.2 = (bf16[96,2048]{1,0:T(8,128)(2,1)S(1)}, bf16[96,2048]{1,0:T(8,128)(2,1)S(1)}, u32[]{:S(2)}, u32[]{:S(2)}) collective-permute-start(bf16[96,2048]{1,0:T(8,128)(2,1)S(1)} %pad_maximum_fusion.1), channel_id=1, source_target_pairs={{0,3},{1,0},{2,1},{3,2},{4,7},{5,4},{6,5},{7,6},{8,11},{9,8},{10,9... | collective-permute-start | bytes 1179656 | tf_op jit(solution)/shard_map/ppermute | solution.py:415
  165.3 1.0 fusion.10
  166.3 0.1 fusion.8
  166.4 0.1 collective-permute-start.1
  166.4 7.5 %collective-permute-done.2 = bf16[96,2048]{1,0:T(8,128)(2,1)S(1)} collective-permute-done((bf16[96,2048]{1,0:T(8,128)(2,1)S(1)}, bf16[96,2048]{1,0:T(8,128)(2,1)S(1)}, u32[]{:S(2)}, u32[]{:S(2)}) %collective-permute-start.2) | collective-permute-done | bytes 393248 | tf_op jit(solution)/shard_map/ppermute | solution.py:415
  173.9 0.1 fusion.9
  174.0 0.1 pad_maximum_fusion
  174.1 3.8 %collective-permute-start.3 = (bf16[192,2048]{1,0:T(8,128)(2,1)S(1)}, bf16[192,2048]{1,0:T(8,128)(2,1)S(1)}, u32[]{:S(2)}, u32[]{:S(2)}) collective-permute-start(bf16[192,2048]{1,0:T(8,128)(2,1)S(1)} %pad_maximum_fusion), channel_id=1, source_target_pairs={{0,3},{1,0},{2,1},{3,2},{4,7},{5,4},{6,5},{7,6},{8,11},{9,8},{10,9... | collective-permute-start | bytes 2359304 | tf_op jit(solution)/shard_map/ppermute | solution.py:415
  177.9 0.2 slice_reduce_fusion.3
  178.2 8.8 %collective-permute-done.1 = bf16[192,2048]{1,0:T(8,128)(2,1)S(1)} collective-permute-done((bf16[192,2048]{1,0:T(8,128)(2,1)S(1)}, bf16[192,2048]{1,0:T(8,128)(2,1)S(1)}, u32[]{:S(2)}, u32[]{:S(2)}) %collective-permute-start.1) | collective-permute-done | bytes 786464 | tf_op jit(solution)/shard_map/ppermute | solution.py:411
  186.9 7.3 %collective-permute-done.3 = bf16[192,2048]{1,0:T(8,128)(2,1)S(1)} collective-permute-done((bf16[192,2048]{1,0:T(8,128)(2,1)S(1)}, bf16[192,2048]{1,0:T(8,128)(2,1)S(1)}, u32[]{:S(2)}, u32[]{:S(2)}) %collective-permute-start.3) | collective-permute-done | bytes 786464 | tf_op jit(solution)/shard_map/ppermute | solution.py:415
  194.2 0.4 convert_add_fusion
  194.6 1.2 copy-done.3
  195.7 0.9 slice.147
  196.6 4.4 %all-to-all-done.2 = bf16[64,96,128]{2,1,0:T(8,128)(2,1)} async-done(((bf16[64,96,128]{2,1,0:T(8,128)(2,1)}), bf16[64,96,128]{2,1,0:T(8,128)(2,1)}, u32[]{:S(2)}, u32[]{:S(2)}) %all-to-all-start.2) | async-done | bytes 1572896 | tf_op jit(solution)/shard_map/all_to_all | solution.py:518
  201.0 2.5 %reshape.35 = bf16[384,2048]{1,0:T(8,128)(2,1)S(1)} reshape(bf16[64,96,128]{2,1,0:T(8,128)(2,1)} %all-to-all-done.2) | data formatting | bytes 3145728 | tf_op jit(solution)/shard_map/reshape | solution.py:519
  203.5 0.5 fusion.22
  204.0 2.2 %fusion.1 = bf16[64,2048]{1,0:T(8,128)(2,1)} fusion(f32[64,2048]{1,0:T(8,128)S(1)} %fusion.22, bf16[384,2048]{1,0:T(8,128)(2,1)S(1)} %reshape.35, f32[192,2048]{1,0:T(8,128)} %copy-done.3, f32[64]{0:T(128)S(1)} %get-tuple-element.35, s32[64]{0:T(128)S(1)} %get-tuple-element.19, f32[64]{0:T(128)S(1)} %get-tuple-element.36, s32[64]{0:T(128)S(1)} %get-tuple-element.20, ...), kind=kOutput, calls=%fused_computation.5 | convolution fusion | flops 101351424 | bytes 2885632 | tf_op jit(solution)/shard_map/dot_general | solution.py:24
  (34 shorter events, 0.1 us)
Async XLA Ops:
  0.6 93.9 %copy-start = (bf16[128,2048]{1,0:T(8,128)(2,1)S(1)}, bf16[128,2048]{1,0:T(8,128)(2,1)}, u32[]{:S(2)}) copy-start(bf16[128,2048]{1,0:T(8,128)(2,1)} %param.37) | copy-start | bytes 1572868
  19.3 80.2 %all-to-all-start = ((bf16[64,104,128]{2,1,0:T(8,128)(2,1)}), bf16[64,104,128]{2,1,0:T(8,128)(2,1)S(1)}, u32[]{:S(2)}, u32[]{:S(2)}) async-start(bf16[64,104,128]{2,1,0:T(8,128)(2,1)} %get-tuple-element.14), calls=%async_computation | async-start | bytes 3407872 | tf_op jit(solution)/shard_map/all_to_all | solution.py:475
  31.3 8.0 %copy-start.4 = (bf16[256,2048]{1,0:T(8,128)(2,1)S(1)}, bf16[256,2048]{1,0:T(8,128)(2,1)}, u32[]{:S(2)}) copy-start(bf16[256,2048]{1,0:T(8,128)(2,1)} %x_ref.1) | copy-start | bytes 3145732
  31.4 27.6 %collective-permute-start.4 = (bf16[2048,256]{1,0:T(8,128)(2,1)}, bf16[2048,256]{1,0:T(8,128)(2,1)}, u32[]{:S(2)}, u32[]{:S(2)}) collective-permute-start(bf16[2048,256]{1,0:T(8,128)(2,1)} %bitcast.48), channel_id=1, source_target_pairs={{0,1},{1,2},{2,3},{3,0},{4,5},{5,6},{6,7},{7,4},{8,9},{9,10},{10,1... | collective-permute-start | bytes 3145736 | tf_op jit(solution)/shard_map/ppermute | solution.py:411
  33.0 29.2 %copy-start.12 = (f32[2048]{0:T(1024)S(1)}, f32[2048]{0:T(1024)}, u32[]{:S(2)}) copy-start(f32[2048]{0:T(1024)} %param.29) | copy-start | bytes 24580
  33.0 26.3 %collective-permute-start.8 = (bf16[2048,256]{1,0:T(8,128)(2,1)}, bf16[2048,256]{1,0:T(8,128)(2,1)}, u32[]{:S(2)}, u32[]{:S(2)}) collective-permute-start(bf16[2048,256]{1,0:T(8,128)(2,1)} %bitcast.51), channel_id=1, source_target_pairs={{0,3},{1,0},{2,1},{3,2},{4,7},{5,4},{6,5},{7,6},{8,11},{9,8},{10,9... | collective-permute-start | bytes 3145736 | tf_op jit(solution)/shard_map/ppermute | solution.py:415
  34.7 81.3 %collective-permute-start.5 = (bf16[2048,256]{1,0:T(8,128)(2,1)}, bf16[2048,256]{1,0:T(8,128)(2,1)}, u32[]{:S(2)}, u32[]{:S(2)}) collective-permute-start(bf16[2048,256]{1,0:T(8,128)(2,1)} %bitcast.49), channel_id=1, source_target_pairs={{0,3},{1,0},{2,1},{3,2},{4,7},{5,4},{6,5},{7,6},{8,11},{9,8},{10,9... | collective-permute-start | bytes 3145736 | tf_op jit(solution)/shard_map/ppermute | solution.py:415
  36.5 81.2 %collective-permute-start.7 = (bf16[2048,256]{1,0:T(8,128)(2,1)}, bf16[2048,256]{1,0:T(8,128)(2,1)}, u32[]{:S(2)}, u32[]{:S(2)}) collective-permute-start(bf16[2048,256]{1,0:T(8,128)(2,1)} %bitcast.52), channel_id=1, source_target_pairs={{0,1},{1,2},{2,3},{3,0},{4,5},{5,6},{6,7},{7,4},{8,9},{9,10},{10,1... | collective-permute-start | bytes 3145736 | tf_op jit(solution)/shard_map/ppermute | solution.py:411
  39.0 53.7 %collective-permute-start.10 = (bf16[128,2048]{1,0:T(8,128)(2,1)}, bf16[128,2048]{1,0:T(8,128)(2,1)}, u32[]{:S(2)}, u32[]{:S(2)}) collective-permute-start(bf16[128,2048]{1,0:T(8,128)(2,1)} %get-tuple-element.29.refs_0_), channel_id=1, source_target_pairs={{0,1},{1,2},{2,3},{3,0},{4,5},{5,6},{6,7},{7,4},{8,9},{9,10},{10,1... | collective-permute-start | bytes 1572872 | tf_op jit(solution)/shard_map/ppermute | solution.py:411
  59.0 59.0 %collective-permute-start.6 = (bf16[2048,256]{1,0:T(8,128)(2,1)}, bf16[2048,256]{1,0:T(8,128)(2,1)}, u32[]{:S(2)}, u32[]{:S(2)}) collective-permute-start(bf16[2048,256]{1,0:T(8,128)(2,1)} %collective-permute-done.4.refs_1_), channel_id=1, source_target_pairs={{0,1},{1,2},{2,3},{3,0},{4,5},{5,6},{6,7},{7,4},{8,9},{9,10},{10,1... | collective-permute-start | bytes 3145736 | tf_op jit(solution)/shard_map/ppermute | solution.py:411
  59.4 61.5 %collective-permute-start.9 = (bf16[2048,256]{1,0:T(8,128)(2,1)}, bf16[2048,256]{1,0:T(8,128)(2,1)}, u32[]{:S(2)}, u32[]{:S(2)}) collective-permute-start(bf16[2048,256]{1,0:T(8,128)(2,1)} %collective-permute-done.8.refs_6_), channel_id=1, source_target_pairs={{0,3},{1,0},{2,1},{3,2},{4,7},{5,4},{6,5},{7,6},{8,11},{9,8},{10,9... | collective-permute-start | bytes 3145736 | tf_op jit(solution)/shard_map/ppermute | solution.py:415
  92.7 21.7 %collective-permute-start.13 = (bf16[128,2048]{1,0:T(8,128)(2,1)}, bf16[128,2048]{1,0:T(8,128)(2,1)}, u32[]{:S(2)}, u32[]{:S(2)}) collective-permute-start(bf16[128,2048]{1,0:T(8,128)(2,1)} %get-tuple-element.28.refs_1_), channel_id=1, source_target_pairs={{0,3},{1,0},{2,1},{3,2},{4,7},{5,4},{6,5},{7,6},{8,11},{9,8},{10,9... | collective-permute-start | bytes 1572872 | tf_op jit(solution)/shard_map/ppermute | solution.py:415
  99.5 1.2 copy-start.2
  102.5 28.8 %all-to-all-start.1 = ((bf16[64,2,128]{2,1,0:T(2,128)(2,1)}), bf16[64,2,128]{2,1,0:T(2,128)(2,1)S(1)}, u32[]{:S(2)}, u32[]{:S(2)}) async-start(bf16[64,2,128]{2,1,0:T(2,128)(2,1)} %state_scan.1), calls=%async_computation.1 | async-start | bytes 65536 | tf_op jit(solution)/shard_map/all_to_all | solution.py:479
  114.4 25.3 %collective-permute-start.11 = (bf16[128,2048]{1,0:T(8,128)(2,1)}, bf16[128,2048]{1,0:T(8,128)(2,1)S(1)}, u32[]{:S(2)}, u32[]{:S(2)}) collective-permute-start(bf16[128,2048]{1,0:T(8,128)(2,1)} %get-tuple-element.28.refs_1_), channel_id=1, source_target_pairs={{0,1},{1,2},{2,3},{3,0},{4,5},{5,6},{6,7},{7,4},{8,9},{9,10},{10,1... | collective-permute-start | bytes 1572872 | tf_op jit(solution)/shard_map/ppermute | solution.py:411
  116.0 23.7 %collective-permute-start.12 = (bf16[128,2048]{1,0:T(8,128)(2,1)}, bf16[128,2048]{1,0:T(8,128)(2,1)S(1)}, u32[]{:S(2)}, u32[]{:S(2)}) collective-permute-start(bf16[128,2048]{1,0:T(8,128)(2,1)} %get-tuple-element.29.refs_0_), channel_id=1, source_target_pairs={{0,3},{1,0},{2,1},{3,2},{4,7},{5,4},{6,5},{7,6},{8,11},{9,8},{10,9... | collective-permute-start | bytes 1572872 | tf_op jit(solution)/shard_map/ppermute | solution.py:415
  117.7 22.5 %collective-permute-start.14 = (bf16[128,2048]{1,0:T(8,128)(2,1)}, bf16[128,2048]{1,0:T(8,128)(2,1)S(1)}, u32[]{:S(2)}, u32[]{:S(2)}) collective-permute-start(bf16[128,2048]{1,0:T(8,128)(2,1)} %collective-permute-done.10.refs_2_), channel_id=1, source_target_pairs={{0,1},{1,2},{2,3},{3,0},{4,5},{5,6},{6,7},{7,4},{8,9},{9,10},{10,1... | collective-permute-start | bytes 1572872 | tf_op jit(solution)/shard_map/ppermute | solution.py:411
  118.0 22.1 %collective-permute-start.15 = (bf16[128,2048]{1,0:T(8,128)(2,1)}, bf16[128,2048]{1,0:T(8,128)(2,1)S(1)}, u32[]{:S(2)}, u32[]{:S(2)}) collective-permute-start(bf16[128,2048]{1,0:T(8,128)(2,1)} %collective-permute-done.13.refs_5_), channel_id=1, source_target_pairs={{0,3},{1,0},{2,1},{3,2},{4,7},{5,4},{6,5},{7,6},{8,11},{9,8},{10,9... | collective-permute-start | bytes 1572872 | tf_op jit(solution)/shard_map/ppermute | solution.py:415
  139.7 25.6 %collective-permute-start = (bf16[96,2048]{1,0:T(8,128)(2,1)}, bf16[96,2048]{1,0:T(8,128)(2,1)}, u32[]{:S(2)}, u32[]{:S(2)}) collective-permute-start(bf16[96,2048]{1,0:T(8,128)(2,1)} %get-tuple-element.26), channel_id=1, source_target_pairs={{0,1},{1,2},{2,3},{3,0},{4,5},{5,6},{6,7},{7,4},{8,9},{9,10},{10,1... | collective-permute-start | bytes 1179656 | tf_op jit(solution)/shard_map/ppermute | solution.py:411
  139.7 0.8 copy-start.7
  139.7 0.9 copy-start.8
  140.1 0.8 copy-start.9
  140.9 0.8 copy-start.10
  150.4 10.6 %copy-start.1 = (bf16[4,128,2048]{2,1,0:T(8,128)(2,1)S(1)}, bf16[4,128,2048]{2,1,0:T(8,128)(2,1)}, u32[]{:S(2)}) copy-start(bf16[4,128,2048]{2,1,0:T(8,128)(2,1)} %mixer_out.1) | copy-start | bytes 6291460
  150.4 50.6 %all-to-all-start.2 = ((bf16[64,96,128]{2,1,0:T(8,128)(2,1)}), bf16[64,96,128]{2,1,0:T(8,128)(2,1)}, u32[]{:S(2)}, u32[]{:S(2)}) async-start(bf16[64,96,128]{2,1,0:T(8,128)(2,1)} %results.1), calls=%async_computation.2 | async-start | bytes 3145728 | tf_op jit(solution)/shard_map/all_to_all | solution.py:518
  161.0 1.0 copy-start.5
  162.0 11.9 %collective-permute-start.2 = (bf16[96,2048]{1,0:T(8,128)(2,1)S(1)}, bf16[96,2048]{1,0:T(8,128)(2,1)S(1)}, u32[]{:S(2)}, u32[]{:S(2)}) collective-permute-start(bf16[96,2048]{1,0:T(8,128)(2,1)S(1)} %pad_maximum_fusion.1), channel_id=1, source_target_pairs={{0,3},{1,0},{2,1},{3,2},{4,7},{5,4},{6,5},{7,6},{8,11},{9,8},{10,9... | collective-permute-start | bytes 1179656 | tf_op jit(solution)/shard_map/ppermute | solution.py:415
  166.4 20.6 %collective-permute-start.1 = (bf16[192,2048]{1,0:T(8,128)(2,1)S(1)}, bf16[192,2048]{1,0:T(8,128)(2,1)S(1)}, u32[]{:S(2)}, u32[]{:S(2)}) collective-permute-start(bf16[192,2048]{1,0:T(8,128)(2,1)S(1)} %fusion.8), channel_id=1, source_target_pairs={{0,1},{1,2},{2,3},{3,0},{4,5},{5,6},{6,7},{7,4},{8,9},{9,10},{10,1... | collective-permute-start | bytes 2359304 | tf_op jit(solution)/shard_map/ppermute | solution.py:411
  173.9 4.0 %copy-start.13 = (f32[64,4]{0,1:T(4,128)S(1)}, f32[64,4]{0,1:T(4,128)}, u32[]{:S(2)}) copy-start(f32[64,4]{0,1:T(4,128)} %param.31) | copy-start | bytes 3076
  173.9 4.0 %copy-start.11 = (s32[64,4]{1,0:T(8,128)S(1)}, s32[64,4]{1,0:T(8,128)}, u32[]{:S(2)}) copy-start(s32[64,4]{1,0:T(8,128)} %get-tuple-element.15) | copy-start | bytes 3076
  173.9 20.3 %copy-start.6 = (bf16[64,2048]{1,0:T(8,128)(2,1)S(1)}, bf16[64,2048]{1,0:T(8,128)(2,1)}, u32[]{:S(2)}) copy-start(bf16[64,2048]{1,0:T(8,128)(2,1)} %get-tuple-element.30) | copy-start | bytes 786436
  174.1 20.1 %collective-permute-start.3 = (bf16[192,2048]{1,0:T(8,128)(2,1)S(1)}, bf16[192,2048]{1,0:T(8,128)(2,1)S(1)}, u32[]{:S(2)}, u32[]{:S(2)}) collective-permute-start(bf16[192,2048]{1,0:T(8,128)(2,1)S(1)} %pad_maximum_fusion), channel_id=1, source_target_pairs={{0,3},{1,0},{2,1},{3,2},{4,7},{5,4},{6,5},{7,6},{8,11},{9,8},{10,9... | collective-permute-start | bytes 2359304 | tf_op jit(solution)/shard_map/ppermute | solution.py:415
  194.6 1.2 copy-start.3

commit v3 on v2

v3 whole, which is shorter than its diff:
```python
import jax
import jax.numpy as jnp
from jax import lax
from jax.experimental import pallas as pl
from jax.experimental.pallas import tpu as pltpu
from jax.sharding import Mesh
from jax.sharding import PartitionSpec as P

HEAD = 64
SPAN = 64
TOP_K = 4
EP = ("ep_0", "ep_1", "ep_2")
EP_TP = ("ep_0", "ep_1", "ep_2", "tp")
UP = [(i, (i + 1) % 4) for i in range(4)]
DOWN = [(i, (i - 1) % 4) for i in range(4)]

epsilon = 1e-06
route_scale = 2.5
f32 = jnp.float32
bf16 = jnp.bfloat16


def dot(a, b, ca=1, cb=0, **kw):
    return lax.dot_general(a, b, (((ca,), (cb,)), ((), ())), preferred_element_type=f32, **kw)


def norm_rows(row_data, gain_vec):
    widened = row_data.astype(f32)
    scaled = widened * lax.rsqrt(jnp.mean(widened * widened, axis=-1, keepdims=True) + epsilon)
    return (scaled * gain_vec).astype(bf16)


def same_head(rows, cols):
    row_head = lax.broadcasted_iota(jnp.int32, (rows, cols), 0) // HEAD
    col_head = lax.broadcasted_iota(jnp.int32, (rows, cols), 1) // HEAD
    return row_head == col_head


def mixer_local_body(
    shift_ref, x_hbm, gain_ref, wq_hbm, wf_hbm, wv_hbm, room_ref,
    part_ref, reach_ref, state_ref, total_ref,
    x_ref, wq_ref, wf_ref, wv_ref, normed_ref, q_ref, f_ref, v_ref, carry_ref, sems,
):
    pairs = ((x_hbm, x_ref), (wf_hbm, wf_ref), (wq_hbm, wq_ref), (wv_hbm, wv_ref))
    copies = [pltpu.make_async_copy(a, b, sems.at[i]) for i, (a, b) in enumerate(pairs)]
    for copy in copies:
        copy.start()
    rows, width = q_ref.shape
    blocks = rows // SPAN
    heads = width // HEAD
    gain = gain_ref[...]

    def norm_block(n, carry):
        at = pl.ds(n * SPAN, SPAN)
        normed_ref[at, :] = norm_rows(x_ref[at, :], gain)
        return carry

    copies[0].wait()
    lax.fori_loop(0, blocks, norm_block, 0)
    normed = normed_ref[...]
    copies[1].wait()
    f_ref[...] = dot(normed, wf_ref[...])
    copies[2].wait()
    q_ref[...] = dot(normed, wq_ref[...])
    copies[3].wait()
    v_ref[...] = dot(normed, wv_ref[...])
    room = room_ref[...]
    diagonal = same_head(width, width).astype(f32)
    row_at = lax.broadcasted_iota(jnp.int32, (width, SPAN), 0) % SPAN
    causal = row_at >= lax.broadcasted_iota(jnp.int32, (width, SPAN), 1)
    lower = (
        lax.broadcasted_iota(jnp.int32, (SPAN, SPAN), 0)
        >= lax.broadcasted_iota(jnp.int32, (SPAN, SPAN), 1)
    ).astype(f32)
    carry_ref[...] = jnp.zeros((width, width), f32)

    def one_block(n, log_before):
        at = pl.ds(pl.multiple_of(n * SPAN, SPAN), SPAN)
        state = carry_ref[...]
        queries = jax.nn.silu(q_ref[at, :])
        rate = room * jax.nn.sigmoid(-(f_ref[at, :] + shift_ref[n * SPAN]))
        values = v_ref[at, :].astype(bf16)
        log_decay = dot(lower, jnp.log1p(-rate), precision=lax.Precision.HIGHEST)
        middle = log_decay[SPAN // 2 : SPAN // 2 + 1]
        block_end = log_decay[SPAN - 1 :]
        from_middle = queries * jnp.exp(log_decay - middle)
        to_middle = (rate * jnp.exp(middle - log_decay)).astype(bf16)
        by_head = (jnp.concatenate([from_middle] * heads, axis=0) * diagonal).astype(bf16)
        scores = jnp.where(causal, dot(by_head, to_middle, 1, 1), 0.0).astype(bf16)
        all_pairs = dot(scores, values) * diagonal
        mixed = all_pairs[:SPAN]
        for h in range(1, heads):
            mixed = mixed + all_pairs[h * SPAN : (h + 1) * SPAN]
        decayed = queries * jnp.exp(log_decay)
        part_ref[at, :] = mixed + dot(decayed.astype(bf16), state.astype(bf16), 1, 1)
        reach_ref[at, :] = (decayed * jnp.exp(log_before)).astype(bf16)
        to_end = (rate * jnp.exp(block_end - log_decay)).astype(bf16)
        carry_ref[...] = state * jnp.exp(block_end) + dot(values, to_end, 0, 0) * diagonal
        return log_before + block_end

    log_before = lax.fori_loop(0, blocks, one_block, jnp.zeros((1, width), f32), unroll=2)
    packed = carry_ref[:HEAD]
    for h in range(1, heads):
        packed = packed + carry_ref[h * HEAD : (h + 1) * HEAD]
    state_ref[...] = packed
    total_ref[...] = jnp.exp(log_before)


def mixer_local(mix_in, shifts, gain, w_query, w_forget, w_value, room):
    rows = mix_in.shape[0]
    width = w_query.shape[1]
    vmem = pl.BlockSpec(memory_space=pltpu.VMEM)
    hbm = pl.BlockSpec(memory_space=pltpu.HBM)
    return pl.pallas_call(
        mixer_local_body,
        in_specs=[pl.BlockSpec(memory_space=pltpu.SMEM), hbm, vmem, hbm, hbm, hbm, vmem],
        out_specs=[vmem] * 4,
        out_shape=[
            jax.ShapeDtypeStruct((rows, width), f32),
            jax.ShapeDtypeStruct((rows, width), bf16),
            jax.ShapeDtypeStruct((HEAD, width), f32),
            jax.ShapeDtypeStruct((1, width), f32),
        ],
        scratch_shapes=[pltpu.VMEM(mix_in.shape, bf16)]
        + [pltpu.VMEM(w_query.shape, bf16)] * 3
        + [pltpu.VMEM(mix_in.shape, bf16)]
        + [pltpu.VMEM((rows, width), f32)] * 3
        + [pltpu.VMEM((width, width), f32), pltpu.SemaphoreType.DMA((4,))],
        compiler_params=pltpu.CompilerParams(vmem_limit_bytes=60 << 20),
        cost_estimate=pl.CostEstimate(
            flops=rows * mix_in.shape[1] * width * 6, bytes_accessed=6 << 20, transcendentals=0
        ),
        name="mixer_local",
    )(shifts, mix_in, gain, w_query, w_forget, w_value, room)


def state_scan_body(got_ref, out_ref):
    def step(i, state):
        tile = got_ref[i].astype(f32)
        out_ref[i] = state.astype(bf16)
        added = tile[0:2] + tile[2:4]
        decay = tile[4:6] + tile[6:8]
        return decay * state + added

    lax.fori_loop(0, got_ref.shape[0], step, jnp.zeros((2, 128), f32), unroll=8)


def state_scan(arrived, pieces):
    peers = arrived.shape[0]
    return pl.pallas_call(
        state_scan_body,
        grid=(1,),
        in_specs=[pl.BlockSpec((peers, 8, 128), lambda i: (0, pieces // 8, 0))],
        out_specs=pl.BlockSpec((peers, 2, 128), lambda i: (0, 0, 0)),
        out_shape=jax.ShapeDtypeStruct((peers, 2, 128), bf16),
        compiler_params=pltpu.CompilerParams(vmem_limit_bytes=8 << 20),
        name="state_scan",
    )(arrived)


def mixer_out_body(
    rank_ref, part_hbm, reach_hbm, state_ref, gain_ref, w_hbm, shared_hbm,
    own_hbm, above_hbm, top_hbm, low_hbm, below_hbm,
    part_ref, reach_ref, w_ref, shared_ref, out_ref, in_sems, out_sems,
):
    sources = ((reach_hbm, reach_ref), (part_hbm, part_ref), (w_hbm, w_ref), (shared_hbm, shared_ref))
    loads = [pltpu.make_async_copy(a, b, in_sems.at[i]) for i, (a, b) in enumerate(sources)]
    for load in loads:
        load.start()
    count, size, _ = out_ref.shape
    width = part_ref.shape[1]
    rows, tokens = part_ref.shape[0] // count, shared_ref.shape[0] // count
    heads = width // HEAD
    half = size // 2
    diagonal = same_head(width, width).astype(f32)
    state = (jnp.concatenate([state_ref[...].astype(f32)] * heads, axis=0) * diagonal).astype(bf16)
    average = diagonal * (1.0 / HEAD)
    for load in loads:
        load.wait()
    stores = []

    def store(source, target):
        stores.append(pltpu.make_async_copy(source, target, out_sems.at[len(stores)]))
        stores[-1].start()

    for i in (2, 1, 3, 0):
        rank = (rank_ref[0] + i) % count
        at = pl.ds(pl.multiple_of(rank * rows, rows), rows)
        mixed = part_ref[at, :] + dot(reach_ref[at, :], state, 1, 1)
        square = dot(mixed * mixed, average, precision=lax.Precision.HIGHEST)
        head_out = (mixed * lax.rsqrt(square + epsilon) * gain_ref[...]).astype(bf16)
        out_ref[i, :rows] = dot(head_out, w_ref[...]).astype(bf16)
        out_ref[i, rows:] = shared_ref[pl.ds(pl.multiple_of(rank * tokens, tokens), tokens), :]
        if i == 2:
            store(out_ref.at[i, pl.ds(0, half)], top_hbm)
            store(out_ref.at[i, pl.ds(half, half)], low_hbm)
        else:
            store(out_ref.at[i], {1: above_hbm, 3: below_hbm, 0: own_hbm}[i])
    for copy in stores:
        copy.wait()


def mixer_out(rank, part, reach, state, gain, w_out, shared, tp_count):
    rows, width = part.shape
    size = (rows + shared.shape[0]) // tp_count
    model = w_out.shape[1]
    sizes = [size, size, size // 2, size // 2, size]
    vmem = pl.BlockSpec(memory_space=pltpu.VMEM)
    hbm = pl.BlockSpec(memory_space=pltpu.HBM)
    return pl.pallas_call(
        mixer_out_body,
        in_specs=[pl.BlockSpec(memory_space=pltpu.SMEM), hbm, hbm, vmem, vmem, hbm, hbm],
        out_specs=[hbm] * 5,
        out_shape=[jax.ShapeDtypeStruct((n, model), bf16) for n in sizes],
        scratch_shapes=[
            pltpu.VMEM(part.shape, f32),
            pltpu.VMEM(reach.shape, bf16),
            pltpu.VMEM(w_out.shape, bf16),
            pltpu.VMEM(shared.shape, bf16),
            pltpu.VMEM((tp_count, size, model), bf16),
            pltpu.SemaphoreType.DMA((4,)),
            pltpu.SemaphoreType.DMA((5,)),
        ],
        compiler_params=pltpu.CompilerParams(vmem_limit_bytes=56 << 20),
        cost_estimate=pl.CostEstimate(
            flops=rows * width * model * 2, bytes_accessed=6 << 20, transcendentals=0
        ),
        name="mixer_out",
    )(rank, part, reach, state, gain, w_out, shared)


def narrow_out(rows_ref, tiles_ref, out_hbm, sems):
    peers, pieces, _ = tiles_ref.shape
    parts = sems.shape[0]
    part = peers // parts
    copies = []
    for i in range(parts):

        def narrow(j, carry, i=i):
            peer = i * part + j
            at = pl.multiple_of(peer * pieces, 8)
            tiles_ref[peer] = rows_ref[pl.ds(at, pieces), :].astype(bf16)
            return carry

        lax.fori_loop(0, part, narrow, 0, unroll=2)
        at = pl.ds(i * part, part)
        copies.append(pltpu.make_async_copy(tiles_ref.at[at], out_hbm.at[at], sems.at[i]))
        copies[-1].start()
    return copies


def dispatch_body(
    rank_ref, x_ref, choice_ref, gain_ref, state_ref, total_ref, out_hbm, slot_hbm,
    rows_ref, high_ref, tiles_ref, slot_ref, sems, slot_sem,
):
    quarter, model = x_ref.shape
    experts, stride, _ = tiles_ref.shape
    capacity = (stride - 8) * 128 // model
    per_row = model // 128
    hidden = norm_rows(x_ref[...], gain_ref[...])
    expert_at = lax.broadcasted_iota(jnp.int32, (quarter, experts), 1)
    chosen = [choice_ref[:, k : k + 1] == expert_at for k in range(TOP_K)]
    named = sum(one.astype(f32) for one in chosen)
    earlier = lax.broadcasted_iota(jnp.int32, (quarter, quarter), 0) > lax.broadcasted_iota(
        jnp.int32, (quarter, quarter), 1
    )
    ranks = dot(earlier.astype(bf16), named.astype(bf16))
    for k in range(TOP_K):
        place = jnp.sum(jnp.where(chosen[k], ranks, 0.0), axis=-1, keepdims=True)
        slot_ref[:, k : k + 1] = choice_ref[:, k : k + 1] * capacity + place.astype(jnp.int32)
    for c in range(capacity):
        holds = jnp.where(ranks == c, named, 0.0).astype(bf16)
        rows = dot(holds, hidden, 0, 0)
        for k in range(per_row):
            rows_ref[pl.ds(c * per_row + k, experts, stride=stride), :] = rows[
                :, k * 128 : (k + 1) * 128
            ]
    base = stride - 8
    total = jnp.broadcast_to(total_ref[...], state_ref.shape)
    high_ref[0] = state_ref[...].astype(bf16)
    high_ref[1] = total.astype(bf16)
    state_high = high_ref[0].astype(f32)
    total_high = high_ref[1].astype(f32)
    sent = (state_high, state_ref[...] - state_high, total_high, total - total_high)
    for i, part in enumerate(sent):
        for j in range(2):
            rows_ref[pl.ds(base + 2 * i + j, experts, stride=stride), :] = part[
                :, j * 128 : (j + 1) * 128
            ]

    slot_copy = pltpu.make_async_copy(slot_ref, slot_hbm, slot_sem)
    slot_copy.start()
    for copy in narrow_out(rows_ref, tiles_ref, out_hbm, sems) + [slot_copy]:
        copy.wait()


def dispatch(rank, moe_in, choice, gain, state, total, quarter, experts, pieces):
    model = moe_in.shape[1]
    mine = lambda i, rank: (rank[0], 0)
    whole = lambda i, rank: (0, 0)
    return pl.pallas_call(
        dispatch_body,
        grid_spec=pltpu.PrefetchScalarGridSpec(
            num_scalar_prefetch=1,
            grid=(1,),
            in_specs=[
                pl.BlockSpec((quarter, model), mine),
                pl.BlockSpec((quarter, TOP_K), mine),
                pl.BlockSpec((1, model), whole),
                pl.BlockSpec(state.shape, whole),
                pl.BlockSpec(total.shape, whole),
            ],
            out_specs=[pl.BlockSpec(memory_space=pltpu.HBM)] * 2,
            scratch_shapes=[
                pltpu.VMEM((experts * (pieces + 8), 128), f32),
                pltpu.VMEM((2, *state.shape), bf16),
                pltpu.VMEM((experts, pieces + 8, 128), bf16),
                pltpu.VMEM((quarter, TOP_K), jnp.int32),
                pltpu.SemaphoreType.DMA((4,)),
                pltpu.SemaphoreType.DMA,
            ],
        ),
        out_shape=[
            jax.ShapeDtypeStruct((experts, pieces + 8, 128), bf16),
            jax.ShapeDtypeStruct((quarter, TOP_K), jnp.int32),
        ],
        compiler_params=pltpu.CompilerParams(vmem_limit_bytes=60 << 20),
        name="dispatch",
    )(rank, moe_in, choice, gain, state, total)


def widen_rows(tiles_ref, rows_ref, start, count):
    pieces = rows_ref.shape[0] // tiles_ref.shape[0]

    def widen(i, carry):
        at = pl.multiple_of((start + i) * pieces, 8)
        rows_ref[pl.ds(at, pieces), :] = tiles_ref[start + i, :pieces].astype(f32)
        return carry

    lax.fori_loop(0, count, widen, 0, unroll=2)


def gather_rows(rows_ref, x_ref, peers):
    slots, model = x_ref.shape
    capacity = slots // peers
    per_row = model // 128
    for c in range(capacity):
        for k in range(per_row):
            x_ref[c * peers : (c + 1) * peers, k * 128 : (k + 1) * 128] = rows_ref[
                pl.ds(c * per_row + k, peers, stride=capacity * per_row), :
            ].astype(bf16)


def hidden_units_body(got_ref, *refs):
    groups = (len(refs) - 3) // 2
    gates, ups = refs[:groups], refs[groups : 2 * groups]
    out_ref, rows_ref, x_ref = refs[2 * groups :]
    peers = got_ref.shape[0]
    width = gates[0].shape[1]
    widen_rows(got_ref, rows_ref, 0, peers)
    gather_rows(rows_ref, x_ref, peers)
    x = x_ref[...]
    for i in range(groups):
        act = jax.nn.silu(dot(x, gates[i][...])) * dot(x, ups[i][...])
        out_ref[:, i * width : (i + 1) * width] = act.astype(bf16)


def hidden_units(arrived, gates, ups, pieces):
    peers = arrived.shape[0]
    model, width = gates[0].shape
    slots = peers * pieces * 128 // model
    groups = len(gates)
    whole = lambda i: (0, 0)
    return pl.pallas_call(
        hidden_units_body,
        grid=(1,),
        in_specs=[pl.BlockSpec((peers, pieces, 128), lambda i: (0, 0, 0))]
        + [pl.BlockSpec((model, width), whole)] * (2 * groups),
        out_specs=pl.BlockSpec((slots, groups * width), whole),
        out_shape=jax.ShapeDtypeStruct((slots, groups * width), bf16),
        scratch_shapes=[pltpu.VMEM((peers * pieces, 128), f32), pltpu.VMEM((slots, model), bf16)],
        compiler_params=pltpu.CompilerParams(vmem_limit_bytes=56 << 20),
        cost_estimate=pl.CostEstimate(
            flops=slots * model * width * 4 * groups,
            bytes_accessed=10 << 20,
            transcendentals=0,
        ),
        name="hidden_units",
    )(arrived, *gates, *ups)


def results_body(act_ref, *refs):
    halves = refs[:-6]
    out_hbm, weight_ref, rows_ref, tiles_ref, sems, out_sems = refs[-6:]
    peers, pieces, _ = tiles_ref.shape
    slots = act_ref.shape[0]
    half, model = halves[0].shape
    capacity = slots // peers
    per_row = model // 128
    parts = sems.shape[0]
    part = model // parts
    loads = [
        [
            pltpu.make_async_copy(
                ref.at[:, pl.ds(i * part, part)],
                weight_ref.at[i, pl.ds(j * half, half)],
                sems.at[i, j],
            )
            for j, ref in enumerate(halves)
        ]
        for i in range(parts)
    ]
    for group in loads:
        for load in group:
            load.start()
    for i in range(parts):
        for load in loads[i]:
            load.wait()
        whole = dot(act_ref[...], weight_ref[i])
        for c in range(capacity):
            for j in range(part // 128):
                k = (i * part) // 128 + j
                rows_ref[pl.ds(c * per_row + k, peers, stride=pieces), :] = whole[
                    c * peers : (c + 1) * peers, j * 128 : (j + 1) * 128
                ]
    for copy in narrow_out(rows_ref, tiles_ref, out_hbm, out_sems):
        copy.wait()


def results(acts, halves, peers):
    slots, width = acts.shape
    _, model = halves[0].shape
    pieces = slots // peers * model // 128
    hbm = pl.BlockSpec(memory_space=pltpu.HBM)
    parts = 4
    return pl.pallas_call(
        results_body,
        in_specs=[pl.BlockSpec(memory_space=pltpu.VMEM)] + [hbm] * len(halves),
        out_specs=hbm,
        out_shape=jax.ShapeDtypeStruct((peers, pieces, 128), bf16),
        scratch_shapes=[
            pltpu.VMEM((parts, width, model // parts), bf16),
            pltpu.VMEM((peers * pieces, 128), f32),
            pltpu.VMEM((peers, pieces, 128), bf16),
            pltpu.SemaphoreType.DMA((parts, len(halves))),
            pltpu.SemaphoreType.DMA((4,)),
        ],
        compiler_params=pltpu.CompilerParams(vmem_limit_bytes=20 << 20),
        cost_estimate=pl.CostEstimate(
            flops=slots * model * width * 2, bytes_accessed=6 << 20, transcendentals=0
        ),
        name="results",
    )(acts, *halves)


def combine_body(got_ref, slot_ref, logit_ref, rest_ref, out_ref, rows_ref, x_ref, split_ref):
    peers = got_ref.shape[0]
    slots = x_ref.shape[0]
    capacity = slots // peers
    widen_rows(got_ref, rows_ref, 0, peers)
    gather_rows(rows_ref, x_ref, peers)
    chance = jax.nn.sigmoid(logit_ref[...])
    weights = chance / jnp.sum(chance, axis=-1, keepdims=True) * route_scale
    tokens = weights.shape[0]
    first = lax.broadcasted_iota(jnp.int32, (tokens, peers), 1) * capacity
    picks = []
    for c in range(capacity):
        picks.append(
            sum(
                jnp.where(slot_ref[:, k : k + 1] == first + c, weights[:, k : k + 1], 0.0)
                for k in range(TOP_K)
            )
        )
    pick = jnp.concatenate(picks, axis=1)
    split_ref[0] = pick.astype(bf16)
    split_ref[1] = (pick - split_ref[0].astype(f32)).astype(bf16)
    x = x_ref[...]
    routed = dot(split_ref[0], x) + dot(split_ref[1], x)
    out_ref[...] = (routed + rest_ref[...]).astype(bf16)


def combine(returned, slot_ids, route_logit, rest):
    peers, pieces, _ = returned.shape
    tokens, model = rest.shape
    slots = peers * pieces * 128 // model
    return pl.pallas_call(
        combine_body,
        out_shape=jax.ShapeDtypeStruct((tokens, model), bf16),
        scratch_shapes=[
            pltpu.VMEM((peers * pieces, 128), f32),
            pltpu.VMEM((slots, model), bf16),
            pltpu.VMEM((2, tokens, slots), bf16),
        ],
        compiler_params=pltpu.CompilerParams(vmem_limit_bytes=16 << 20),
        name="combine",
    )(returned, slot_ids, route_logit, rest)


def shift_up(x):
    return lax.ppermute(x, "tp", UP)


def shift_down(x):
    return lax.ppermute(x, "tp", DOWN)


def after(x, *others):
    return lax.optimization_barrier((x, *others))[0]


def local(
    mix_in,
    forget_shift,
    mix_gain,
    w_query,
    w_forget,
    w_value,
    forget_room,
    head_gain,
    w_out,
    moe_in,
    moe_gain,
    expert_choice,
    route_logit,
    w_exp_gate,
    w_exp_up,
    w_exp_down,
    w_sh_gate,
    w_sh_up,
    w_sh_down,
):
    tp_count = 4
    tp_rank = lax.axis_index("tp")
    row_count, model = moe_in.shape
    quarter = row_count // tp_count
    experts = lax.axis_size(EP) * w_exp_gate.shape[0]
    mean_load = quarter * TOP_K // experts
    capacity = mean_load + mean_load // 2
    pieces = capacity * model // 128

    gate_own, up_own, down_own = w_exp_gate[0], w_exp_up[0], w_exp_down[0]
    gate_below = shift_up(gate_own)
    up_above = shift_down(up_own)
    up_below = shift_up(up_own)
    gate_above = shift_down(gate_own)
    gate_far = shift_up(gate_below)
    up_far = shift_down(up_above)
    half_units = down_own.shape[0] // 2
    top, low = down_own[:half_units], down_own[half_units:]
    top_below = shift_up(top)
    low_above = shift_down(low)
    low_below = shift_up(low)
    top_above = shift_down(top)

    part, reach, added, total = mixer_local(
        mix_in, forget_shift, mix_gain[None], w_query, w_forget, w_value, forget_room[None]
    )
    outgoing, slot_ids = dispatch(
        tp_rank.reshape(1), moe_in, expert_choice, moe_gain[None], added, total,
        quarter, experts, pieces,
    )
    arrived = lax.all_to_all(outgoing, EP, split_axis=0, concat_axis=0, tiled=True)
    hidden = norm_rows(moe_in, moe_gain)
    shared_gate = dot(hidden, w_sh_gate)
    shared_up = dot(hidden, w_sh_up)
    shared_act = (jax.nn.silu(shared_gate) * shared_up).astype(bf16)
    shared_part = dot(shared_act, w_sh_down).astype(bf16)
    arrived = after(arrived, shared_part)
    state_next = state_scan(arrived, pieces)
    top_far = shift_up(after(top_below, state_next))
    low_far = shift_down(after(low_above, state_next))
    state_start = lax.all_to_all(state_next, EP, split_axis=0, concat_axis=0, tiled=True)
    state_start = state_start.reshape(HEAD, -1)
    own, to_above, across_top, across_low, to_below = mixer_out(
        tp_rank.reshape(1), part, reach, state_start, head_gain[None], w_out, shared_part, tp_count
    )

    acts = hidden_units(
        arrived,
        [gate_own, gate_below, gate_above, gate_far],
        [up_own, up_below, up_above, up_far],
        pieces,
    )
    ready = results(
        acts,
        [top, low, top_below, low_below, top_above, low_above, top_far, low_far],
        experts,
    )
    returned = lax.all_to_all(ready, EP, split_axis=0, concat_axis=0, tiled=True)

    middle = across_top.shape[0]
    via_below = shift_up(across_top)
    via_above = shift_down(across_low)
    to_above = jnp.concatenate([to_above[:middle] + via_below, to_above[middle:]], axis=0)
    to_below = jnp.concatenate([to_below[:middle], to_below[middle:] + via_above], axis=0)
    from_below = shift_up(to_above)
    from_above = shift_down(to_below)
    total_rows = own.astype(f32) + from_below.astype(f32) + from_above.astype(f32)
    mixer_rows = mix_in.shape[0] // tp_count
    return (
        total_rows[:mixer_rows].astype(bf16),
        combine(returned, slot_ids, route_logit, total_rows[mixer_rows:]),
    )


def solution(mesh):
    finer = Mesh(mesh.devices.reshape(8, 4, 2, mesh.shape["tp"]), ("ep_0", "ep_1", "ep_2", "tp"))
    in_specs = (
        P(EP, None),
        P(EP),
        P(),
        P(None, "tp"),
        P(None, "tp"),
        P(None, "tp"),
        P("tp"),
        P("tp"),
        P("tp", None),
        P(EP, None),
        P(),
        P(EP, None),
        P(EP_TP, None),
        P(EP, None, "tp"),
        P(EP, None, "tp"),
        P(EP, "tp", None),
        P(None, "tp"),
        P(None, "tp"),
        P("tp", None),
    )
    out_specs = (P(EP_TP, None), P(EP_TP, None))

    return jax.shard_map(local, mesh=finer, in_specs=in_specs, out_specs=out_specs, check_vma=False)
```

time: 207 us -> 210 us (1.014)
  waiting for transfers between devices: 78.1 us -> 93.9 us
  local copies, waits for them, and re-layouts: 18.5 us -> 5.62 us
  matrix products: 7.21 us -> 3.68 us
    ppermute x8, waiting for transfers between devices: 16.4 us -> 55.6 us  [shift_down(): return lax.ppermute(x, 'tp', DOWN)]
    ppermute x8, waiting for transfers between devices: 57.4 us -> 34.6 us  [shift_up(): return lax.ppermute(x, 'tp', UP)]
    dot_general x4 -> x2, matrix products: 7.21 us -> 3.68 us  [dot(): lax.dot_general(a, b, (((ca,), (cb,)), ((), ())), preferred_element_type=...]
    reshape x2 -> x0, local copies, waits for them, and re-layouts: 3.36 us -> none  [the longest x1 2.55 us: local(): returned = returned.reshape(slots, model)]
    unnamed x30 -> x25, local copies, waits for them, and re-layouts: 6.79 us -> 3.46 us
    slice x3 -> x1, local copies, waits for them, and re-layouts: 2.87 us -> 0.04 us  [local(): total_rows[mixer_rows:]]
    pallas_call x3 -> x4, Pallas kernels: 24.9 us -> 26.6 us  [the longest x1 9.96 us: hidden_units(): pl.pallas_call(hidden_units_body, grid=(1,), in_specs=[pl.BlockSpec((peer...]
  transfers between devices with their start and end apart: 19 -> 19, of which waited for: 8 -> 7; matrix products, arithmetic and copies ran while one was open for 7% -> 5% of each run, Pallas kernels for 13% -> 11%
where the time goes in v3:
time: 210 us; the launch traced here: 209 us
  waiting for transfers between devices  93.9 us (45%)
  starting transfers between devices  58.2 us (28%)
  Pallas kernels  43.4 us (21%)
  local copies, waits for them, and re-layouts  5.62 us (3%)
  matrix products  3.68 us (2%)
  other arithmetic  3.46 us (2%)
    ppermute x8, waiting for transfers between devices, shift_down(): return lax.ppermute(x, 'tp', DOWN)  55.6 us
    ppermute x8, waiting for transfers between devices, shift_up(): return lax.ppermute(x, 'tp', UP)  34.6 us
    ppermute x8, starting transfers between devices, shift_down(): return lax.ppermute(x, 'tp', DOWN)  20.6 us
    pallas_call x1, Pallas kernels, mixer_local(): pl.pallas_call(mixer_local_body, in_specs=[pl.BlockSpec(memory_space=pltp...  12.2 us
    all_to_all x1, starting transfers between devices, local(): lax.all_to_all(outgoing, EP, split_axis=0, concat_axis=0, tiled=True)  12 us
    all_to_all x1, starting transfers between devices, local(): lax.all_to_all(ready, EP, split_axis=0, concat_axis=0, tiled=True)  10.4 us
    all_to_all x1, starting transfers between devices, local(): lax.all_to_all(state_next, EP, split_axis=0, concat_axis=0, tiled=True)  10.3 us
    pallas_call x1, Pallas kernels, hidden_units(): pl.pallas_call(hidden_units_body, grid=(1,), in_specs=[pl.BlockSpec((peer...  9.96 us
  transfers between devices with their start and end apart: 19, of which 7 were waited for; matrix products, arithmetic and copies ran while one was open for 5% of the time, Pallas kernels for 11%

profile of v3, /device:TPU:2, one launch (start us, length us, event | category | flops | bytes accessed | tf_op | source)
XLA Modules:
  0.0 209.1 jit_solution(10074230050741182318)
XLA Ops:
  0.6 0.0 copy-start
  0.6 1.5 copy.21.choice_ref
  2.2 12.2 %mixer_local.1 = (f32[512,256]{1,0:T(8,128)}, bf16[512,256]{1,0:T(8,128)(2,1)}, f32[64,256]{1,0:T(8,128)}, f32[1,256]{1,0:T(1,128)}) custom-call(f32[512]{0:T(512)} %shift_ref.1, bf16[512,2048]{1,0:T(8,128)(2,1)} %x_hbm.1, f32[1,2048]{1,0:T(1,128)} %bitcast.22, bf16[2048,256]{1,0:T(8,128)(2,1)} %wq_hbm.1, bf16[2048,256]{1,0:T(8,128)(2,1)} %wf_hbm.1, ...), custom_call_target="tpu_custom_call" | custom-call | flops 1610612736 | bytes 6291456 | tf_op jit(solution)/shard_map/mixer_local/pallas_call | solution.py:114
  14.4 3.5 %dispatch.1 = (bf16[64,104,128]{2,1,0:T(8,128)(2,1)}, s32[64,4]{1,0:T(8,128)}) custom-call(s32[1]{0:T(128)} %bitcast.rank_ref, bf16[256,2048]{1,0:T(8,128)(2,1)} %x_ref.1, s32[256,4]{1,0:T(8,128)} %copy.21.choice_ref, f32[1,2048]{1,0:T(1,128)} %bitcast.20, f32[64,256]{1,0:T(8,128)} %get-tuple-element.18.state_ref, f32[1,256]{1,0:T(1,128)} %get-tuple-element.19.total_ref), custom_call_target="tpu_custom_call" | custom-call | tf_op jit(solution)/shard_map/dispatch/pallas_call | solution.py:301
  17.9 12.0 %all-to-all-start = ((bf16[64,104,128]{2,1,0:T(8,128)(2,1)}), bf16[64,104,128]{2,1,0:T(8,128)(2,1)S(1)}, u32[]{:S(2)}, u32[]{:S(2)}) async-start(bf16[64,104,128]{2,1,0:T(8,128)(2,1)} %get-tuple-element.20), calls=%async_computation | async-start | bytes 3407872 | tf_op jit(solution)/shard_map/all_to_all | solution.py:562
  30.0 0.0 copy-start.5
  30.0 0.0 copy-start.8
  30.0 0.0 copy-start.10
  30.0 1.7 collective-permute-start.4
  31.7 1.7 collective-permute-start.8
  33.3 1.3 slice_bitcast_fusion
  34.6 0.4 collective-permute-start.10
  35.0 2.9 %collective-permute-start.5 = (bf16[2048,256]{1,0:T(8,128)(2,1)}, bf16[2048,256]{1,0:T(8,128)(2,1)}, u32[]{:S(2)}, u32[]{:S(2)}) collective-permute-start(bf16[2048,256]{1,0:T(8,128)(2,1)} %bitcast.5.refs_0_), channel_id=1, source_target_pairs={{0,3},{1,0},{2,1},{3,2},{4,7},{5,4},{6,5},{7,6},{8,11},{9,8},{10,9... | collective-permute-start | bytes 3145736 | tf_op jit(solution)/shard_map/ppermute | solution.py:504
  37.9 0.0 collective-permute-start.7
  37.9 19.7 %collective-permute-done.4.refs_1_ = bf16[2048,256]{1,0:T(8,128)(2,1)} collective-permute-done((bf16[2048,256]{1,0:T(8,128)(2,1)}, bf16[2048,256]{1,0:T(8,128)(2,1)}, u32[]{:S(2)}, u32[]{:S(2)}) %collective-permute-start.4) | collective-permute-done | bytes 1048608 | tf_op jit(solution)/shard_map/ppermute | solution.py:500
  57.6 0.4 collective-permute-start.6
  58.0 0.0 collective-permute-done.8.refs_6_
  58.0 2.9 %collective-permute-start.9 = (bf16[2048,256]{1,0:T(8,128)(2,1)}, bf16[2048,256]{1,0:T(8,128)(2,1)}, u32[]{:S(2)}, u32[]{:S(2)}) collective-permute-start(bf16[2048,256]{1,0:T(8,128)(2,1)} %collective-permute-done.8.refs_6_), channel_id=1, source_target_pairs={{0,3},{1,0},{2,1},{3,2},{4,7},{5,4},{6,5},{7,6},{8,11},{9,8},{10,9... | collective-permute-start | bytes 3145736 | tf_op jit(solution)/shard_map/ppermute | solution.py:504
  60.9 0.3 fusion
  61.2 7.7 %collective-permute-done.10.refs_2_ = bf16[128,2048]{1,0:T(8,128)(2,1)} collective-permute-done((bf16[128,2048]{1,0:T(8,128)(2,1)S(1)}, bf16[128,2048]{1,0:T(8,128)(2,1)}, u32[]{:S(2)}, u32[]{:S(2)}) %collective-permute-start.10) | collective-permute-done | bytes 524320 | tf_op jit(solution)/shard_map/ppermute | solution.py:500
  68.9 1.8 collective-permute-start.13
  70.7 0.0 copy-done.8
  70.7 0.5 fusion.6
  71.2 3.2 %convolution_convert_fusion.shared_hbm = bf16[256,2048]{1,0:T(8,128)(2,1)} fusion(bf16[128,2048]{1,0:T(8,128)(2,1)S(1)} %copy-done, bf16[2048,128]{1,0:T(8,128)(2,1)} %param.36, bf16[256,2048]{1,0:T(8,128)(2,1)} %x_ref.1, f32[2048]{0:T(1024)S(1)} %copy-done.8, f32[256]{0:T(256)S(1)} %add_rsqrt_fusion, f32[256,128]{1,0:T(8,128)S(1)} %fusion.6), kind=kOutput, calls=%fused_computation.2 | convolution fusion | flops 271253504 | bytes 3286016 | tf_op jit(solution)/shard_map/dot_general | solution.py:24
  74.4 0.0 all-to-all-done.got_ref
  74.4 1.1 state_scan.1
  75.5 37.6 %collective-permute-done.13.refs_5_ = bf16[128,2048]{1,0:T(8,128)(2,1)} collective-permute-done((bf16[128,2048]{1,0:T(8,128)(2,1)S(1)}, bf16[128,2048]{1,0:T(8,128)(2,1)}, u32[]{:S(2)}, u32[]{:S(2)}) %collective-permute-start.13) | collective-permute-done | bytes 524320 | tf_op jit(solution)/shard_map/ppermute | solution.py:504
  113.1 1.6 collective-permute-start.11
  114.6 0.0 collective-permute-done.5.refs_2_
  114.6 1.7 collective-permute-start.12
  116.3 0.0 collective-permute-done.7.refs_5_
  116.3 0.4 collective-permute-start.14
  116.7 0.0 collective-permute-done.6.refs_3_
  116.7 2.9 %collective-permute-start.15 = (bf16[128,2048]{1,0:T(8,128)(2,1)}, bf16[128,2048]{1,0:T(8,128)(2,1)}, u32[]{:S(2)}, u32[]{:S(2)}) collective-permute-start(bf16[128,2048]{1,0:T(8,128)(2,1)} %collective-permute-done.13.refs_5_), channel_id=1, source_target_pairs={{0,3},{1,0},{2,1},{3,2},{4,7},{5,4},{6,5},{7,6},{8,11},{9,8},{10,9... | collective-permute-start | bytes 1572872 | tf_op jit(solution)/shard_map/ppermute | solution.py:504
  119.5 10.3 %all-to-all-start.1 = ((bf16[64,2,128]{2,1,0:T(2,128)(2,1)}), bf16[64,2,128]{2,1,0:T(2,128)(2,1)S(1)}, u32[]{:S(2)}, u32[]{:S(2)}) async-start(bf16[64,2,128]{2,1,0:T(2,128)(2,1)} %state_scan.1), calls=%async_computation.1 | async-start | bytes 65536 | tf_op jit(solution)/shard_map/all_to_all | solution.py:572
  129.8 0.0 collective-permute-done.9.refs_7_
  129.9 10.0 %hidden_units.1.act_ref = bf16[384,1024]{1,0:T(8,128)(2,1)} custom-call(bf16[64,104,128]{2,1,0:T(8,128)(2,1)} %copy-done.1, bf16[2048,256]{1,0:T(8,128)(2,1)} %bitcast.5.refs_0_, bf16[2048,256]{1,0:T(8,128)(2,1)} %collective-permute-done.4.refs_1_, bf16[2048,256]{1,0:T(8,128)(2,1)} %collective-permute-done.5.refs_2_, ...), custom_call_target="tpu_custom_call" | custom-call | flops 3221225472 | bytes 10485760 | tf_op jit(solution)/shard_map/hidden_units/pallas_call | solution.py:374
  139.8 0.0 all-to-all-done.1
  139.8 0.6 copy.25
  140.5 6.4 %mixer_out.1 = (bf16[192,2048]{1,0:T(8,128)(2,1)}, bf16[192,2048]{1,0:T(8,128)(2,1)}, bf16[96,2048]{1,0:T(8,128)(2,1)}, bf16[96,2048]{1,0:T(8,128)(2,1)}, bf16[192,2048]{1,0:T(8,128)(2,1)}) custom-call(s32[1]{0:T(128)} %bitcast.rank_ref, f32[512,256]{1,0:T(8,128)} %get-tuple-element.16.part_hbm, bf16[512,256]{1,0:T(8,128)(2,1)} %get-tuple-element.17.reach_hbm, ...), custom_call_target="tpu_custom_call" | custom-call | flops 536870912 | bytes 6291456 | tf_op jit(solution)/shard_map/mixer_out/pallas_call | solution.py:210
  146.9 0.3 collective-permute-start
  147.2 0.0 collective-permute-done.11.refs_3_
  147.2 0.0 collective-permute-done.12.refs_4_
  147.2 0.0 collective-permute-done.14.refs_6_
  147.2 0.0 collective-permute-done.15.refs_7_
  147.2 6.3 %results.1 = bf16[64,96,128]{2,1,0:T(8,128)(2,1)S(1)} custom-call(bf16[384,1024]{1,0:T(8,128)(2,1)S(1)} %copy-done.3, bf16[128,2048]{1,0:T(8,128)(2,1)S(1)} %get-tuple-element.31.refs_0_, bf16[128,2048]{1,0:T(8,128)(2,1)S(1)} %get-tuple-element.30.refs_1_, bf16[128,2048]{1,0:T(8,128)(2,1)} %collective-permute-done.10.refs_2_, ...), custom_call_target="tpu_custom_call" | custom-call | flops 1610612736 | bytes 6291456 | tf_op jit(solution)/shard_map/results/pallas_call | solution.py:436
  153.6 1.2 copy-done.2
  154.8 10.4 %all-to-all-start.2 = ((bf16[64,96,128]{2,1,0:T(8,128)(2,1)}), bf16[64,96,128]{2,1,0:T(8,128)(2,1)S(1)}, u32[]{:S(2)}, u32[]{:S(2)}) async-start(bf16[64,96,128]{2,1,0:T(8,128)(2,1)} %copy-done.2), calls=%async_computation.2 | async-start | bytes 3145728 | tf_op jit(solution)/shard_map/all_to_all | solution.py:589
  165.2 3.3 %collective-permute-start.2 = (bf16[96,2048]{1,0:T(8,128)(2,1)}, bf16[96,2048]{1,0:T(8,128)(2,1)S(1)}, u32[]{:S(2)}, u32[]{:S(2)}) collective-permute-start(bf16[96,2048]{1,0:T(8,128)(2,1)} %get-tuple-element.26), channel_id=1, source_target_pairs={{0,3},{1,0},{2,1},{3,2},{4,7},{5,4},{6,5},{7,6},{8,11},{9,8},{10,9... | collective-permute-start | bytes 1179656 | tf_op jit(solution)/shard_map/ppermute | solution.py:504
  168.5 0.0 collective-permute-done
  168.5 0.1 slice_add_fusion.1
  168.6 0.1 pad_maximum_fusion
  168.6 0.1 collective-permute-start.1
  168.7 8.7 %collective-permute-done.2 = bf16[96,2048]{1,0:T(8,128)(2,1)S(1)} collective-permute-done((bf16[96,2048]{1,0:T(8,128)(2,1)}, bf16[96,2048]{1,0:T(8,128)(2,1)S(1)}, u32[]{:S(2)}, u32[]{:S(2)}) %collective-permute-start.2) | collective-permute-done | bytes 393248 | tf_op jit(solution)/shard_map/ppermute | solution.py:504
  177.5 0.1 fusion.15
  177.5 1.0 pad_maximum_fusion.1
  178.5 3.6 %collective-permute-start.3 = (bf16[192,2048]{1,0:T(8,128)(2,1)}, bf16[192,2048]{1,0:T(8,128)(2,1)}, u32[]{:S(2)}, u32[]{:S(2)}) collective-permute-start(bf16[192,2048]{1,0:T(8,128)(2,1)} %pad_maximum_fusion.1), channel_id=1, source_target_pairs={{0,3},{1,0},{2,1},{3,2},{4,7},{5,4},{6,5},{7,6},{8,11},{9,8},{10,9... | collective-permute-start | bytes 2359304 | tf_op jit(solution)/shard_map/ppermute | solution.py:504
  182.1 0.1 copy.22.logit_ref
  182.2 7.1 %collective-permute-done.1 = bf16[192,2048]{1,0:T(8,128)(2,1)} collective-permute-done((bf16[192,2048]{1,0:T(8,128)(2,1)S(1)}, bf16[192,2048]{1,0:T(8,128)(2,1)}, u32[]{:S(2)}, u32[]{:S(2)}) %collective-permute-start.1) | collective-permute-done | bytes 786464 | tf_op jit(solution)/shard_map/ppermute | solution.py:500
  189.3 9.3 %collective-permute-done.3 = bf16[192,2048]{1,0:T(8,128)(2,1)} collective-permute-done((bf16[192,2048]{1,0:T(8,128)(2,1)}, bf16[192,2048]{1,0:T(8,128)(2,1)}, u32[]{:S(2)}, u32[]{:S(2)}) %collective-permute-start.3) | collective-permute-done | bytes 786464 | tf_op jit(solution)/shard_map/ppermute | solution.py:504
  198.6 2.0 convert_add_fusion
  200.7 0.9 slice.48
  201.6 3.7 %all-to-all-done.2.got_ref = bf16[64,96,128]{2,1,0:T(8,128)(2,1)S(1)} async-done(((bf16[64,96,128]{2,1,0:T(8,128)(2,1)}), bf16[64,96,128]{2,1,0:T(8,128)(2,1)S(1)}, u32[]{:S(2)}, u32[]{:S(2)}) %all-to-all-start.2) | async-done | bytes 1572896 | tf_op jit(solution)/shard_map/all_to_all | solution.py:589
  205.2 3.9 %combine.1 = bf16[64,2048]{1,0:T(8,128)(2,1)} custom-call(bf16[64,96,128]{2,1,0:T(8,128)(2,1)S(1)} %all-to-all-done.2.got_ref, s32[64,4]{1,0:T(8,128)S(1)} %copy-done.4, f32[64,4]{1,0:T(8,128)S(1)} %copy.22.logit_ref, f32[64,2048]{1,0:T(8,128)S(1)} %slice.42.rest_ref), custom_call_target="tpu_custom_call" | custom-call | tf_op jit(solution)/shard_map/combine/pallas_call | solution.py:486
  (18 shorter events, 0.1 us)
Async XLA Ops:
  0.6 70.6 %copy-start = (bf16[128,2048]{1,0:T(8,128)(2,1)S(1)}, bf16[128,2048]{1,0:T(8,128)(2,1)}, u32[]{:S(2)}) copy-start(bf16[128,2048]{1,0:T(8,128)(2,1)} %param.37) | copy-start | bytes 1572868
  17.9 56.4 %all-to-all-start = ((bf16[64,104,128]{2,1,0:T(8,128)(2,1)}), bf16[64,104,128]{2,1,0:T(8,128)(2,1)S(1)}, u32[]{:S(2)}, u32[]{:S(2)}) async-start(bf16[64,104,128]{2,1,0:T(8,128)(2,1)} %get-tuple-element.20), calls=%async_computation | async-start | bytes 3407872 | tf_op jit(solution)/shard_map/all_to_all | solution.py:562
  30.0 30.9 %copy-start.5 = (bf16[256,2048]{1,0:T(8,128)(2,1)S(1)}, bf16[256,2048]{1,0:T(8,128)(2,1)}, u32[]{:S(2)}) copy-start(bf16[256,2048]{1,0:T(8,128)(2,1)} %x_ref.1) | copy-start | bytes 3145732
  30.0 40.7 %copy-start.8 = (f32[2048]{0:T(1024)S(1)}, f32[2048]{0:T(1024)}, u32[]{:S(2)}) copy-start(f32[2048]{0:T(1024)} %param.29) | copy-start | bytes 24580
  30.0 40.7 %copy-start.10 = (bf16[2048,128]{1,0:T(8,128)(2,1)S(1)}, bf16[2048,128]{1,0:T(8,128)(2,1)}, u32[]{:S(2)}) copy-start(bf16[2048,128]{1,0:T(8,128)(2,1)} %param.35) | copy-start | bytes 1572868
  30.0 27.6 %collective-permute-start.4 = (bf16[2048,256]{1,0:T(8,128)(2,1)}, bf16[2048,256]{1,0:T(8,128)(2,1)}, u32[]{:S(2)}, u32[]{:S(2)}) collective-permute-start(bf16[2048,256]{1,0:T(8,128)(2,1)} %bitcast.5.refs_0_), channel_id=1, source_target_pairs={{0,1},{1,2},{2,3},{3,0},{4,5},{5,6},{6,7},{7,4},{8,9},{9,10},{10,1... | collective-permute-start | bytes 3145736 | tf_op jit(solution)/shard_map/ppermute | solution.py:500
  31.7 26.3 %collective-permute-start.8 = (bf16[2048,256]{1,0:T(8,128)(2,1)}, bf16[2048,256]{1,0:T(8,128)(2,1)}, u32[]{:S(2)}, u32[]{:S(2)}) collective-permute-start(bf16[2048,256]{1,0:T(8,128)(2,1)} %bitcast.6.refs_4_), channel_id=1, source_target_pairs={{0,3},{1,0},{2,1},{3,2},{4,7},{5,4},{6,5},{7,6},{8,11},{9,8},{10,9... | collective-permute-start | bytes 3145736 | tf_op jit(solution)/shard_map/ppermute | solution.py:504
  34.6 34.3 %collective-permute-start.10 = (bf16[128,2048]{1,0:T(8,128)(2,1)S(1)}, bf16[128,2048]{1,0:T(8,128)(2,1)}, u32[]{:S(2)}, u32[]{:S(2)}) collective-permute-start(bf16[128,2048]{1,0:T(8,128)(2,1)S(1)} %get-tuple-element.31.refs_0_), channel_id=1, source_target_pairs={{0,1},{1,2},{2,3},{3,0},{4,5},{5,6},{6,7},{7,4},{8,9},{9,10},{10,1... | collective-permute-start | bytes 1572872 | tf_op jit(solution)/shard_map/ppermute | solution.py:500
  35.0 79.6 %collective-permute-start.5 = (bf16[2048,256]{1,0:T(8,128)(2,1)}, bf16[2048,256]{1,0:T(8,128)(2,1)}, u32[]{:S(2)}, u32[]{:S(2)}) collective-permute-start(bf16[2048,256]{1,0:T(8,128)(2,1)} %bitcast.5.refs_0_), channel_id=1, source_target_pairs={{0,3},{1,0},{2,1},{3,2},{4,7},{5,4},{6,5},{7,6},{8,11},{9,8},{10,9... | collective-permute-start | bytes 3145736 | tf_op jit(solution)/shard_map/ppermute | solution.py:504
  37.9 78.4 %collective-permute-start.7 = (bf16[2048,256]{1,0:T(8,128)(2,1)}, bf16[2048,256]{1,0:T(8,128)(2,1)}, u32[]{:S(2)}, u32[]{:S(2)}) collective-permute-start(bf16[2048,256]{1,0:T(8,128)(2,1)} %bitcast.6.refs_4_), channel_id=1, source_target_pairs={{0,1},{1,2},{2,3},{3,0},{4,5},{5,6},{6,7},{7,4},{8,9},{9,10},{10,1... | collective-permute-start | bytes 3145736 | tf_op jit(solution)/shard_map/ppermute | solution.py:500
  57.6 59.0 %collective-permute-start.6 = (bf16[2048,256]{1,0:T(8,128)(2,1)}, bf16[2048,256]{1,0:T(8,128)(2,1)}, u32[]{:S(2)}, u32[]{:S(2)}) collective-permute-start(bf16[2048,256]{1,0:T(8,128)(2,1)} %collective-permute-done.4.refs_1_), channel_id=1, source_target_pairs={{0,1},{1,2},{2,3},{3,0},{4,5},{5,6},{6,7},{7,4},{8,9},{9,10},{10,1... | collective-permute-start | bytes 3145736 | tf_op jit(solution)/shard_map/ppermute | solution.py:500
  58.0 71.8 %collective-permute-start.9 = (bf16[2048,256]{1,0:T(8,128)(2,1)}, bf16[2048,256]{1,0:T(8,128)(2,1)}, u32[]{:S(2)}, u32[]{:S(2)}) collective-permute-start(bf16[2048,256]{1,0:T(8,128)(2,1)} %collective-permute-done.8.refs_6_), channel_id=1, source_target_pairs={{0,3},{1,0},{2,1},{3,2},{4,7},{5,4},{6,5},{7,6},{8,11},{9,8},{10,9... | collective-permute-start | bytes 3145736 | tf_op jit(solution)/shard_map/ppermute | solution.py:504
  68.9 44.2 %collective-permute-start.13 = (bf16[128,2048]{1,0:T(8,128)(2,1)S(1)}, bf16[128,2048]{1,0:T(8,128)(2,1)}, u32[]{:S(2)}, u32[]{:S(2)}) collective-permute-start(bf16[128,2048]{1,0:T(8,128)(2,1)S(1)} %get-tuple-element.30.refs_1_), channel_id=1, source_target_pairs={{0,3},{1,0},{2,1},{3,2},{4,7},{5,4},{6,5},{7,6},{8,11},{9,8},{10,9... | collective-permute-start | bytes 1572872 | tf_op jit(solution)/shard_map/ppermute | solution.py:504
  74.4 55.5 %copy-start.1 = (bf16[64,104,128]{2,1,0:T(8,128)(2,1)}, bf16[64,104,128]{2,1,0:T(8,128)(2,1)S(1)}, u32[]{:S(2)}) copy-start(bf16[64,104,128]{2,1,0:T(8,128)(2,1)S(1)} %all-to-all-done.got_ref) | copy-start | bytes 5111812
  113.1 34.1 %collective-permute-start.11 = (bf16[128,2048]{1,0:T(8,128)(2,1)S(1)}, bf16[128,2048]{1,0:T(8,128)(2,1)}, u32[]{:S(2)}, u32[]{:S(2)}) collective-permute-start(bf16[128,2048]{1,0:T(8,128)(2,1)S(1)} %get-tuple-element.30.refs_1_), channel_id=1, source_target_pairs={{0,1},{1,2},{2,3},{3,0},{4,5},{5,6},{6,7},{7,4},{8,9},{9,10},{10,1... | collective-permute-start | bytes 1572872 | tf_op jit(solution)/shard_map/ppermute | solution.py:500
  114.6 32.6 %collective-permute-start.12 = (bf16[128,2048]{1,0:T(8,128)(2,1)S(1)}, bf16[128,2048]{1,0:T(8,128)(2,1)}, u32[]{:S(2)}, u32[]{:S(2)}) collective-permute-start(bf16[128,2048]{1,0:T(8,128)(2,1)S(1)} %get-tuple-element.31.refs_0_), channel_id=1, source_target_pairs={{0,3},{1,0},{2,1},{3,2},{4,7},{5,4},{6,5},{7,6},{8,11},{9,8},{10,9... | collective-permute-start | bytes 1572872 | tf_op jit(solution)/shard_map/ppermute | solution.py:504
  116.3 30.9 %collective-permute-start.14 = (bf16[128,2048]{1,0:T(8,128)(2,1)}, bf16[128,2048]{1,0:T(8,128)(2,1)}, u32[]{:S(2)}, u32[]{:S(2)}) collective-permute-start(bf16[128,2048]{1,0:T(8,128)(2,1)} %collective-permute-done.10.refs_2_), channel_id=1, source_target_pairs={{0,1},{1,2},{2,3},{3,0},{4,5},{5,6},{6,7},{7,4},{8,9},{9,10},{10,1... | collective-permute-start | bytes 1572872 | tf_op jit(solution)/shard_map/ppermute | solution.py:500
  116.7 30.6 %collective-permute-start.15 = (bf16[128,2048]{1,0:T(8,128)(2,1)}, bf16[128,2048]{1,0:T(8,128)(2,1)}, u32[]{:S(2)}, u32[]{:S(2)}) collective-permute-start(bf16[128,2048]{1,0:T(8,128)(2,1)} %collective-permute-done.13.refs_5_), channel_id=1, source_target_pairs={{0,3},{1,0},{2,1},{3,2},{4,7},{5,4},{6,5},{7,6},{8,11},{9,8},{10,9... | collective-permute-start | bytes 1572872 | tf_op jit(solution)/shard_map/ppermute | solution.py:504
  119.5 20.3 %all-to-all-start.1 = ((bf16[64,2,128]{2,1,0:T(2,128)(2,1)}), bf16[64,2,128]{2,1,0:T(2,128)(2,1)S(1)}, u32[]{:S(2)}, u32[]{:S(2)}) async-start(bf16[64,2,128]{2,1,0:T(2,128)(2,1)} %state_scan.1), calls=%async_computation.1 | async-start | bytes 65536 | tf_op jit(solution)/shard_map/all_to_all | solution.py:572
  139.8 7.4 %copy-start.3 = (bf16[384,1024]{1,0:T(8,128)(2,1)S(1)}, bf16[384,1024]{1,0:T(8,128)(2,1)}, u32[]{:S(2)}) copy-start(bf16[384,1024]{1,0:T(8,128)(2,1)} %hidden_units.1.act_ref) | copy-start | bytes 2359300
  146.9 21.6 %collective-permute-start = (bf16[96,2048]{1,0:T(8,128)(2,1)}, bf16[96,2048]{1,0:T(8,128)(2,1)S(1)}, u32[]{:S(2)}, u32[]{:S(2)}) collective-permute-start(bf16[96,2048]{1,0:T(8,128)(2,1)} %get-tuple-element.24), channel_id=1, source_target_pairs={{0,1},{1,2},{2,3},{3,0},{4,5},{5,6},{6,7},{7,4},{8,9},{9,10},{10,1... | collective-permute-start | bytes 1179656 | tf_op jit(solution)/shard_map/ppermute | solution.py:500
  153.6 1.2 copy-start.2
  154.8 13.7 %copy-start.7 = (bf16[192,2048]{1,0:T(8,128)(2,1)S(1)}, bf16[192,2048]{1,0:T(8,128)(2,1)}, u32[]{:S(2)}) copy-start(bf16[192,2048]{1,0:T(8,128)(2,1)} %get-tuple-element.23) | copy-start | bytes 2359300
  154.8 50.4 %all-to-all-start.2 = ((bf16[64,96,128]{2,1,0:T(8,128)(2,1)}), bf16[64,96,128]{2,1,0:T(8,128)(2,1)S(1)}, u32[]{:S(2)}, u32[]{:S(2)}) async-start(bf16[64,96,128]{2,1,0:T(8,128)(2,1)} %copy-done.2), calls=%async_computation.2 | async-start | bytes 3145728 | tf_op jit(solution)/shard_map/all_to_all | solution.py:589
  165.2 12.3 %collective-permute-start.2 = (bf16[96,2048]{1,0:T(8,128)(2,1)}, bf16[96,2048]{1,0:T(8,128)(2,1)S(1)}, u32[]{:S(2)}, u32[]{:S(2)}) collective-permute-start(bf16[96,2048]{1,0:T(8,128)(2,1)} %get-tuple-element.26), channel_id=1, source_target_pairs={{0,3},{1,0},{2,1},{3,2},{4,7},{5,4},{6,5},{7,6},{8,11},{9,8},{10,9... | collective-permute-start | bytes 1179656 | tf_op jit(solution)/shard_map/ppermute | solution.py:504
  168.5 9.0 %copy-start.6 = (bf16[192,2048]{1,0:T(8,128)(2,1)S(1)}, bf16[192,2048]{1,0:T(8,128)(2,1)}, u32[]{:S(2)}) copy-start(bf16[192,2048]{1,0:T(8,128)(2,1)} %get-tuple-element.25) | copy-start | bytes 2359300
  168.6 20.7 %collective-permute-start.1 = (bf16[192,2048]{1,0:T(8,128)(2,1)S(1)}, bf16[192,2048]{1,0:T(8,128)(2,1)}, u32[]{:S(2)}, u32[]{:S(2)}) collective-permute-start(bf16[192,2048]{1,0:T(8,128)(2,1)S(1)} %pad_maximum_fusion), channel_id=1, source_target_pairs={{0,1},{1,2},{2,3},{3,0},{4,5},{5,6},{6,7},{7,4},{8,9},{9,10},{10,1... | collective-permute-start | bytes 2359304 | tf_op jit(solution)/shard_map/ppermute | solution.py:500
  177.5 4.6 %copy-start.9 = (f32[64,4]{0,1:T(4,128)S(1)}, f32[64,4]{0,1:T(4,128)}, u32[]{:S(2)}) copy-start(f32[64,4]{0,1:T(4,128)} %param.31) | copy-start | bytes 3076
  178.5 20.1 %collective-permute-start.3 = (bf16[192,2048]{1,0:T(8,128)(2,1)}, bf16[192,2048]{1,0:T(8,128)(2,1)}, u32[]{:S(2)}, u32[]{:S(2)}) collective-permute-start(bf16[192,2048]{1,0:T(8,128)(2,1)} %pad_maximum_fusion.1), channel_id=1, source_target_pairs={{0,3},{1,0},{2,1},{3,2},{4,7},{5,4},{6,5},{7,6},{8,11},{9,8},{10,9... | collective-permute-start | bytes 2359304 | tf_op jit(solution)/shard_map/ppermute | solution.py:504
  200.6 4.6 %copy-start.4 = (s32[64,4]{1,0:T(8,128)S(1)}, s32[64,4]{1,0:T(8,128)}, u32[]{:S(2)}) copy-start(s32[64,4]{1,0:T(8,128)} %get-tuple-element.29.slot_ref) | copy-start | bytes 3076

commit v4 on v3

--- a/solution.py
+++ b/solution.py
@@ -37,14 +37,10 @@
 
 
 def mixer_local_body(
-    shift_ref, x_hbm, gain_ref, wq_hbm, wf_hbm, wv_hbm, room_ref,
+    shift_ref, x_ref, gain_ref, wq_ref, wf_ref, wv_ref, room_ref,
     part_ref, reach_ref, state_ref, total_ref,
-    x_ref, wq_ref, wf_ref, wv_ref, normed_ref, q_ref, f_ref, v_ref, carry_ref, sems,
+    normed_ref, q_ref, f_ref, v_ref, carry_ref,
 ):
-    pairs = ((x_hbm, x_ref), (wf_hbm, wf_ref), (wq_hbm, wq_ref), (wv_hbm, wv_ref))
-    copies = [pltpu.make_async_copy(a, b, sems.at[i]) for i, (a, b) in enumerate(pairs)]
-    for copy in copies:
-        copy.start()
     rows, width = q_ref.shape
     blocks = rows // SPAN
     heads = width // HEAD
@@ -55,14 +51,10 @@
         normed_ref[at, :] = norm_rows(x_ref[at, :], gain)
         return carry
 
-    copies[0].wait()
     lax.fori_loop(0, blocks, norm_block, 0)
     normed = normed_ref[...]
-    copies[1].wait()
     f_ref[...] = dot(normed, wf_ref[...])
-    copies[2].wait()
     q_ref[...] = dot(normed, wq_ref[...])
-    copies[3].wait()
     v_ref[...] = dot(normed, wv_ref[...])
     room = room_ref[...]
     diagonal = same_head(width, width).astype(f32)
@@ -113,7 +105,12 @@
     hbm = pl.BlockSpec(memory_space=pltpu.HBM)
     return pl.pallas_call(
         mixer_local_body,
-        in_specs=[pl.BlockSpec(memory_space=pltpu.SMEM), hbm, vmem, hbm, hbm, hbm, vmem],
+        grid=(1,),
+        in_specs=[pl.BlockSpec(memory_space=pltpu.SMEM)]
+        + [
+            pl.BlockSpec(x.shape, lambda i: (0, 0))
+            for x in (mix_in, gain, w_query, w_forget, w_value, room)
+        ],
         out_specs=[vmem] * 4,
         out_shape=[
             jax.ShapeDtypeStruct((rows, width), f32),
@@ -122,10 +119,8 @@
             jax.ShapeDtypeStruct((1, width), f32),
         ],
         scratch_shapes=[pltpu.VMEM(mix_in.shape, bf16)]
-        + [pltpu.VMEM(w_query.shape, bf16)] * 3
-        + [pltpu.VMEM(mix_in.shape, bf16)]
         + [pltpu.VMEM((rows, width), f32)] * 3
-        + [pltpu.VMEM((width, width), f32), pltpu.SemaphoreType.DMA((4,))],
+        + [pltpu.VMEM((width, width), f32)],
         compiler_params=pltpu.CompilerParams(vmem_limit_bytes=60 << 20),
         cost_estimate=pl.CostEstimate(
             flops=rows * mix_in.shape[1] * width * 6, bytes_accessed=6 << 20, transcendentals=0
@@ -390,78 +385,62 @@
 
 
 def results_body(act_ref, *refs):
-    halves = refs[:-6]
-    out_hbm, weight_ref, rows_ref, tiles_ref, sems, out_sems = refs[-6:]
+    halves = refs[:-4]
+    out_hbm, rows_ref, tiles_ref, sems = refs[-4:]
     peers, pieces, _ = tiles_ref.shape
     slots = act_ref.shape[0]
-    half, model = halves[0].shape
+    model = halves[0].shape[1]
     capacity = slots // peers
     per_row = model // 128
-    parts = sems.shape[0]
-    part = model // parts
-    loads = [
-        [
-            pltpu.make_async_copy(
-                ref.at[:, pl.ds(i * part, part)],
-                weight_ref.at[i, pl.ds(j * half, half)],
-                sems.at[i, j],
-            )
-            for j, ref in enumerate(halves)
-        ]
-        for i in range(parts)
-    ]
-    for group in loads:
-        for load in group:
-            load.start()
-    for i in range(parts):
-        for load in loads[i]:
-            load.wait()
-        whole = dot(act_ref[...], weight_ref[i])
+    part = 256
+    act = act_ref[...]
+    for col in range(0, model, part):
+        weight = jnp.concatenate([ref[:, col : col + part] for ref in halves], axis=0)
+        whole = dot(act, weight)
         for c in range(capacity):
             for j in range(part // 128):
-                k = (i * part) // 128 + j
+                k = col // 128 + j
                 rows_ref[pl.ds(c * per_row + k, peers, stride=pieces), :] = whole[
                     c * peers : (c + 1) * peers, j * 128 : (j + 1) * 128
                 ]
-    for copy in narrow_out(rows_ref, tiles_ref, out_hbm, out_sems):
+    for copy in narrow_out(rows_ref, tiles_ref, out_hbm, sems):
         copy.wait()
 
 
-def results(acts, halves, peers):
+def results(acts, weights, peers):
     slots, width = acts.shape
-    _, model = halves[0].shape
+    model = weights[0].shape[1]
     pieces = slots // peers * model // 128
-    hbm = pl.BlockSpec(memory_space=pltpu.HBM)
-    parts = 4
+    whole = lambda i: (0, 0)
     return pl.pallas_call(
         results_body,
-        in_specs=[pl.BlockSpec(memory_space=pltpu.VMEM)] + [hbm] * len(halves),
-        out_specs=hbm,
+        grid=(1,),
+        in_specs=[pl.BlockSpec((slots, width), whole)]
+        + [pl.BlockSpec(w.shape, whole) for w in weights],
+        out_specs=pl.BlockSpec(memory_space=pltpu.HBM),
         out_shape=jax.ShapeDtypeStruct((peers, pieces, 128), bf16),
         scratch_shapes=[
-            pltpu.VMEM((parts, width, model // parts), bf16),
             pltpu.VMEM((peers * pieces, 128), f32),
             pltpu.VMEM((peers, pieces, 128), bf16),
-            pltpu.SemaphoreType.DMA((parts, len(halves))),
             pltpu.SemaphoreType.DMA((4,)),
         ],
-        compiler_params=pltpu.CompilerParams(vmem_limit_bytes=20 << 20),
+        compiler_params=pltpu.CompilerParams(vmem_limit_bytes=60 << 20),
         cost_estimate=pl.CostEstimate(
             flops=slots * model * width * 2, bytes_accessed=6 << 20, transcendentals=0
         ),
         name="results",
-    )(acts, *halves)
-
-
-def combine_body(got_ref, slot_ref, logit_ref, rest_ref, out_ref, rows_ref, x_ref, split_ref):
+    )(acts, *weights)
+
+
+def combine_body(got_ref, slot_ref, logit_ref, rest_ref, out_ref, rows_ref, split_ref):
     peers = got_ref.shape[0]
-    slots = x_ref.shape[0]
+    tokens, model = out_ref.shape
+    slots = split_ref.shape[2]
     capacity = slots // peers
+    per_row = model // 128
     widen_rows(got_ref, rows_ref, 0, peers)
-    gather_rows(rows_ref, x_ref, peers)
     chance = jax.nn.sigmoid(logit_ref[...])
     weights = chance / jnp.sum(chance, axis=-1, keepdims=True) * route_scale
-    tokens = weights.shape[0]
     first = lax.broadcasted_iota(jnp.int32, (tokens, peers), 1) * capacity
     picks = []
     for c in range(capacity):
@@ -474,9 +453,24 @@
     pick = jnp.concatenate(picks, axis=1)
     split_ref[0] = pick.astype(bf16)
     split_ref[1] = (pick - split_ref[0].astype(f32)).astype(bf16)
-    x = x_ref[...]
-    routed = dot(split_ref[0], x) + dot(split_ref[1], x)
-    out_ref[...] = (routed + rest_ref[...]).astype(bf16)
+    both = jnp.concatenate([split_ref[0], split_ref[1]], axis=0)
+    for k in range(0, per_row, 2):
+        x = jnp.concatenate(
+            [
+                jnp.concatenate(
+                    [
+                        rows_ref[pl.ds(c * per_row + k + j, peers, stride=capacity * per_row), :]
+                        for j in range(2)
+                    ],
+                    axis=1,
+                )
+                for c in range(capacity)
+            ],
+            axis=0,
+        ).astype(bf16)
+        sums = dot(both, x)
+        cols = slice(k * 128, (k + 2) * 128)
+        out_ref[:, cols] = (sums[:tokens] + sums[tokens:] + rest_ref[:, cols]).astype(bf16)
 
 
 def combine(returned, slot_ids, route_logit, rest):
@@ -488,7 +482,6 @@
         out_shape=jax.ShapeDtypeStruct((tokens, model), bf16),
         scratch_shapes=[
             pltpu.VMEM((peers * pieces, 128), f32),
-            pltpu.VMEM((slots, model), bf16),
             pltpu.VMEM((2, tokens, slots), bf16),
         ],
         compiler_params=pltpu.CompilerParams(vmem_limit_bytes=16 << 20),
@@ -583,7 +576,7 @@
     )
     ready = results(
         acts,
-        [top, low, top_below, low_below, top_above, low_above, top_far, low_far],
+        [down_own, top_below, low_below, top_above, low_above, top_far, low_far],
         experts,
     )
     returned = lax.all_to_all(ready, EP, split_axis=0, concat_axis=0, tiled=True)

time: 210 us -> 208 us (level)
    ppermute x8, waiting for transfers between devices: 55.6 us -> 53.2 us  [shift_down(): return lax.ppermute(x, 'tp', DOWN)]
  transfers between devices with their start and end apart: 19 -> 19, of which waited for: 7 -> 7; matrix products, arithmetic and copies ran while one was open for 5% -> 5% of each run, Pallas kernels for 11% -> 12%
where the time goes in v4:
time: 208 us
  waiting for transfers between devices  93.3 us (45%)
  starting transfers between devices  58.4 us (28%)
  Pallas kernels  42 us (20%)
  local copies, waits for them, and re-layouts  5.17 us (2%)
  other arithmetic  4.52 us (2%)
  matrix products  3.38 us (2%)
    ppermute x8, waiting for transfers between devices, shift_down(): return lax.ppermute(x, 'tp', DOWN)  53.2 us
    ppermute x8, waiting for transfers between devices, shift_up(): return lax.ppermute(x, 'tp', UP)  36.2 us
    ppermute x8, starting transfers between devices, shift_down(): return lax.ppermute(x, 'tp', DOWN)  20.7 us
    all_to_all x1, starting transfers between devices, local(): lax.all_to_all(outgoing, EP, split_axis=0, concat_axis=0, tiled=True)  12.2 us
    pallas_call x1, Pallas kernels, mixer_local(): pl.pallas_call(mixer_local_body, grid=(1,), in_specs=[pl.BlockSpec(memory...  10.8 us
    all_to_all x1, starting transfers between devices, local(): lax.all_to_all(ready, EP, split_axis=0, concat_axis=0, tiled=True)  10.4 us
    all_to_all x1, starting transfers between devices, local(): lax.all_to_all(state_next, EP, split_axis=0, concat_axis=0, tiled=True)  10.3 us
    pallas_call x1, Pallas kernels, hidden_units(): pl.pallas_call(hidden_units_body, grid=(1,), in_specs=[pl.BlockSpec((peer...  9.98 us
  transfers between devices with their start and end apart: 19, of which 7 were waited for; matrix products, arithmetic and copies ran while one was open for 5% of the time, Pallas kernels for 12%

profile of v4, /device:TPU:2, one launch (start us, length us, event | category | flops | bytes accessed | tf_op | source)
XLA Modules:
  0.0 207.6 jit_solution(8858215190224850420)
XLA Ops:
  0.6 0.0 copy-start
  0.6 1.5 copy.21.choice_ref
  2.2 10.8 %mixer_local.1 = (f32[512,256]{1,0:T(8,128)}, bf16[512,256]{1,0:T(8,128)(2,1)}, f32[64,256]{1,0:T(8,128)}, f32[1,256]{1,0:T(1,128)}) custom-call(f32[512]{0:T(512)} %shift_ref.1, bf16[512,2048]{1,0:T(8,128)(2,1)} %x_ref.2, f32[1,2048]{1,0:T(1,128)} %bitcast.30, bf16[2048,256]{1,0:T(8,128)(2,1)} %wq_ref.1, bf16[2048,256]{1,0:T(8,128)(2,1)} %wf_ref.1, ...), custom_call_target="tpu_custom_call" | custom-call | flops 1610612736 | bytes 6291456 | tf_op jit(solution)/shard_map/mixer_local/pallas_call | solution.py:106
  13.0 3.5 %dispatch.1 = (bf16[64,104,128]{2,1,0:T(8,128)(2,1)}, s32[64,4]{1,0:T(8,128)}) custom-call(s32[1]{0:T(128)} %bitcast.rank_ref, bf16[256,2048]{1,0:T(8,128)(2,1)} %x_ref.3, s32[256,4]{1,0:T(8,128)} %copy.21.choice_ref, f32[1,2048]{1,0:T(1,128)} %bitcast.22, f32[64,256]{1,0:T(8,128)} %get-tuple-element.18.state_ref, f32[1,256]{1,0:T(1,128)} %get-tuple-element.19.total_ref), custom_call_target="tpu_custom_call" | custom-call | tf_op jit(solution)/shard_map/dispatch/pallas_call | solution.py:296
  16.6 0.0 copy-start.3
  16.6 12.2 %all-to-all-start = ((bf16[64,104,128]{2,1,0:T(8,128)(2,1)}), bf16[64,104,128]{2,1,0:T(8,128)(2,1)S(1)}, u32[]{:S(2)}, u32[]{:S(2)}) async-start(bf16[64,104,128]{2,1,0:T(8,128)(2,1)} %get-tuple-element.20), calls=%async_computation | async-start | bytes 3407872 | tf_op jit(solution)/shard_map/all_to_all | solution.py:555
  28.7 0.0 copy-start.4
  28.8 0.0 copy-start.10
  28.8 0.0 copy-start.12
  28.8 1.7 collective-permute-start.4
  30.5 1.6 collective-permute-start.8
  32.1 1.0 slice_bitcast_fusion
  33.1 0.4 collective-permute-start.10
  33.5 2.9 %collective-permute-start.5 = (bf16[2048,256]{1,0:T(8,128)(2,1)}, bf16[2048,256]{1,0:T(8,128)(2,1)}, u32[]{:S(2)}, u32[]{:S(2)}) collective-permute-start(bf16[2048,256]{1,0:T(8,128)(2,1)} %bitcast.25), channel_id=1, source_target_pairs={{0,3},{1,0},{2,1},{3,2},{4,7},{5,4},{6,5},{7,6},{8,11},{9,8},{10,9... | collective-permute-start | bytes 3145736 | tf_op jit(solution)/shard_map/ppermute | solution.py:497
  36.4 0.0 collective-permute-start.7
  36.4 20.0 %collective-permute-done.4.refs_1_ = bf16[2048,256]{1,0:T(8,128)(2,1)} collective-permute-done((bf16[2048,256]{1,0:T(8,128)(2,1)}, bf16[2048,256]{1,0:T(8,128)(2,1)}, u32[]{:S(2)}, u32[]{:S(2)}) %collective-permute-start.4) | collective-permute-done | bytes 1048608 | tf_op jit(solution)/shard_map/ppermute | solution.py:493
  56.4 0.4 collective-permute-start.6
  56.8 0.0 collective-permute-done.8.refs_6_
  56.8 2.9 %collective-permute-start.9 = (bf16[2048,256]{1,0:T(8,128)(2,1)}, bf16[2048,256]{1,0:T(8,128)(2,1)}, u32[]{:S(2)}, u32[]{:S(2)}) collective-permute-start(bf16[2048,256]{1,0:T(8,128)(2,1)} %collective-permute-done.8.refs_6_), channel_id=1, source_target_pairs={{0,3},{1,0},{2,1},{3,2},{4,7},{5,4},{6,5},{7,6},{8,11},{9,8},{10,9... | collective-permute-start | bytes 3145736 | tf_op jit(solution)/shard_map/ppermute | solution.py:497
  59.7 0.3 fusion
  60.0 7.7 %collective-permute-done.10.refs_1_ = bf16[128,2048]{1,0:T(8,128)(2,1)} collective-permute-done((bf16[128,2048]{1,0:T(8,128)(2,1)}, bf16[128,2048]{1,0:T(8,128)(2,1)}, u32[]{:S(2)}, u32[]{:S(2)}) %collective-permute-start.10) | collective-permute-done | bytes 524320 | tf_op jit(solution)/shard_map/ppermute | solution.py:493
  67.7 1.8 collective-permute-start.13
  69.5 0.5 fusion.6
  70.0 2.9 %convolution_convert_fusion.shared_hbm = bf16[256,2048]{1,0:T(8,128)(2,1)} fusion(bf16[128,2048]{1,0:T(8,128)(2,1)S(1)} %copy-done, bf16[2048,128]{1,0:T(8,128)(2,1)} %param.36, bf16[256,2048]{1,0:T(8,128)(2,1)S(1)} %copy-done.5, f32[2048]{0:T(1024)S(1)} %copy-done.10, f32[256]{0:T(256)S(1)} %add_rsqrt_fusion, f32[256,128]{1,0:T(8,128)S(1)} %fusion.6), kind=kOutput, calls=%fused_computation.2 | convolution fusion | flops 271253504 | bytes 3286016 | tf_op jit(solution)/shard_map/dot_general | solution.py:24
  72.9 0.0 all-to-all-done.got_ref
  72.9 1.1 state_scan.1
  74.0 37.9 %collective-permute-done.13.refs_4_ = bf16[128,2048]{1,0:T(8,128)(2,1)} collective-permute-done((bf16[128,2048]{1,0:T(8,128)(2,1)}, bf16[128,2048]{1,0:T(8,128)(2,1)}, u32[]{:S(2)}, u32[]{:S(2)}) %collective-permute-start.13) | collective-permute-done | bytes 524320 | tf_op jit(solution)/shard_map/ppermute | solution.py:497
  111.8 1.6 collective-permute-start.11
  113.4 0.0 collective-permute-done.5.refs_2_
  113.4 1.7 collective-permute-start.12
  115.1 0.0 collective-permute-done.7.refs_5_
  115.1 0.4 collective-permute-start.14
  115.5 0.0 collective-permute-done.6.refs_3_
  115.5 2.9 %collective-permute-start.15 = (bf16[128,2048]{1,0:T(8,128)(2,1)}, bf16[128,2048]{1,0:T(8,128)(2,1)}, u32[]{:S(2)}, u32[]{:S(2)}) collective-permute-start(bf16[128,2048]{1,0:T(8,128)(2,1)} %collective-permute-done.13.refs_4_), channel_id=1, source_target_pairs={{0,3},{1,0},{2,1},{3,2},{4,7},{5,4},{6,5},{7,6},{8,11},{9,8},{10,9... | collective-permute-start | bytes 1572872 | tf_op jit(solution)/shard_map/ppermute | solution.py:497
  118.3 10.3 %all-to-all-start.1 = ((bf16[64,2,128]{2,1,0:T(2,128)(2,1)}), bf16[64,2,128]{2,1,0:T(2,128)(2,1)S(1)}, u32[]{:S(2)}, u32[]{:S(2)}) async-start(bf16[64,2,128]{2,1,0:T(2,128)(2,1)} %state_scan.1), calls=%async_computation.1 | async-start | bytes 65536 | tf_op jit(solution)/shard_map/all_to_all | solution.py:565
  128.6 0.0 collective-permute-done.9.refs_7_
  128.7 10.0 %hidden_units.1.act_ref = bf16[384,1024]{1,0:T(8,128)(2,1)} custom-call(bf16[64,104,128]{2,1,0:T(8,128)(2,1)} %copy-done.1, bf16[2048,256]{1,0:T(8,128)(2,1)} %bitcast.26, bf16[2048,256]{1,0:T(8,128)(2,1)} %collective-permute-done.4.refs_1_, bf16[2048,256]{1,0:T(8,128)(2,1)} %collective-permute-done.5.refs_2_, ...), custom_call_target="tpu_custom_call" | custom-call | flops 3221225472 | bytes 10485760 | tf_op jit(solution)/shard_map/hidden_units/pallas_call | solution.py:369
  138.6 0.0 all-to-all-done.1
  138.6 0.6 copy.25
  139.2 6.4 %mixer_out.1 = (bf16[192,2048]{1,0:T(8,128)(2,1)}, bf16[192,2048]{1,0:T(8,128)(2,1)}, bf16[96,2048]{1,0:T(8,128)(2,1)}, bf16[96,2048]{1,0:T(8,128)(2,1)}, bf16[192,2048]{1,0:T(8,128)(2,1)}) custom-call(s32[1]{0:T(128)} %bitcast.rank_ref, f32[512,256]{1,0:T(8,128)} %get-tuple-element.16.part_hbm, bf16[512,256]{1,0:T(8,128)(2,1)} %get-tuple-element.17.reach_hbm, ...), custom_call_target="tpu_custom_call" | custom-call | flops 536870912 | bytes 6291456 | tf_op jit(solution)/shard_map/mixer_out/pallas_call | solution.py:205
  145.7 0.3 collective-permute-start
  146.0 0.0 collective-permute-done.11.refs_2_
  146.0 0.0 copy-start.8
  146.0 0.0 collective-permute-done.12.refs_3_
  146.0 0.0 collective-permute-done.15.refs_6_
  146.0 0.7 copy-done.8
  146.8 0.2 copy-done.9
  147.0 7.0 %results.1 = bf16[64,96,128]{2,1,0:T(8,128)(2,1)} custom-call(bf16[384,1024]{1,0:T(8,128)(2,1)} %hidden_units.1.act_ref, bf16[256,2048]{1,0:T(8,128)(2,1)} %bitcast.19, bf16[128,2048]{1,0:T(8,128)(2,1)} %collective-permute-done.10.refs_1_, bf16[128,2048]{1,0:T(8,128)(2,1)} %copy-done.8, bf16[128,2048]{1,0:T(8,128)(2,1)} %copy-done.9, ...), custom_call_target="tpu_custom_call" | custom-call | flops 1610612736 | bytes 6291456 | tf_op jit(solution)/shard_map/results/pallas_call | solution.py:415
  154.0 10.4 %all-to-all-start.2 = ((bf16[64,96,128]{2,1,0:T(8,128)(2,1)}), bf16[64,96,128]{2,1,0:T(8,128)(2,1)S(1)}, u32[]{:S(2)}, u32[]{:S(2)}) async-start(bf16[64,96,128]{2,1,0:T(8,128)(2,1)} %results.1), calls=%async_computation.2 | async-start | bytes 3145728 | tf_op jit(solution)/shard_map/all_to_all | solution.py:582
  164.5 3.3 %collective-permute-start.2 = (bf16[96,2048]{1,0:T(8,128)(2,1)S(1)}, bf16[96,2048]{1,0:T(8,128)(2,1)S(1)}, u32[]{:S(2)}, u32[]{:S(2)}) collective-permute-start(bf16[96,2048]{1,0:T(8,128)(2,1)S(1)} %copy-done.13), channel_id=1, source_target_pairs={{0,3},{1,0},{2,1},{3,2},{4,7},{5,4},{6,5},{7,6},{8,11},{9,8},{10,9... | collective-permute-start | bytes 1179656 | tf_op jit(solution)/shard_map/ppermute | solution.py:497
  167.8 1.1 slice_add_fusion.1
  168.9 0.1 pad_maximum_fusion
  169.0 0.1 collective-permute-start.1
  169.1 7.3 %collective-permute-done.2 = bf16[96,2048]{1,0:T(8,128)(2,1)S(1)} collective-permute-done((bf16[96,2048]{1,0:T(8,128)(2,1)S(1)}, bf16[96,2048]{1,0:T(8,128)(2,1)S(1)}, u32[]{:S(2)}, u32[]{:S(2)}) %collective-permute-start.2) | collective-permute-done | bytes 393248 | tf_op jit(solution)/shard_map/ppermute | solution.py:497
  176.4 0.1 fusion.15
  176.5 1.0 pad_maximum_fusion.1
  177.5 3.7 %collective-permute-start.3 = (bf16[192,2048]{1,0:T(8,128)(2,1)}, bf16[192,2048]{1,0:T(8,128)(2,1)}, u32[]{:S(2)}, u32[]{:S(2)}) collective-permute-start(bf16[192,2048]{1,0:T(8,128)(2,1)} %pad_maximum_fusion.1), channel_id=1, source_target_pairs={{0,3},{1,0},{2,1},{3,2},{4,7},{5,4},{6,5},{7,6},{8,11},{9,8},{10,9... | collective-permute-start | bytes 2359304 | tf_op jit(solution)/shard_map/ppermute | solution.py:497
  181.1 0.1 copy.22.logit_ref
  181.2 8.4 %collective-permute-done.1 = bf16[192,2048]{1,0:T(8,128)(2,1)} collective-permute-done((bf16[192,2048]{1,0:T(8,128)(2,1)S(1)}, bf16[192,2048]{1,0:T(8,128)(2,1)}, u32[]{:S(2)}, u32[]{:S(2)}) %collective-permute-start.1) | collective-permute-done | bytes 786464 | tf_op jit(solution)/shard_map/ppermute | solution.py:493
  189.7 8.0 %collective-permute-done.3 = bf16[192,2048]{1,0:T(8,128)(2,1)} collective-permute-done((bf16[192,2048]{1,0:T(8,128)(2,1)}, bf16[192,2048]{1,0:T(8,128)(2,1)}, u32[]{:S(2)}, u32[]{:S(2)}) %collective-permute-start.3) | collective-permute-done | bytes 786464 | tf_op jit(solution)/shard_map/ppermute | solution.py:497
  197.7 2.0 convert_add_fusion
  199.7 0.9 slice.48
  200.6 3.9 %all-to-all-done.2.got_ref = bf16[64,96,128]{2,1,0:T(8,128)(2,1)S(1)} async-done(((bf16[64,96,128]{2,1,0:T(8,128)(2,1)}), bf16[64,96,128]{2,1,0:T(8,128)(2,1)S(1)}, u32[]{:S(2)}, u32[]{:S(2)}) %all-to-all-start.2) | async-done | bytes 1572896 | tf_op jit(solution)/shard_map/all_to_all | solution.py:582
  204.5 3.1 %combine.1 = bf16[64,2048]{1,0:T(8,128)(2,1)} custom-call(bf16[64,96,128]{2,1,0:T(8,128)(2,1)S(1)} %all-to-all-done.2.got_ref, s32[64,4]{1,0:T(8,128)S(1)} %copy-done.2, f32[64,4]{1,0:T(8,128)S(1)} %copy.22.logit_ref, f32[64,2048]{1,0:T(8,128)S(1)} %slice.42.rest_ref), custom_call_target="tpu_custom_call" | custom-call | tf_op jit(solution)/shard_map/combine/pallas_call | solution.py:480
  (24 shorter events, 0.1 us)
Async XLA Ops:
  0.6 69.4 %copy-start = (bf16[128,2048]{1,0:T(8,128)(2,1)S(1)}, bf16[128,2048]{1,0:T(8,128)(2,1)}, u32[]{:S(2)}) copy-start(bf16[128,2048]{1,0:T(8,128)(2,1)} %param.37) | copy-start | bytes 1572868
  16.6 15.5 %copy-start.3 = (bf16[1,256,2048]{2,1,0:T(8,128)(2,1)S(1)}, bf16[1,256,2048]{2,1,0:T(8,128)(2,1)}, u32[]{:S(2)}) copy-start(bf16[1,256,2048]{2,1,0:T(8,128)(2,1)} %param.34) | copy-start | bytes 3145732
  16.6 56.3 %all-to-all-start = ((bf16[64,104,128]{2,1,0:T(8,128)(2,1)}), bf16[64,104,128]{2,1,0:T(8,128)(2,1)S(1)}, u32[]{:S(2)}, u32[]{:S(2)}) async-start(bf16[64,104,128]{2,1,0:T(8,128)(2,1)} %get-tuple-element.20), calls=%async_computation | async-start | bytes 3407872 | tf_op jit(solution)/shard_map/all_to_all | solution.py:555
  28.7 30.9 %copy-start.4 = (bf16[256,2048]{1,0:T(8,128)(2,1)S(1)}, bf16[256,2048]{1,0:T(8,128)(2,1)}, u32[]{:S(2)}) copy-start(bf16[256,2048]{1,0:T(8,128)(2,1)} %x_ref.3) | copy-start | bytes 3145732
  28.8 40.7 %copy-start.10 = (f32[2048]{0:T(1024)S(1)}, f32[2048]{0:T(1024)}, u32[]{:S(2)}) copy-start(f32[2048]{0:T(1024)} %param.29) | copy-start | bytes 24580
  28.8 40.7 %copy-start.12 = (bf16[2048,128]{1,0:T(8,128)(2,1)S(1)}, bf16[2048,128]{1,0:T(8,128)(2,1)}, u32[]{:S(2)}) copy-start(bf16[2048,128]{1,0:T(8,128)(2,1)} %param.35) | copy-start | bytes 1572868
  28.8 27.6 %collective-permute-start.4 = (bf16[2048,256]{1,0:T(8,128)(2,1)}, bf16[2048,256]{1,0:T(8,128)(2,1)}, u32[]{:S(2)}, u32[]{:S(2)}) collective-permute-start(bf16[2048,256]{1,0:T(8,128)(2,1)} %bitcast.24), channel_id=1, source_target_pairs={{0,1},{1,2},{2,3},{3,0},{4,5},{5,6},{6,7},{7,4},{8,9},{9,10},{10,1... | collective-permute-start | bytes 3145736 | tf_op jit(solution)/shard_map/ppermute | solution.py:493
  30.5 26.3 %collective-permute-start.8 = (bf16[2048,256]{1,0:T(8,128)(2,1)}, bf16[2048,256]{1,0:T(8,128)(2,1)}, u32[]{:S(2)}, u32[]{:S(2)}) collective-permute-start(bf16[2048,256]{1,0:T(8,128)(2,1)} %bitcast.27), channel_id=1, source_target_pairs={{0,3},{1,0},{2,1},{3,2},{4,7},{5,4},{6,5},{7,6},{8,11},{9,8},{10,9... | collective-permute-start | bytes 3145736 | tf_op jit(solution)/shard_map/ppermute | solution.py:497
  33.1 36.8 %copy-start.5 = (bf16[256,2048]{1,0:T(8,128)(2,1)S(1)}, bf16[256,2048]{1,0:T(8,128)(2,1)}, u32[]{:S(2)}) copy-start(bf16[256,2048]{1,0:T(8,128)(2,1)} %x_ref.3) | copy-start | bytes 3145732
  33.1 34.5 %collective-permute-start.10 = (bf16[128,2048]{1,0:T(8,128)(2,1)}, bf16[128,2048]{1,0:T(8,128)(2,1)}, u32[]{:S(2)}, u32[]{:S(2)}) collective-permute-start(bf16[128,2048]{1,0:T(8,128)(2,1)} %get-tuple-element.31), channel_id=1, source_target_pairs={{0,1},{1,2},{2,3},{3,0},{4,5},{5,6},{6,7},{7,4},{8,9},{9,10},{10,1... | collective-permute-start | bytes 1572872 | tf_op jit(solution)/shard_map/ppermute | solution.py:493
  33.5 79.9 %collective-permute-start.5 = (bf16[2048,256]{1,0:T(8,128)(2,1)}, bf16[2048,256]{1,0:T(8,128)(2,1)}, u32[]{:S(2)}, u32[]{:S(2)}) collective-permute-start(bf16[2048,256]{1,0:T(8,128)(2,1)} %bitcast.25), channel_id=1, source_target_pairs={{0,3},{1,0},{2,1},{3,2},{4,7},{5,4},{6,5},{7,6},{8,11},{9,8},{10,9... | collective-permute-start | bytes 3145736 | tf_op jit(solution)/shard_map/ppermute | solution.py:497
  36.4 78.7 %collective-permute-start.7 = (bf16[2048,256]{1,0:T(8,128)(2,1)}, bf16[2048,256]{1,0:T(8,128)(2,1)}, u32[]{:S(2)}, u32[]{:S(2)}) collective-permute-start(bf16[2048,256]{1,0:T(8,128)(2,1)} %bitcast.28), channel_id=1, source_target_pairs={{0,1},{1,2},{2,3},{3,0},{4,5},{5,6},{6,7},{7,4},{8,9},{9,10},{10,1... | collective-permute-start | bytes 3145736 | tf_op jit(solution)/shard_map/ppermute | solution.py:493
  56.4 59.0 %collective-permute-start.6 = (bf16[2048,256]{1,0:T(8,128)(2,1)}, bf16[2048,256]{1,0:T(8,128)(2,1)}, u32[]{:S(2)}, u32[]{:S(2)}) collective-permute-start(bf16[2048,256]{1,0:T(8,128)(2,1)} %collective-permute-done.4.refs_1_), channel_id=1, source_target_pairs={{0,1},{1,2},{2,3},{3,0},{4,5},{5,6},{6,7},{7,4},{8,9},{9,10},{10,1... | collective-permute-start | bytes 3145736 | tf_op jit(solution)/shard_map/ppermute | solution.py:493
  56.8 71.8 %collective-permute-start.9 = (bf16[2048,256]{1,0:T(8,128)(2,1)}, bf16[2048,256]{1,0:T(8,128)(2,1)}, u32[]{:S(2)}, u32[]{:S(2)}) collective-permute-start(bf16[2048,256]{1,0:T(8,128)(2,1)} %collective-permute-done.8.refs_6_), channel_id=1, source_target_pairs={{0,3},{1,0},{2,1},{3,2},{4,7},{5,4},{6,5},{7,6},{8,11},{9,8},{10,9... | collective-permute-start | bytes 3145736 | tf_op jit(solution)/shard_map/ppermute | solution.py:497
  67.7 44.2 %collective-permute-start.13 = (bf16[128,2048]{1,0:T(8,128)(2,1)}, bf16[128,2048]{1,0:T(8,128)(2,1)}, u32[]{:S(2)}, u32[]{:S(2)}) collective-permute-start(bf16[128,2048]{1,0:T(8,128)(2,1)} %get-tuple-element.30), channel_id=1, source_target_pairs={{0,3},{1,0},{2,1},{3,2},{4,7},{5,4},{6,5},{7,6},{8,11},{9,8},{10,9... | collective-permute-start | bytes 1572872 | tf_op jit(solution)/shard_map/ppermute | solution.py:497
  72.9 55.8 %copy-start.1 = (bf16[64,104,128]{2,1,0:T(8,128)(2,1)}, bf16[64,104,128]{2,1,0:T(8,128)(2,1)S(1)}, u32[]{:S(2)}) copy-start(bf16[64,104,128]{2,1,0:T(8,128)(2,1)S(1)} %all-to-all-done.got_ref) | copy-start | bytes 5111812
  111.8 34.1 %collective-permute-start.11 = (bf16[128,2048]{1,0:T(8,128)(2,1)}, bf16[128,2048]{1,0:T(8,128)(2,1)S(1)}, u32[]{:S(2)}, u32[]{:S(2)}) collective-permute-start(bf16[128,2048]{1,0:T(8,128)(2,1)} %get-tuple-element.30), channel_id=1, source_target_pairs={{0,1},{1,2},{2,3},{3,0},{4,5},{5,6},{6,7},{7,4},{8,9},{9,10},{10,1... | collective-permute-start | bytes 1572872 | tf_op jit(solution)/shard_map/ppermute | solution.py:493
  113.4 32.6 %collective-permute-start.12 = (bf16[128,2048]{1,0:T(8,128)(2,1)}, bf16[128,2048]{1,0:T(8,128)(2,1)S(1)}, u32[]{:S(2)}, u32[]{:S(2)}) collective-permute-start(bf16[128,2048]{1,0:T(8,128)(2,1)} %get-tuple-element.31), channel_id=1, source_target_pairs={{0,3},{1,0},{2,1},{3,2},{4,7},{5,4},{6,5},{7,6},{8,11},{9,8},{10,9... | collective-permute-start | bytes 1572872 | tf_op jit(solution)/shard_map/ppermute | solution.py:497
  115.1 30.9 %collective-permute-start.14 = (bf16[128,2048]{1,0:T(8,128)(2,1)}, bf16[128,2048]{1,0:T(8,128)(2,1)}, u32[]{:S(2)}, u32[]{:S(2)}) collective-permute-start(bf16[128,2048]{1,0:T(8,128)(2,1)} %collective-permute-done.10.refs_1_), channel_id=1, source_target_pairs={{0,1},{1,2},{2,3},{3,0},{4,5},{5,6},{6,7},{7,4},{8,9},{9,10},{10,1... | collective-permute-start | bytes 1572872 | tf_op jit(solution)/shard_map/ppermute | solution.py:493
  115.5 30.6 %collective-permute-start.15 = (bf16[128,2048]{1,0:T(8,128)(2,1)}, bf16[128,2048]{1,0:T(8,128)(2,1)}, u32[]{:S(2)}, u32[]{:S(2)}) collective-permute-start(bf16[128,2048]{1,0:T(8,128)(2,1)} %collective-permute-done.13.refs_4_), channel_id=1, source_target_pairs={{0,3},{1,0},{2,1},{3,2},{4,7},{5,4},{6,5},{7,6},{8,11},{9,8},{10,9... | collective-permute-start | bytes 1572872 | tf_op jit(solution)/shard_map/ppermute | solution.py:497
  118.3 20.3 %all-to-all-start.1 = ((bf16[64,2,128]{2,1,0:T(2,128)(2,1)}), bf16[64,2,128]{2,1,0:T(2,128)(2,1)S(1)}, u32[]{:S(2)}, u32[]{:S(2)}) async-start(bf16[64,2,128]{2,1,0:T(2,128)(2,1)} %state_scan.1), calls=%async_computation.1 | async-start | bytes 65536 | tf_op jit(solution)/shard_map/all_to_all | solution.py:565
  145.7 22.1 %collective-permute-start = (bf16[96,2048]{1,0:T(8,128)(2,1)}, bf16[96,2048]{1,0:T(8,128)(2,1)}, u32[]{:S(2)}, u32[]{:S(2)}) collective-permute-start(bf16[96,2048]{1,0:T(8,128)(2,1)} %get-tuple-element.24), channel_id=1, source_target_pairs={{0,1},{1,2},{2,3},{3,0},{4,5},{5,6},{6,7},{7,4},{8,9},{9,10},{10,1... | collective-permute-start | bytes 1179656 | tf_op jit(solution)/shard_map/ppermute | solution.py:493
  146.0 0.8 copy-start.8
  146.0 1.0 copy-start.9
  154.0 10.5 %copy-start.13 = (bf16[96,2048]{1,0:T(8,128)(2,1)S(1)}, bf16[96,2048]{1,0:T(8,128)(2,1)}, u32[]{:S(2)}) copy-start(bf16[96,2048]{1,0:T(8,128)(2,1)} %get-tuple-element.26) | copy-start | bytes 1179652
  154.0 13.8 %copy-start.7 = (bf16[192,2048]{1,0:T(8,128)(2,1)S(1)}, bf16[192,2048]{1,0:T(8,128)(2,1)}, u32[]{:S(2)}) copy-start(bf16[192,2048]{1,0:T(8,128)(2,1)} %get-tuple-element.23) | copy-start | bytes 2359300
  154.0 50.5 %all-to-all-start.2 = ((bf16[64,96,128]{2,1,0:T(8,128)(2,1)}), bf16[64,96,128]{2,1,0:T(8,128)(2,1)S(1)}, u32[]{:S(2)}, u32[]{:S(2)}) async-start(bf16[64,96,128]{2,1,0:T(8,128)(2,1)} %results.1), calls=%async_computation.2 | async-start | bytes 3145728 | tf_op jit(solution)/shard_map/all_to_all | solution.py:582
  164.5 11.9 %collective-permute-start.2 = (bf16[96,2048]{1,0:T(8,128)(2,1)S(1)}, bf16[96,2048]{1,0:T(8,128)(2,1)S(1)}, u32[]{:S(2)}, u32[]{:S(2)}) collective-permute-start(bf16[96,2048]{1,0:T(8,128)(2,1)S(1)} %copy-done.13), channel_id=1, source_target_pairs={{0,3},{1,0},{2,1},{3,2},{4,7},{5,4},{6,5},{7,6},{8,11},{9,8},{10,9... | collective-permute-start | bytes 1179656 | tf_op jit(solution)/shard_map/ppermute | solution.py:497
  167.8 8.7 %copy-start.6 = (bf16[192,2048]{1,0:T(8,128)(2,1)S(1)}, bf16[192,2048]{1,0:T(8,128)(2,1)}, u32[]{:S(2)}) copy-start(bf16[192,2048]{1,0:T(8,128)(2,1)} %get-tuple-element.25) | copy-start | bytes 2359300
  169.0 20.7 %collective-permute-start.1 = (bf16[192,2048]{1,0:T(8,128)(2,1)S(1)}, bf16[192,2048]{1,0:T(8,128)(2,1)}, u32[]{:S(2)}, u32[]{:S(2)}) collective-permute-start(bf16[192,2048]{1,0:T(8,128)(2,1)S(1)} %pad_maximum_fusion), channel_id=1, source_target_pairs={{0,1},{1,2},{2,3},{3,0},{4,5},{5,6},{6,7},{7,4},{8,9},{9,10},{10,1... | collective-permute-start | bytes 2359304 | tf_op jit(solution)/shard_map/ppermute | solution.py:493
  176.4 4.7 %copy-start.11 = (f32[64,4]{0,1:T(4,128)S(1)}, f32[64,4]{0,1:T(4,128)}, u32[]{:S(2)}) copy-start(f32[64,4]{0,1:T(4,128)} %param.31) | copy-start | bytes 3076
  177.5 20.2 %collective-permute-start.3 = (bf16[192,2048]{1,0:T(8,128)(2,1)}, bf16[192,2048]{1,0:T(8,128)(2,1)}, u32[]{:S(2)}, u32[]{:S(2)}) collective-permute-start(bf16[192,2048]{1,0:T(8,128)(2,1)} %pad_maximum_fusion.1), channel_id=1, source_target_pairs={{0,3},{1,0},{2,1},{3,2},{4,7},{5,4},{6,5},{7,6},{8,11},{9,8},{10,9... | collective-permute-start | bytes 2359304 | tf_op jit(solution)/shard_map/ppermute | solution.py:497
  199.7 4.8 %copy-start.2 = (s32[64,4]{1,0:T(8,128)S(1)}, s32[64,4]{1,0:T(8,128)}, u32[]{:S(2)}) copy-start(s32[64,4]{1,0:T(8,128)} %get-tuple-element.29.slot_ref) | copy-start | bytes 3076
